TPU v7x, 512 devices: a whole 4x8x8 slice. The times are simulated.
512 devices in a mesh: ep: 32 (over z, x), tp: 16 (over y, core).
Axes of the slice: x: 4, y: 8, z: 8, core: 2. Of those that a mesh axis runs over, the one named last changes fastest.
Arguments:
- tokens: bfloat16 [8192, 2048], P('ep')
- norm_gain: float32 [2048], replicated, may hold values from 0.1 to 1.9
- chosen: int32 [32, 1024], replicated, may hold values from 0 to 8191, as said below
- route_weight: float32 [32, 1024], P('ep'), may hold values from 0.2 to 1
- gate_weight: bfloat16 [32, 2048, 4096], P('ep', None, 'tp'), may hold values from -0.125 to 0.125
- up_weight: bfloat16 [32, 2048, 4096], P('ep', None, 'tp'), may hold values from -0.125 to 0.125
- down_weight: bfloat16 [32, 4096, 2048], P('ep', 'tp'), may hold values from -0.09375 to 0.09375
Outputs:
- combined: bfloat16 [8192, 2048], P('ep', 'tp')
Inputs may be any that keep to these rules, and one draw needn't show every extreme that they name: Each row of chosen lists 1024 distinct token numbers in ascending order. Of the 256 consecutive tokens of one index of ep, a row holds at most 48, and every draw has rows that hold exactly 48 of them.
All inputs are finite; a program needn't handle non-finite values.
Results may differ from a plain program's by a relative error of at most 0.02.
Values may be sent and summed in bfloat16 or wider, within the bound.
No kernel may reach another device: no remote copies, remote signals or barrier semaphores. Data moves between devices by JAX's collectives and lax.ppermute only.
A program may use at most 64 MiB of HBM per device.

v0:
```python
import functools

import jax
import jax.numpy as jnp
from jax import lax
from jax.experimental import pallas as pl
from jax.experimental.pallas import tpu as pltpu
from jax.sharding import Mesh
from jax.sharding import PartitionSpec as P


BF16 = jnp.bfloat16
F32 = jnp.float32
I32 = jnp.int32
OVER_ROWS = (((0,), (0,)), ((), ()))


def dot(a, b, dims=(((1,), (0,)), ((), ()))):
    return lax.dot_general(a, b, dims, preferred_element_type=F32)


def dispatch_kernel(
    slots, where_ref, tokens_in, gain_in, chosen_in, pick_ref, sent_ref,
    held, tokens_ref, gain_ref, chosen_ref, sems,
):
    copies = [
        pltpu.make_async_copy(chosen_in, chosen_ref, sems.at[0]),
        pltpu.make_async_copy(tokens_in, tokens_ref, sems.at[1]),
        pltpu.make_async_copy(gain_in, gain_ref, sems.at[2]),
    ]
    for copy in copies:
        copy.start()
    copies[0].wait()
    tok_rows, width = tokens_ref.shape
    experts, capacity = chosen_ref.shape
    q, first_token, parity = where_ref[0] & 3, where_ref[2], where_ref[3]
    chosen = chosen_ref[...]
    run_start = jnp.sum((chosen < first_token).astype(I32), axis=1, keepdims=True)
    run_end = jnp.sum((chosen < first_token + tok_rows).astype(I32), axis=1, keepdims=True)
    first = run_start + ((run_start + parity) & 1)
    rank = lax.broadcasted_iota(I32, (slots, capacity), 1)
    step = 2 * lax.broadcasted_iota(I32, (slots, capacity), 0)
    ahead = rank - step
    slot = 2 * lax.broadcasted_iota(I32, (slots, 1), 0)
    column = lax.broadcasted_iota(I32, (slots, tok_rows), 1)
    for e in range(experts):
        start = first[e : e + 1, :]
        token = jnp.sum(
            jnp.where(ahead == start, chosen[e : e + 1, :], 0), axis=1, keepdims=True
        )
        local = jnp.where(slot + start < run_end[e : e + 1, :], token - first_token, tok_rows)
        held[e * slots : (e + 1) * slots, :] = (column == local).astype(F32)
    copies[1].wait()
    copies[2].wait()
    values = tokens_ref[...].astype(F32)
    scale = lax.rsqrt(jnp.mean(values * values, axis=-1, keepdims=True) + 1e-06)
    piece = width // 8
    pick = held[...].astype(BF16)
    pick_ref[...] = pick
    for s in range(2):
        at = pl.multiple_of(s * (width // 2) + q * piece, piece)
        part = tokens_ref[:, pl.ds(at, piece)].astype(F32)
        normed = (part * scale * gain_ref[:, pl.ds(at, piece)]).astype(BF16)
        sent_ref[:, s * piece : (s + 1) * piece] = jnp.dot(
            pick, normed, preferred_element_type=F32
        ).astype(BF16)


def dispatch(tokens, norm_gain, chosen, where, slots):
    experts = chosen.shape[0]
    tok_rows, width = tokens.shape
    rows = experts * slots
    vmem = pl.BlockSpec(memory_space=pltpu.VMEM)
    return pl.pallas_call(
        functools.partial(dispatch_kernel, slots),
        out_shape=(
            jax.ShapeDtypeStruct((rows, tok_rows), BF16),
            jax.ShapeDtypeStruct((rows, width // 4), BF16),
        ),
        in_specs=[pl.BlockSpec(memory_space=pltpu.SMEM)] + [pl.BlockSpec(memory_space=pltpu.HBM)] * 3,
        out_specs=(vmem, vmem),
        scratch_shapes=[
            pltpu.VMEM((rows, tok_rows), F32),
            pltpu.VMEM((tok_rows, width), BF16),
            pltpu.VMEM((1, width), F32),
            pltpu.VMEM(chosen.shape, I32),
            pltpu.SemaphoreType.DMA((3,)),
        ],
        compiler_params=pltpu.CompilerParams(vmem_limit_bytes=60 << 20),
    )(where, tokens, norm_gain.reshape(1, width), chosen)


def flat(rows):
    return rows.reshape(rows.shape[0] * rows.shape[1], rows.shape[2])


def columns(ref, where_ref, k, piece):
    j = (where_ref[0] + k * where_ref[1]) & 7
    return ref[:, pl.ds(pl.multiple_of(j * piece, piece), piece)]


def near_kernel(where_ref, own, major, minor, *refs):
    weights, totals, far_rows, held, sems = refs[:4], refs[4:8], refs[8], refs[9], refs[10]
    y, d = where_ref[0], where_ref[1]
    quarters = (y & 3, (y - d) & 3, (y + d) & 3, (y + 2) & 3)
    copies = [
        [
            pltpu.make_async_copy(
                w.at[:, j], held.at[n, i] if i < 3 else far_rows.at[n], sems.at[n, i]
            )
            for i, j in enumerate(quarters)
        ]
        for n, w in enumerate(weights)
    ]
    for i in range(4):
        for n in range(4):
            copies[n][i].start()
    for n, total in enumerate(totals):
        for copy in copies[n][:3]:
            copy.wait()
        total[...] = (
            dot(own[...], flat(held[n, 0]))
            + dot(major[...], flat(held[n, 1]))
            + dot(minor[...], flat(held[n, 2]))
        )
    for n in range(4):
        copies[n][3].wait()


def far_kernel(where_ref, far, t_gate, t_up, t_gate_m, t_up_m, far_rows, down, down_m, hid, hid_m, first):
    piece = first.shape[1]
    d_own = columns(down, where_ref, 4, piece)
    d_mate = columns(down_m, where_ref, 4, piece)
    mid = far.shape[0] // 2

    def gated(rows, t_g, t_u, w_g, w_u):
        g = t_g[rows, :] + dot(far[rows, :], w_g)
        u = t_u[rows, :] + dot(far[rows, :], w_u)
        return (g / (1.0 + jnp.exp(-g)) * u).astype(BF16)

    w = [flat(far_rows[n]) for n in range(4)]
    for r in range(2):
        rows = slice(r * mid, (r + 1) * mid)
        h_own = gated(rows, t_gate, t_up, w[0], w[1])
        h_mate = gated(rows, t_gate_m, t_up_m, w[2], w[3])
        hid[rows, :] = h_own
        hid_m[rows, :] = h_mate
        first[rows, :] = (dot(h_own, d_own) + dot(h_mate, d_mate)).astype(first.dtype)


def out_kernel(offsets, where_ref, hid, hid_m, down, down_m, *outs):
    piece = outs[0].shape[1]
    for k, out in zip(offsets, outs):
        value = dot(hid[...], columns(down, where_ref, k, piece))
        value = value + dot(hid_m[...], columns(down_m, where_ref, k, piece))
        out[...] = value.astype(out.dtype)


def own_kernel(where_ref, k_slot, got, own):
    row = lax.broadcasted_iota(I32, (own.shape[0], got.shape[0]), 0)
    pick = (row == k_slot[...]).astype(F32).astype(BF16)
    own[...] = dot(pick, got[...]).astype(BF16)


def back_kernel(where_ref, k_slot, own, r_major, r_minor, weight, back):
    row = lax.broadcasted_iota(I32, (back.shape[0], own.shape[0]), 1)
    pick = (row == k_slot[...]).astype(F32).astype(BF16)
    total = own[...] + r_major[...].astype(F32) + r_minor[...].astype(F32)
    weighted = (total * weight[...]).astype(BF16)
    back[...] = dot(pick, weighted).astype(BF16)


def call_vmem(kernel, out_shape, flops, where, arrays, apart=(), scratch=()):
    vmem = pl.BlockSpec(memory_space=pltpu.VMEM)
    return pl.pallas_call(
        kernel,
        out_shape=out_shape,
        in_specs=[pl.BlockSpec(memory_space=pltpu.SMEM)]
        + [vmem] * len(arrays)
        + [pl.BlockSpec(memory_space=pl.ANY)] * len(apart),
        out_specs=tuple(vmem for _ in out_shape),
        scratch_shapes=list(scratch),
        cost_estimate=pl.CostEstimate(flops=flops, bytes_accessed=8 << 20, transcendentals=0),
        compiler_params=pltpu.CompilerParams(vmem_limit_bytes=20 << 20),
    )(where, *arrays, *apart)


def shards(tokens, norm_gain, chosen, route_weight, gate_weight, up_weight, down_weight):
    tok_rows, width = tokens.shape
    experts, capacity = chosen.shape
    p = lax.axis_index("ep")
    y = lax.axis_index("y")
    c = lax.axis_index("c")
    block = width // 16
    piece = 2 * block
    quarter = 2 * piece
    half_rows = capacity // 2
    slots = 3 * tok_rows // 32
    mate = [(0, 1), (1, 0)]
    tp = ("y", "c")
    to_major = [(2 * i + j, 2 * ((i + 1 - 2 * j) % 8) + j) for i in range(8) for j in range(2)]
    to_minor = [(target, source) for source, target in to_major]

    place = jnp.stack([y, 1 - 2 * c, p * tok_rows, c]).astype(I32)
    pick_token, sent = dispatch(tokens, norm_gain, chosen, place, slots)
    got = lax.all_to_all(sent.reshape(experts, slots, quarter), "ep", 0, 0, tiled=True)
    got = got.reshape(experts * slots, quarter)

    gate_w, up_w, down_w, _ = lax.optimization_barrier(
        (gate_weight[0], up_weight[0], down_weight[0], sent)
    )
    gate_m = lax.ppermute(gate_w, "c", mate)
    up_m = lax.ppermute(up_w, "c", mate)
    down_m = lax.ppermute(down_w, "c", mate)

    mine = lax.dynamic_index_in_dim(chosen, p, 0, keepdims=False)
    edges = jnp.arange(experts + 1, dtype=I32) * tok_rows
    src_edge = jnp.sum((mine[None, :] < edges[:, None]).astype(I32), axis=1)
    k_edge = lax.shift_right_logical(src_edge - c + 1, 1)
    k_slot = k_edge[:-1, None] + jnp.arange(slots, dtype=I32)[None, :]
    k_slot = jnp.where(k_slot < k_edge[1:, None], k_slot, half_rows).reshape(experts * slots)
    my_weight = lax.dynamic_index_in_dim(
        route_weight.reshape(half_rows, 2), c, 1, keepdims=True
    )

    (own,) = call_vmem(
        own_kernel,
        [jax.ShapeDtypeStruct((half_rows, quarter), BF16)],
        2 * half_rows * experts * slots * quarter,
        place,
        [k_slot.reshape(1, experts * slots), got],
    )
    major = lax.ppermute(own, tp, to_major)
    minor = lax.ppermute(own, tp, to_minor)
    far = lax.ppermute(major, tp, to_major)

    def view(w):
        return w.reshape(2, 4, piece, w.shape[1])

    units = gate_w.shape[1]
    *totals, far_rows = call_vmem(
        near_kernel,
        [jax.ShapeDtypeStruct((half_rows, units), F32)] * 4
        + [jax.ShapeDtypeStruct((4, 2, piece, units), BF16)],
        2 * half_rows * 3 * quarter * 4 * units,
        place,
        [own, major, minor],
        [view(w) for w in (gate_w, up_w, gate_m, up_m)],
        [pltpu.VMEM((4, 3, 2, piece, units), BF16), pltpu.SemaphoreType.DMA((4, 4))],
    )
    hid_shape = jax.ShapeDtypeStruct((half_rows, units), BF16)
    hid, hid_m, first = call_vmem(
        far_kernel,
        [hid_shape, hid_shape, jax.ShapeDtypeStruct((half_rows, piece), BF16)],
        2 * half_rows * (quarter * 4 * units + 2 * units * piece),
        place,
        [far, *totals, far_rows, down_w, down_m],
    )

    def outs_at(offsets, dtype):
        return call_vmem(
            functools.partial(out_kernel, offsets),
            [jax.ShapeDtypeStruct((half_rows, piece), dtype)] * len(offsets),
            2 * half_rows * 2 * units * len(offsets) * piece,
            place,
            [hid, hid_m, down_w, down_m],
        )

    def passed(mine, received):
        return (mine + received.astype(F32)).astype(BF16)

    r_major = lax.ppermute(first, tp, to_major)
    near_3, far_3 = outs_at((-3, 3), F32)
    r_minor = lax.ppermute(near_3.astype(BF16), tp, to_minor)
    r_major = lax.ppermute(passed(far_3, r_major), tp, to_major)
    near_2, far_2 = outs_at((-2, 2), F32)
    r_minor = lax.ppermute(passed(near_2, r_minor), tp, to_minor)
    r_major = lax.ppermute(passed(far_2, r_major), tp, to_major)
    near_1, far_1, own_out = outs_at((-1, 1, 0), F32)
    r_minor = lax.ppermute(passed(near_1, r_minor), tp, to_minor)
    r_major = lax.ppermute(passed(far_1, r_major), tp, to_major)
    (back,) = call_vmem(
        back_kernel,
        [jax.ShapeDtypeStruct((experts * slots, piece), BF16)],
        2 * experts * slots * half_rows * piece,
        place,
        [k_slot.reshape(experts * slots, 1), own_out, r_major, r_minor, my_weight],
    )
    back = back.reshape(experts, slots, piece)
    returned = lax.all_to_all(back, "ep", 0, 0, tiled=True).reshape(experts * slots, piece)
    part = dot(pick_token, returned, OVER_ROWS)

    other = lax.dynamic_slice_in_dim(part, (1 - c) * block, block, 1).astype(BF16)
    theirs = lax.ppermute(other, "c", mate)
    combined = lax.dynamic_slice_in_dim(part, c * block, block, 1) + theirs.astype(F32)
    return combined.astype(BF16)


def solution(mesh):
    finer = Mesh(mesh.devices.reshape(mesh.shape["ep"], 8, 2), ("ep", "y", "c"))
    tp = ("y", "c")
    in_specs = (
        P("ep", None),
        P(),
        P(),
        P("ep", None),
        P("ep", None, tp),
        P("ep", None, tp),
        P("ep", tp, None),
    )

    return jax.shard_map(
        shards, mesh=finer, in_specs=in_specs, out_specs=P("ep", tp), check_vma=False
    )
```

profile of v0, /device:TPU:1, one launch (start us, length us, event | category | flops | bytes accessed | tf_op | source)
XLA Modules:
  0.0 141.0 jit_solution(15376374284308256631)
XLA Ops:
  0.0 0.6 pad_add_fusion.where_ref
  0.6 3.8 %shard_map.73 = (bf16[768,256]{1,0:T(8,128)(2,1)}, bf16[768,512]{1,0:T(8,128)(2,1)}) custom-call(s32[4]{0:T(128)} %pad_add_fusion.where_ref, bf16[256,2048]{1,0:T(8,128)(2,1)} %tokens_in.1, f32[1,2048]{1,0:T(1,128)} %bitcast.28, s32[32,1024]{1,0:T(8,128)} %chosen_in.1), custom_call_target="tpu_custom_call" | custom-call | tf_op jit(solution)/shard_map/pallas_call | solution.py:74
  4.5 13.8 %all-to-all-start = ((bf16[32,24,512]{2,1,0:T(8,128)(2,1)}), bf16[32,24,512]{2,1,0:T(8,128)(2,1)S(1)}, u32[]{:S(2)}, u32[]{:S(2)}) async-start(bf16[32,24,512]{2,1,0:T(8,128)(2,1)} %bitcast.26), calls=%async_computation | async-start | bytes 1572864 | tf_op jit(solution)/shard_map/all_to_all | solution.py:206
  18.3 2.9 %collective-permute-start.3 = (bf16[2048,256]{1,0:T(8,128)(2,1)}, bf16[2048,256]{1,0:T(8,128)(2,1)}, u32[]{:S(2)}, u32[]{:S(2)}) collective-permute-start(bf16[2048,256]{1,0:T(8,128)(2,1)} %bitcast.8), channel_id=1, source_target_pairs={{0,1},{1,0},{2,3},{3,2},{4,5},{5,4},{6,7},{7,6},{8,9},{9,8},{10,11... | collective-permute-start | bytes 3145736 | tf_op jit(solution)/shard_map/ppermute | solution.py:212
  21.2 1.9 %collective-permute-start.4 = (bf16[2048,256]{1,0:T(8,128)(2,1)}, bf16[2048,256]{1,0:T(8,128)(2,1)}, u32[]{:S(2)}, u32[]{:S(2)}) collective-permute-start(bf16[2048,256]{1,0:T(8,128)(2,1)} %bitcast.9), channel_id=1, source_target_pairs={{0,1},{1,0},{2,3},{3,2},{4,5},{5,4},{6,7},{7,6},{8,9},{9,8},{10,11... | collective-permute-start | bytes 3145736 | tf_op jit(solution)/shard_map/ppermute | solution.py:213
  23.1 2.4 %collective-permute-start.5 = (bf16[256,2048]{1,0:T(8,128)(2,1)S(1)}, bf16[256,2048]{1,0:T(8,128)(2,1)S(1)}, u32[]{:S(2)}, u32[]{:S(2)}) collective-permute-start(bf16[256,2048]{1,0:T(8,128)(2,1)S(1)} %bitcast.19), channel_id=1, source_target_pairs={{0,1},{1,0},{2,3},{3,2},{4,5},{5,4},{6,7},{7,6},{8,9},{9,8},{10,11... | collective-permute-start | bytes 3145736 | tf_op jit(solution)/shard_map/ppermute | solution.py:214
  25.6 0.8 constant_dynamic-slice_fusion.1
  26.3 0.2 convert_reduce_fusion
  26.5 0.1 fusion
  26.6 0.1 iota_add_fusion
  26.7 0.1 add.74
  26.8 0.1 lt.65
  27.0 12.4 %all-to-all-done = bf16[32,24,512]{2,1,0:T(8,128)(2,1)S(1)} async-done(((bf16[32,24,512]{2,1,0:T(8,128)(2,1)}), bf16[32,24,512]{2,1,0:T(8,128)(2,1)S(1)}, u32[]{:S(2)}, u32[]{:S(2)}) %all-to-all-start) | async-done | bytes 786464 | tf_op jit(solution)/shard_map/all_to_all | solution.py:206
  39.4 1.1 shard_map.74.own
  40.5 5.1 %collective-permute-start = (bf16[512,512]{1,0:T(8,128)(2,1)S(1)}, bf16[512,512]{1,0:T(8,128)(2,1)S(1)}, u32[]{:S(2)}, u32[]{:S(2)}) collective-permute-start(bf16[512,512]{1,0:T(8,128)(2,1)S(1)} %shard_map.74.own), channel_id=1, source_target_pairs={{0,2},{1,15},{2,4},{3,1},{4,6},{5,3},{6,8},{7,5},{8,10},{9,7},{10,... | collective-permute-start | bytes 1572872 | tf_op jit(solution)/shard_map/ppermute | solution.py:233
  45.6 1.9 %collective-permute-start.2 = (bf16[512,512]{1,0:T(8,128)(2,1)S(1)}, bf16[512,512]{1,0:T(8,128)(2,1)S(1)}, u32[]{:S(2)}, u32[]{:S(2)}) collective-permute-start(bf16[512,512]{1,0:T(8,128)(2,1)S(1)} %shard_map.74.own), channel_id=1, source_target_pairs={{2,0},{15,1},{4,2},{1,3},{6,4},{3,5},{8,6},{5,7},{10,8},{7,9},{12,... | collective-permute-start | bytes 1572872 | tf_op jit(solution)/shard_map/ppermute | solution.py:234
  47.5 4.6 %collective-permute-done.major = bf16[512,512]{1,0:T(8,128)(2,1)S(1)} collective-permute-done((bf16[512,512]{1,0:T(8,128)(2,1)S(1)}, bf16[512,512]{1,0:T(8,128)(2,1)S(1)}, u32[]{:S(2)}, u32[]{:S(2)}) %collective-permute-start) | collective-permute-done | bytes 524320 | tf_op jit(solution)/shard_map/ppermute | solution.py:233
  52.2 5.3 %collective-permute-start.1 = (bf16[512,512]{1,0:T(8,128)(2,1)S(1)}, bf16[512,512]{1,0:T(8,128)(2,1)S(1)}, u32[]{:S(2)}, u32[]{:S(2)}) collective-permute-start(bf16[512,512]{1,0:T(8,128)(2,1)S(1)} %collective-permute-done.major), channel_id=1, source_target_pairs={{0,2},{1,15},{2,4},{3,1},{4,6},{5,3},{6,8},{7,5},{8,10},{9,7},{10,... | collective-permute-start | bytes 1572872 | tf_op jit(solution)/shard_map/ppermute | solution.py:235
  57.5 3.2 %collective-permute-done.2.minor = bf16[512,512]{1,0:T(8,128)(2,1)S(1)} collective-permute-done((bf16[512,512]{1,0:T(8,128)(2,1)S(1)}, bf16[512,512]{1,0:T(8,128)(2,1)S(1)}, u32[]{:S(2)}, u32[]{:S(2)}) %collective-permute-start.2) | collective-permute-done | bytes 524320 | tf_op jit(solution)/shard_map/ppermute | solution.py:234
  60.7 6.1 %shard_map.75 = (f32[512,256]{1,0:T(8,128)S(1)}, f32[512,256]{1,0:T(8,128)S(1)}, f32[512,256]{1,0:T(8,128)S(1)}, f32[512,256]{1,0:T(8,128)S(1)}, bf16[4,2,256,256]{3,2,1,0:T(8,128)(2,1)S(1)}) custom-call(s32[4]{0:T(128)S(1)} %copy-done.1, bf16[512,512]{1,0:T(8,128)(2,1)S(1)} %shard_map.74.own, bf16[512,512]{1,0:T(8,128)(2,1)S(1)} %collective-permute-done.major, ...), custom_call_target="tpu_custom_call" | custom-call | flops 1610612736 | bytes 8388608 | tf_op jit(solution)/shard_map/pallas_call | solution.py:175
  66.9 1.7 %shard_map.76 = (bf16[512,256]{1,0:T(8,128)(2,1)S(1)}, bf16[512,256]{1,0:T(8,128)(2,1)S(1)}, bf16[512,256]{1,0:T(8,128)(2,1)S(1)}) custom-call(s32[4]{0:T(128)S(1)} %copy-done.1, bf16[512,512]{1,0:T(8,128)(2,1)S(1)} %collective-permute-done.1.far, f32[512,256]{1,0:T(8,128)S(1)} %get-tuple-element.29.t_gate, f32[512,256]{1,0:T(8,128)S(1)} %get-tuple-element.30.t_up, ...), custom_call_target="tpu_custom_call" | custom-call | flops 671088640 | bytes 8388608 | tf_op jit(solution)/shard_map/pallas_call | solution.py:175
  68.6 3.5 %collective-permute-start.6 = (bf16[512,256]{1,0:T(8,128)(2,1)S(1)}, bf16[512,256]{1,0:T(8,128)(2,1)S(1)}, u32[]{:S(2)}, u32[]{:S(2)}) collective-permute-start(bf16[512,256]{1,0:T(8,128)(2,1)S(1)} %get-tuple-element.41), channel_id=1, source_target_pairs={{0,2},{1,15},{2,4},{3,1},{4,6},{5,3},{6,8},{7,5},{8,10},{9,7},{10,... | collective-permute-start | bytes 786440 | tf_op jit(solution)/shard_map/ppermute | solution.py:272
  72.0 0.6 broadcast.40
  72.6 0.6 reduce.3
  73.3 0.2 reshape.117
  73.5 1.0 shard_map.79
  74.5 1.9 %collective-permute-start.10 = (bf16[512,256]{1,0:T(8,128)(2,1)S(1)}, bf16[512,256]{1,0:T(8,128)(2,1)S(1)}, u32[]{:S(2)}, u32[]{:S(2)}) collective-permute-start(bf16[512,256]{1,0:T(8,128)(2,1)S(1)} %convert_element_type.52), channel_id=1, source_target_pairs={{2,0},{15,1},{4,2},{1,3},{6,4},{3,5},{8,6},{5,7},{10,8},{7,9},{12,... | collective-permute-start | bytes 786440 | tf_op jit(solution)/shard_map/ppermute | solution.py:274
  76.5 4.6 %collective-permute-start.7 = (bf16[512,256]{1,0:T(8,128)(2,1)S(1)}, bf16[512,256]{1,0:T(8,128)(2,1)S(1)}, u32[]{:S(2)}, u32[]{:S(2)}) collective-permute-start(bf16[512,256]{1,0:T(8,128)(2,1)S(1)} %add_convert_fusion.4), channel_id=1, source_target_pairs={{0,2},{1,15},{2,4},{3,1},{4,6},{5,3},{6,8},{7,5},{8,10},{9,7},{10,... | collective-permute-start | bytes 786440 | tf_op jit(solution)/shard_map/ppermute | solution.py:275
  81.1 1.0 shard_map.78
  82.1 3.6 %collective-permute-done.10 = bf16[512,256]{1,0:T(8,128)(2,1)S(1)} collective-permute-done((bf16[512,256]{1,0:T(8,128)(2,1)S(1)}, bf16[512,256]{1,0:T(8,128)(2,1)S(1)}, u32[]{:S(2)}, u32[]{:S(2)}) %collective-permute-start.10) | collective-permute-done | bytes 262176 | tf_op jit(solution)/shard_map/ppermute | solution.py:274
  85.8 1.9 %collective-permute-start.11 = (bf16[512,256]{1,0:T(8,128)(2,1)S(1)}, bf16[512,256]{1,0:T(8,128)(2,1)S(1)}, u32[]{:S(2)}, u32[]{:S(2)}) collective-permute-start(bf16[512,256]{1,0:T(8,128)(2,1)S(1)} %add_convert_fusion.1), channel_id=1, source_target_pairs={{2,0},{15,1},{4,2},{1,3},{6,4},{3,5},{8,6},{5,7},{10,8},{7,9},{12,... | collective-permute-start | bytes 786440 | tf_op jit(solution)/shard_map/ppermute | solution.py:277
  87.8 4.6 %collective-permute-start.8 = (bf16[512,256]{1,0:T(8,128)(2,1)S(1)}, bf16[512,256]{1,0:T(8,128)(2,1)S(1)}, u32[]{:S(2)}, u32[]{:S(2)}) collective-permute-start(bf16[512,256]{1,0:T(8,128)(2,1)S(1)} %add_convert_fusion.3), channel_id=1, source_target_pairs={{0,2},{1,15},{2,4},{3,1},{4,6},{5,3},{6,8},{7,5},{8,10},{9,7},{10,... | collective-permute-start | bytes 786440 | tf_op jit(solution)/shard_map/ppermute | solution.py:278
  92.4 1.1 shard_map.77
  93.5 2.8 %collective-permute-done.11 = bf16[512,256]{1,0:T(8,128)(2,1)S(1)} collective-permute-done((bf16[512,256]{1,0:T(8,128)(2,1)S(1)}, bf16[512,256]{1,0:T(8,128)(2,1)S(1)}, u32[]{:S(2)}, u32[]{:S(2)}) %collective-permute-start.11) | collective-permute-done | bytes 262176 | tf_op jit(solution)/shard_map/ppermute | solution.py:277
  96.4 1.9 %collective-permute-start.12 = (bf16[512,256]{1,0:T(8,128)(2,1)S(1)}, bf16[512,256]{1,0:T(8,128)(2,1)S(1)}, u32[]{:S(2)}, u32[]{:S(2)}) collective-permute-start(bf16[512,256]{1,0:T(8,128)(2,1)S(1)} %add_convert_fusion), channel_id=1, source_target_pairs={{2,0},{15,1},{4,2},{1,3},{6,4},{3,5},{8,6},{5,7},{10,8},{7,9},{12,... | collective-permute-start | bytes 786440 | tf_op jit(solution)/shard_map/ppermute | solution.py:280
  98.4 4.6 %collective-permute-start.9 = (bf16[512,256]{1,0:T(8,128)(2,1)S(1)}, bf16[512,256]{1,0:T(8,128)(2,1)S(1)}, u32[]{:S(2)}, u32[]{:S(2)}) collective-permute-start(bf16[512,256]{1,0:T(8,128)(2,1)S(1)} %add_convert_fusion.2), channel_id=1, source_target_pairs={{0,2},{1,15},{2,4},{3,1},{4,6},{5,3},{6,8},{7,5},{8,10},{9,7},{10,... | collective-permute-start | bytes 786440 | tf_op jit(solution)/shard_map/ppermute | solution.py:281
  103.0 0.1 constant_dynamic-slice_fusion.weight
  103.1 0.2 add.84
  103.3 0.2 lt.70
  103.5 2.6 %collective-permute-done.12.r_minor = bf16[512,256]{1,0:T(8,128)(2,1)S(1)} collective-permute-done((bf16[512,256]{1,0:T(8,128)(2,1)S(1)}, bf16[512,256]{1,0:T(8,128)(2,1)S(1)}, u32[]{:S(2)}, u32[]{:S(2)}) %collective-permute-start.12) | collective-permute-done | bytes 262176 | tf_op jit(solution)/shard_map/ppermute | solution.py:280
  106.1 0.2 collective-permute-done.9.r_major
  106.3 1.8 %shard_map.80 = bf16[768,256]{1,0:T(8,128)(2,1)} custom-call(s32[4]{0:T(128)S(1)} %copy-done.1, s32[768,1]{1,0:T(8,128)S(1)} %compare_select_fusion.k_slot, f32[512,256]{1,0:T(8,128)S(1)} %get-tuple-element.37.own, bf16[512,256]{1,0:T(8,128)(2,1)S(1)} %collective-permute-done.9.r_major, bf16[512,256]{1,0:T(8,128)(2,1)S(1)} %collective-permute-done.12.r_minor, ...), custom_call_target="tpu_custom_call" | custom-call | flops 201326592 | bytes 8388608 | tf_op jit(solution)/shard_map/pallas_call | solution.py:175
  108.1 7.1 %all-to-all-start.1 = ((bf16[32,24,256]{2,1,0:T(8,128)(2,1)}), bf16[32,24,256]{2,1,0:T(8,128)(2,1)S(1)}, u32[]{:S(2)}, u32[]{:S(2)}) async-start(bf16[32,24,256]{2,1,0:T(8,128)(2,1)} %bitcast.15), calls=%async_computation.1 | async-start | bytes 786432 | tf_op jit(solution)/shard_map/all_to_all | solution.py:290
  115.2 11.4 %all-to-all-done.1 = bf16[32,24,256]{2,1,0:T(8,128)(2,1)S(1)} async-done(((bf16[32,24,256]{2,1,0:T(8,128)(2,1)}), bf16[32,24,256]{2,1,0:T(8,128)(2,1)S(1)}, u32[]{:S(2)}, u32[]{:S(2)}) %all-to-all-start.1) | async-done | bytes 393248 | tf_op jit(solution)/shard_map/all_to_all | solution.py:290
  126.7 0.3 fusion.1
  127.0 12.5 %collective-permute-start.13 = (bf16[256,128]{1,0:T(8,128)(2,1)S(1)}, bf16[256,128]{1,0:T(8,128)(2,1)S(1)}, u32[]{:S(2)}, u32[]{:S(2)}) collective-permute-start(bf16[256,128]{1,0:T(8,128)(2,1)S(1)} %dynamic-slice_convert_fusion), channel_id=1, source_target_pairs={{0,1},{1,0},{2,3},{3,2},{4,5},{5,4},{6,7},{7,6},{8,9},{9,8},{10,11... | collective-permute-start | bytes 196616 | tf_op jit(solution)/shard_map/ppermute | solution.py:294
  139.5 0.9 collective-permute-done.13
  140.4 0.6 add_convert_fusion.5
  (27 shorter events, 0.5 us)
Async XLA Ops:
  4.4 18.7 %copy-start = (bf16[1,256,2048]{2,1,0:T(8,128)(2,1)S(1)}, bf16[1,256,2048]{2,1,0:T(8,128)(2,1)}, u32[]{:S(2)}) copy-start(bf16[1,256,2048]{2,1,0:T(8,128)(2,1)} %param.13) | copy-start | bytes 3145732
  4.5 34.9 %all-to-all-start = ((bf16[32,24,512]{2,1,0:T(8,128)(2,1)}), bf16[32,24,512]{2,1,0:T(8,128)(2,1)S(1)}, u32[]{:S(2)}, u32[]{:S(2)}) async-start(bf16[32,24,512]{2,1,0:T(8,128)(2,1)} %bitcast.26), calls=%async_computation | async-start | bytes 1572864 | tf_op jit(solution)/shard_map/all_to_all | solution.py:206
  18.3 39.2 %collective-permute-start.3 = (bf16[2048,256]{1,0:T(8,128)(2,1)}, bf16[2048,256]{1,0:T(8,128)(2,1)}, u32[]{:S(2)}, u32[]{:S(2)}) collective-permute-start(bf16[2048,256]{1,0:T(8,128)(2,1)} %bitcast.8), channel_id=1, source_target_pairs={{0,1},{1,0},{2,3},{3,2},{4,5},{5,4},{6,7},{7,6},{8,9},{9,8},{10,11... | collective-permute-start | bytes 3145736 | tf_op jit(solution)/shard_map/ppermute | solution.py:212
  21.2 36.3 %collective-permute-start.4 = (bf16[2048,256]{1,0:T(8,128)(2,1)}, bf16[2048,256]{1,0:T(8,128)(2,1)}, u32[]{:S(2)}, u32[]{:S(2)}) collective-permute-start(bf16[2048,256]{1,0:T(8,128)(2,1)} %bitcast.9), channel_id=1, source_target_pairs={{0,1},{1,0},{2,3},{3,2},{4,5},{5,4},{6,7},{7,6},{8,9},{9,8},{10,11... | collective-permute-start | bytes 3145736 | tf_op jit(solution)/shard_map/ppermute | solution.py:213
  23.1 43.7 %collective-permute-start.5 = (bf16[256,2048]{1,0:T(8,128)(2,1)S(1)}, bf16[256,2048]{1,0:T(8,128)(2,1)S(1)}, u32[]{:S(2)}, u32[]{:S(2)}) collective-permute-start(bf16[256,2048]{1,0:T(8,128)(2,1)S(1)} %bitcast.19), channel_id=1, source_target_pairs={{0,1},{1,0},{2,3},{3,2},{4,5},{5,4},{6,7},{7,6},{8,9},{9,8},{10,11... | collective-permute-start | bytes 3145736 | tf_op jit(solution)/shard_map/ppermute | solution.py:214
  26.9 12.4 %copy-start.1 = (s32[4]{0:T(128)S(1)}, s32[4]{0:T(128)}, u32[]{:S(2)}) copy-start(s32[4]{0:T(128)} %pad_add_fusion.where_ref) | copy-start | bytes 52
  40.5 11.7 %collective-permute-start = (bf16[512,512]{1,0:T(8,128)(2,1)S(1)}, bf16[512,512]{1,0:T(8,128)(2,1)S(1)}, u32[]{:S(2)}, u32[]{:S(2)}) collective-permute-start(bf16[512,512]{1,0:T(8,128)(2,1)S(1)} %shard_map.74.own), channel_id=1, source_target_pairs={{0,2},{1,15},{2,4},{3,1},{4,6},{5,3},{6,8},{7,5},{8,10},{9,7},{10,... | collective-permute-start | bytes 1572872 | tf_op jit(solution)/shard_map/ppermute | solution.py:233
  45.6 15.1 %collective-permute-start.2 = (bf16[512,512]{1,0:T(8,128)(2,1)S(1)}, bf16[512,512]{1,0:T(8,128)(2,1)S(1)}, u32[]{:S(2)}, u32[]{:S(2)}) collective-permute-start(bf16[512,512]{1,0:T(8,128)(2,1)S(1)} %shard_map.74.own), channel_id=1, source_target_pairs={{2,0},{15,1},{4,2},{1,3},{6,4},{3,5},{8,6},{5,7},{10,8},{7,9},{12,... | collective-permute-start | bytes 1572872 | tf_op jit(solution)/shard_map/ppermute | solution.py:234
  52.2 14.7 %collective-permute-start.1 = (bf16[512,512]{1,0:T(8,128)(2,1)S(1)}, bf16[512,512]{1,0:T(8,128)(2,1)S(1)}, u32[]{:S(2)}, u32[]{:S(2)}) collective-permute-start(bf16[512,512]{1,0:T(8,128)(2,1)S(1)} %collective-permute-done.major), channel_id=1, source_target_pairs={{0,2},{1,15},{2,4},{3,1},{4,6},{5,3},{6,8},{7,5},{8,10},{9,7},{10,... | collective-permute-start | bytes 1572872 | tf_op jit(solution)/shard_map/ppermute | solution.py:235
  68.6 4.1 %copy-start.3 = (f32[1,1024]{1,0:T(1,128)S(1)}, f32[1,1024]{1,0:T(1,128)}, u32[]{:S(2)}) copy-start(f32[1,1024]{1,0:T(1,128)} %param.10) | copy-start | bytes 12292
  68.6 7.9 %collective-permute-start.6 = (bf16[512,256]{1,0:T(8,128)(2,1)S(1)}, bf16[512,256]{1,0:T(8,128)(2,1)S(1)}, u32[]{:S(2)}, u32[]{:S(2)}) collective-permute-start(bf16[512,256]{1,0:T(8,128)(2,1)S(1)} %get-tuple-element.41), channel_id=1, source_target_pairs={{0,2},{1,15},{2,4},{3,1},{4,6},{5,3},{6,8},{7,5},{8,10},{9,7},{10,... | collective-permute-start | bytes 786440 | tf_op jit(solution)/shard_map/ppermute | solution.py:272
  74.5 11.2 %collective-permute-start.10 = (bf16[512,256]{1,0:T(8,128)(2,1)S(1)}, bf16[512,256]{1,0:T(8,128)(2,1)S(1)}, u32[]{:S(2)}, u32[]{:S(2)}) collective-permute-start(bf16[512,256]{1,0:T(8,128)(2,1)S(1)} %convert_element_type.52), channel_id=1, source_target_pairs={{2,0},{15,1},{4,2},{1,3},{6,4},{3,5},{8,6},{5,7},{10,8},{7,9},{12,... | collective-permute-start | bytes 786440 | tf_op jit(solution)/shard_map/ppermute | solution.py:274
  76.5 11.2 %collective-permute-start.7 = (bf16[512,256]{1,0:T(8,128)(2,1)S(1)}, bf16[512,256]{1,0:T(8,128)(2,1)S(1)}, u32[]{:S(2)}, u32[]{:S(2)}) collective-permute-start(bf16[512,256]{1,0:T(8,128)(2,1)S(1)} %add_convert_fusion.4), channel_id=1, source_target_pairs={{0,2},{1,15},{2,4},{3,1},{4,6},{5,3},{6,8},{7,5},{8,10},{9,7},{10,... | collective-permute-start | bytes 786440 | tf_op jit(solution)/shard_map/ppermute | solution.py:275
  85.8 10.6 %collective-permute-start.11 = (bf16[512,256]{1,0:T(8,128)(2,1)S(1)}, bf16[512,256]{1,0:T(8,128)(2,1)S(1)}, u32[]{:S(2)}, u32[]{:S(2)}) collective-permute-start(bf16[512,256]{1,0:T(8,128)(2,1)S(1)} %add_convert_fusion.1), channel_id=1, source_target_pairs={{2,0},{15,1},{4,2},{1,3},{6,4},{3,5},{8,6},{5,7},{10,8},{7,9},{12,... | collective-permute-start | bytes 786440 | tf_op jit(solution)/shard_map/ppermute | solution.py:277
  87.8 10.6 %collective-permute-start.8 = (bf16[512,256]{1,0:T(8,128)(2,1)S(1)}, bf16[512,256]{1,0:T(8,128)(2,1)S(1)}, u32[]{:S(2)}, u32[]{:S(2)}) collective-permute-start(bf16[512,256]{1,0:T(8,128)(2,1)S(1)} %add_convert_fusion.3), channel_id=1, source_target_pairs={{0,2},{1,15},{2,4},{3,1},{4,6},{5,3},{6,8},{7,5},{8,10},{9,7},{10,... | collective-permute-start | bytes 786440 | tf_op jit(solution)/shard_map/ppermute | solution.py:278
  96.4 9.7 %collective-permute-start.12 = (bf16[512,256]{1,0:T(8,128)(2,1)S(1)}, bf16[512,256]{1,0:T(8,128)(2,1)S(1)}, u32[]{:S(2)}, u32[]{:S(2)}) collective-permute-start(bf16[512,256]{1,0:T(8,128)(2,1)S(1)} %add_convert_fusion), channel_id=1, source_target_pairs={{2,0},{15,1},{4,2},{1,3},{6,4},{3,5},{8,6},{5,7},{10,8},{7,9},{12,... | collective-permute-start | bytes 786440 | tf_op jit(solution)/shard_map/ppermute | solution.py:280
  98.4 7.9 %collective-permute-start.9 = (bf16[512,256]{1,0:T(8,128)(2,1)S(1)}, bf16[512,256]{1,0:T(8,128)(2,1)S(1)}, u32[]{:S(2)}, u32[]{:S(2)}) collective-permute-start(bf16[512,256]{1,0:T(8,128)(2,1)S(1)} %add_convert_fusion.2), channel_id=1, source_target_pairs={{0,2},{1,15},{2,4},{3,1},{4,6},{5,3},{6,8},{7,5},{8,10},{9,7},{10,... | collective-permute-start | bytes 786440 | tf_op jit(solution)/shard_map/ppermute | solution.py:281
  108.1 18.6 %copy-start.2 = (bf16[768,256]{1,0:T(8,128)(2,1)S(1)}, bf16[768,256]{1,0:T(8,128)(2,1)}, u32[]{:S(2)}) copy-start(bf16[768,256]{1,0:T(8,128)(2,1)} %get-tuple-element.25) | copy-start | bytes 1179652
  108.1 18.6 %all-to-all-start.1 = ((bf16[32,24,256]{2,1,0:T(8,128)(2,1)}), bf16[32,24,256]{2,1,0:T(8,128)(2,1)S(1)}, u32[]{:S(2)}, u32[]{:S(2)}) async-start(bf16[32,24,256]{2,1,0:T(8,128)(2,1)} %bitcast.15), calls=%async_computation.1 | async-start | bytes 786432 | tf_op jit(solution)/shard_map/all_to_all | solution.py:290
  127.0 13.4 %collective-permute-start.13 = (bf16[256,128]{1,0:T(8,128)(2,1)S(1)}, bf16[256,128]{1,0:T(8,128)(2,1)S(1)}, u32[]{:S(2)}, u32[]{:S(2)}) collective-permute-start(bf16[256,128]{1,0:T(8,128)(2,1)S(1)} %dynamic-slice_convert_fusion), channel_id=1, source_target_pairs={{0,1},{1,0},{2,3},{3,2},{4,5},{5,4},{6,7},{7,6},{8,9},{9,8},{10,11... | collective-permute-start | bytes 196616 | tf_op jit(solution)/shard_map/ppermute | solution.py:294
where the time goes:
time: 142 us; the launch traced here: 141 us
  starting transfers between devices  75.9 us (53%)
  waiting for transfers between devices  41.8 us (29%)
  Pallas kernels  17.7 us (12%)
  other arithmetic  2.51 us (2%)
  local copies, waits for them, and re-layouts  2.37 us (2%)
    all_to_all x1, starting transfers between devices, shards(): lax.all_to_all(sent.reshape(experts, slots, quarter), 'ep', 0, 0, tiled=T...  13.8 us
    pallas_call x7, Pallas kernels, call_vmem(): pl.pallas_call(kernel, out_shape=out_shape, in_specs=[pl.BlockSpec(memory...  13.8 us
    ppermute x1, starting transfers between devices, shards(): theirs = lax.ppermute(other, 'c', mate)  12.5 us
    all_to_all x1, waiting for transfers between devices, shards(): lax.all_to_all(sent.reshape(experts, slots, quarter), 'ep', 0, 0, tiled=T...  12.4 us
    all_to_all x1, waiting for transfers between devices, shards(): lax.all_to_all(back, 'ep', 0, 0, tiled=True).reshape(experts * slots, piece)  11.4 us
    all_to_all x1, starting transfers between devices, shards(): lax.all_to_all(back, 'ep', 0, 0, tiled=True).reshape(experts * slots, piece)  7.12 us
    ppermute x1, starting transfers between devices, shards(): far = lax.ppermute(major, tp, to_major)  5.31 us
    ppermute x1, starting transfers between devices, shards(): major = lax.ppermute(own, tp, to_major)  5.09 us
  transfers between devices with their start and end apart: 16, of which 9 were waited for; matrix products, arithmetic and copies ran while one was open for 3% of the time, Pallas kernels for 7%

commit v1 on v0

--- a/solution.py
+++ b/solution.py
@@ -99,7 +99,7 @@
     return ref[:, pl.ds(pl.multiple_of(j * piece, piece), piece)]
 
 
-def near_kernel(where_ref, own, major, minor, *refs):
+def near_kernel(where_ref, own, major_a, major_b, minor_a, minor_b, *refs):
     weights, totals, far_rows, held, sems = refs[:4], refs[4:8], refs[8], refs[9], refs[10]
     y, d = where_ref[0], where_ref[1]
     quarters = (y & 3, (y - d) & 3, (y + d) & 3, (y + 2) & 3)
@@ -112,40 +112,46 @@
         ]
         for n, w in enumerate(weights)
     ]
-    for i in range(4):
-        for n in range(4):
-            copies[n][i].start()
+    for row in copies:
+        for copy in row[:3]:
+            copy.start()
+    for row in copies:
+        row[3].start()
+    mid = major_a.shape[0]
     for n, total in enumerate(totals):
         for copy in copies[n][:3]:
             copy.wait()
-        total[...] = (
-            dot(own[...], flat(held[n, 0]))
-            + dot(major[...], flat(held[n, 1]))
-            + dot(minor[...], flat(held[n, 2]))
-        )
-    for n in range(4):
-        copies[n][3].wait()
-
-
-def far_kernel(where_ref, far, t_gate, t_up, t_gate_m, t_up_m, far_rows, down, down_m, hid, hid_m, first):
-    piece = first.shape[1]
+        w_own, w_major, w_minor = [flat(held[n, i]) for i in range(3)]
+        for r, (major, minor) in enumerate(((major_a, minor_a), (major_b, minor_b))):
+            rows = slice(r * mid, (r + 1) * mid)
+            total[rows, :] = (
+                dot(own[rows, :], w_own) + dot(major[...], w_major) + dot(minor[...], w_minor)
+            )
+    for row in copies:
+        row[3].wait()
+
+
+def far_kernel(
+    where_ref, far_a, far_b, t_gate, t_up, t_gate_m, t_up_m, far_rows, down, down_m,
+    hid, hid_m, first_a, first_b,
+):
+    mid, piece = first_a.shape
     d_own = columns(down, where_ref, 4, piece)
     d_mate = columns(down_m, where_ref, 4, piece)
-    mid = far.shape[0] // 2
-
-    def gated(rows, t_g, t_u, w_g, w_u):
-        g = t_g[rows, :] + dot(far[rows, :], w_g)
-        u = t_u[rows, :] + dot(far[rows, :], w_u)
-        return (g / (1.0 + jnp.exp(-g)) * u).astype(BF16)
-
     w = [flat(far_rows[n]) for n in range(4)]
-    for r in range(2):
+    for r, (far, first) in enumerate(((far_a, first_a), (far_b, first_b))):
         rows = slice(r * mid, (r + 1) * mid)
-        h_own = gated(rows, t_gate, t_up, w[0], w[1])
-        h_mate = gated(rows, t_gate_m, t_up_m, w[2], w[3])
+
+        def gated(t_g, t_u, w_g, w_u):
+            g = t_g[rows, :] + dot(far[...], w_g)
+            u = t_u[rows, :] + dot(far[...], w_u)
+            return (g / (1.0 + jnp.exp(-g)) * u).astype(BF16)
+
+        h_own = gated(t_gate, t_up, w[0], w[1])
+        h_mate = gated(t_gate_m, t_up_m, w[2], w[3])
         hid[rows, :] = h_own
         hid_m[rows, :] = h_mate
-        first[rows, :] = (dot(h_own, d_own) + dot(h_mate, d_mate)).astype(first.dtype)
+        first[...] = (dot(h_own, d_own) + dot(h_mate, d_mate)).astype(first.dtype)
 
 
 def out_kernel(offsets, where_ref, hid, hid_m, down, down_m, *outs):
@@ -156,10 +162,14 @@
         out[...] = value.astype(out.dtype)
 
 
-def own_kernel(where_ref, k_slot, got, own):
+def own_kernel(where_ref, k_slot, got, own, own_a, own_b):
     row = lax.broadcasted_iota(I32, (own.shape[0], got.shape[0]), 0)
     pick = (row == k_slot[...]).astype(F32).astype(BF16)
-    own[...] = dot(pick, got[...]).astype(BF16)
+    rows = dot(pick, got[...]).astype(BF16)
+    mid = own_a.shape[0]
+    own[...] = rows
+    own_a[...] = rows[:mid, :]
+    own_b[...] = rows[mid:, :]
 
 
 def back_kernel(where_ref, k_slot, own, r_major, r_minor, weight, back):
@@ -198,8 +208,13 @@
     slots = 3 * tok_rows // 32
     mate = [(0, 1), (1, 0)]
     tp = ("y", "c")
-    to_major = [(2 * i + j, 2 * ((i + 1 - 2 * j) % 8) + j) for i in range(8) for j in range(2)]
-    to_minor = [(target, source) for source, target in to_major]
+    to_major, to_major_2 = [
+        [(2 * i + j, 2 * ((i + k * (1 - 2 * j)) % 8) + j) for i in range(8) for j in range(2)]
+        for k in (1, 2)
+    ]
+    to_minor, to_minor_2 = [
+        [(target, source) for source, target in pairs] for pairs in (to_major, to_major_2)
+    ]
 
     place = jnp.stack([y, 1 - 2 * c, p * tok_rows, c]).astype(I32)
     pick_token, sent = dispatch(tokens, norm_gain, chosen, place, slots)
@@ -223,16 +238,23 @@
         route_weight.reshape(half_rows, 2), c, 1, keepdims=True
     )
 
-    (own,) = call_vmem(
+    k_row, k_column = k_slot.reshape(1, experts * slots), k_slot.reshape(experts * slots, 1)
+    k_row, k_column, my_weight, got = lax.optimization_barrier((k_row, k_column, my_weight, got))
+    mid = half_rows // 2
+    mid_shape = jax.ShapeDtypeStruct((mid, quarter), BF16)
+    own, own_a, own_b = call_vmem(
         own_kernel,
-        [jax.ShapeDtypeStruct((half_rows, quarter), BF16)],
+        [jax.ShapeDtypeStruct((half_rows, quarter), BF16), mid_shape, mid_shape],
         2 * half_rows * experts * slots * quarter,
         place,
-        [k_slot.reshape(1, experts * slots), got],
-    )
-    major = lax.ppermute(own, tp, to_major)
-    minor = lax.ppermute(own, tp, to_minor)
-    far = lax.ppermute(major, tp, to_major)
+        [k_row, got],
+    )
+    major_a = lax.ppermute(own_a, tp, to_major)
+    minor_b = lax.ppermute(own_b, tp, to_minor)
+    major_b = lax.ppermute(own_b, tp, to_major)
+    minor_a = lax.ppermute(own_a, tp, to_minor)
+    far_a = lax.ppermute(major_a, tp, to_major)
+    far_b = lax.ppermute(minor_b, tp, to_minor)
 
     def view(w):
         return w.reshape(2, 4, piece, w.shape[1])
@@ -244,17 +266,18 @@
         + [jax.ShapeDtypeStruct((4, 2, piece, units), BF16)],
         2 * half_rows * 3 * quarter * 4 * units,
         place,
-        [own, major, minor],
+        [own, major_a, major_b, minor_a, minor_b],
         [view(w) for w in (gate_w, up_w, gate_m, up_m)],
         [pltpu.VMEM((4, 3, 2, piece, units), BF16), pltpu.SemaphoreType.DMA((4, 4))],
     )
     hid_shape = jax.ShapeDtypeStruct((half_rows, units), BF16)
-    hid, hid_m, first = call_vmem(
+    first_shape = jax.ShapeDtypeStruct((mid, piece), BF16)
+    hid, hid_m, first_a, first_b = call_vmem(
         far_kernel,
-        [hid_shape, hid_shape, jax.ShapeDtypeStruct((half_rows, piece), BF16)],
+        [hid_shape, hid_shape, first_shape, first_shape],
         2 * half_rows * (quarter * 4 * units + 2 * units * piece),
         place,
-        [far, *totals, far_rows, down_w, down_m],
+        [far_a, far_b, *totals, far_rows, down_w, down_m],
     )
 
     def outs_at(offsets, dtype):
@@ -269,22 +292,25 @@
     def passed(mine, received):
         return (mine + received.astype(F32)).astype(BF16)
 
-    r_major = lax.ppermute(first, tp, to_major)
-    near_3, far_3 = outs_at((-3, 3), F32)
-    r_minor = lax.ppermute(near_3.astype(BF16), tp, to_minor)
-    r_major = lax.ppermute(passed(far_3, r_major), tp, to_major)
-    near_2, far_2 = outs_at((-2, 2), F32)
-    r_minor = lax.ppermute(passed(near_2, r_minor), tp, to_minor)
-    r_major = lax.ppermute(passed(far_2, r_major), tp, to_major)
-    near_1, far_1, own_out = outs_at((-1, 1, 0), F32)
-    r_minor = lax.ppermute(passed(near_1, r_minor), tp, to_minor)
-    r_major = lax.ppermute(passed(far_1, r_major), tp, to_major)
+    jump_major = lax.ppermute(first_a, tp, to_major_2)
+    jump_minor = lax.ppermute(first_b, tp, to_minor_2)
+    major_3, minor_3 = outs_at((3, -3), BF16)
+    r_major = lax.ppermute(major_3, tp, to_major)
+    r_minor = lax.ppermute(minor_3, tp, to_minor)
+    major_2, minor_2 = outs_at((2, -2), F32)
+    major_2 = major_2 + jnp.pad(jump_major.astype(F32), ((0, mid), (0, 0)))
+    minor_2 = minor_2 + jnp.pad(jump_minor.astype(F32), ((mid, 0), (0, 0)))
+    r_major = lax.ppermute(passed(major_2, r_major), tp, to_major)
+    r_minor = lax.ppermute(passed(minor_2, r_minor), tp, to_minor)
+    major_1, minor_1, own_out = outs_at((1, -1, 0), F32)
+    r_major = lax.ppermute(passed(major_1, r_major), tp, to_major)
+    r_minor = lax.ppermute(passed(minor_1, r_minor), tp, to_minor)
     (back,) = call_vmem(
         back_kernel,
         [jax.ShapeDtypeStruct((experts * slots, piece), BF16)],
         2 * experts * slots * half_rows * piece,
         place,
-        [k_slot.reshape(experts * slots, 1), own_out, r_major, r_minor, my_weight],
+        [k_column, own_out, r_major, r_minor, my_weight],
     )
     back = back.reshape(experts, slots, piece)
     returned = lax.all_to_all(back, "ep", 0, 0, tiled=True).reshape(experts * slots, piece)

time: 142 us -> 141 us (level)
  waiting for transfers between devices: 41.8 us -> 35.2 us
  starting transfers between devices: 75.9 us -> 81.4 us
  Pallas kernels: 17.7 us -> 15.6 us
  local copies, waits for them, and re-layouts: 2.37 us -> 3.91 us
    ppermute x10 -> x14, starting transfers between devices: 35.3 us -> 43.3 us  [the longest x1 5.09 us: shards(): major_a = lax.ppermute(own_a, tp, to_major)]
    all_to_all x1, waiting for transfers between devices: 12.4 us -> 7.75 us  [shards(): lax.all_to_all(sent.reshape(experts, slots, quarter), 'ep', 0, 0, tiled=T...]
    ppermute x1, starting transfers between devices: 12.5 us -> 8.64 us  [shards(): theirs = lax.ppermute(other, 'c', mate)]
    pallas_call x7, Pallas kernels: 13.8 us -> 11.8 us  [call_vmem(): pl.pallas_call(kernel, out_shape=out_shape, in_specs=[pl.BlockSpec(memory...]
    ppermute x10 -> x14, waiting for transfers between devices: 17.1 us -> 15.1 us  [the longest x1 3.11 us: shards(): r_minor = lax.ppermute(passed(minor_1, r_minor), tp, to_minor)]
  transfers between devices with their start and end apart: 16 -> 20, of which waited for: 9 -> 10; matrix products, arithmetic and copies ran while one was open for 3% -> 4% of each run, Pallas kernels for 7% -> 5%
where the time goes in v1:
time: 141 us
  starting transfers between devices  81.4 us (58%)
  waiting for transfers between devices  35.2 us (25%)
  Pallas kernels  15.6 us (11%)
  local copies, waits for them, and re-layouts  3.91 us (3%)
  other arithmetic  3.69 us (3%)
    all_to_all x1, starting transfers between devices, shards(): lax.all_to_all(sent.reshape(experts, slots, quarter), 'ep', 0, 0, tiled=T...  13.8 us
    pallas_call x7, Pallas kernels, call_vmem(): pl.pallas_call(kernel, out_shape=out_shape, in_specs=[pl.BlockSpec(memory...  11.8 us
    all_to_all x1, waiting for transfers between devices, shards(): lax.all_to_all(back, 'ep', 0, 0, tiled=True).reshape(experts * slots, piece)  11.4 us
    ppermute x1, starting transfers between devices, shards(): theirs = lax.ppermute(other, 'c', mate)  8.64 us
    all_to_all x1, starting transfers between devices, shards(): lax.all_to_all(back, 'ep', 0, 0, tiled=True).reshape(experts * slots, piece)  8.36 us
    all_to_all x1, waiting for transfers between devices, shards(): lax.all_to_all(sent.reshape(experts, slots, quarter), 'ep', 0, 0, tiled=T...  7.75 us
    ppermute x1, starting transfers between devices, shards(): major_a = lax.ppermute(own_a, tp, to_major)  5.09 us
    ppermute x1, starting transfers between devices, shards(): major_b = lax.ppermute(own_b, tp, to_major)  4.57 us
  transfers between devices with their start and end apart: 20, of which 10 were waited for; matrix products, arithmetic and copies ran while one was open for 4% of the time, Pallas kernels for 5%

profile of v1, /device:TPU:1, one launch (start us, length us, event | category | flops | bytes accessed | tf_op | source)
XLA Modules:
  0.0 140.6 jit_solution(9896080907186600026)
XLA Ops:
  0.0 0.7 pad_add_fusion.where_ref
  0.7 3.9 %shard_map.73 = (bf16[768,256]{1,0:T(8,128)(2,1)}, bf16[768,512]{1,0:T(8,128)(2,1)}) custom-call(s32[4]{0:T(128)} %pad_add_fusion.where_ref, bf16[256,2048]{1,0:T(8,128)(2,1)} %tokens_in.1, f32[1,2048]{1,0:T(1,128)} %bitcast.28, s32[32,1024]{1,0:T(8,128)} %chosen_in.1), custom_call_target="tpu_custom_call" | custom-call | tf_op jit(solution)/shard_map/pallas_call | solution.py:74
  4.5 13.8 %all-to-all-start = ((bf16[32,24,512]{2,1,0:T(8,128)(2,1)}), bf16[32,24,512]{2,1,0:T(8,128)(2,1)S(1)}, u32[]{:S(2)}, u32[]{:S(2)}) async-start(bf16[32,24,512]{2,1,0:T(8,128)(2,1)} %bitcast.26), calls=%async_computation | async-start | bytes 1572864 | tf_op jit(solution)/shard_map/all_to_all | solution.py:221
  18.4 2.9 %collective-permute-start.6 = (bf16[2048,256]{1,0:T(8,128)(2,1)}, bf16[2048,256]{1,0:T(8,128)(2,1)}, u32[]{:S(2)}, u32[]{:S(2)}) collective-permute-start(bf16[2048,256]{1,0:T(8,128)(2,1)} %bitcast.8), channel_id=1, source_target_pairs={{0,1},{1,0},{2,3},{3,2},{4,5},{5,4},{6,7},{7,6},{8,9},{9,8},{10,11... | collective-permute-start | bytes 3145736 | tf_op jit(solution)/shard_map/ppermute | solution.py:227
  21.3 1.9 %collective-permute-start.7 = (bf16[2048,256]{1,0:T(8,128)(2,1)}, bf16[2048,256]{1,0:T(8,128)(2,1)}, u32[]{:S(2)}, u32[]{:S(2)}) collective-permute-start(bf16[2048,256]{1,0:T(8,128)(2,1)} %bitcast.9), channel_id=1, source_target_pairs={{0,1},{1,0},{2,3},{3,2},{4,5},{5,4},{6,7},{7,6},{8,9},{9,8},{10,11... | collective-permute-start | bytes 3145736 | tf_op jit(solution)/shard_map/ppermute | solution.py:228
  23.2 2.4 %collective-permute-start.8 = (bf16[256,2048]{1,0:T(8,128)(2,1)S(1)}, bf16[256,2048]{1,0:T(8,128)(2,1)S(1)}, u32[]{:S(2)}, u32[]{:S(2)}) collective-permute-start(bf16[256,2048]{1,0:T(8,128)(2,1)S(1)} %bitcast.19), channel_id=1, source_target_pairs={{0,1},{1,0},{2,3},{3,2},{4,5},{5,4},{6,7},{7,6},{8,9},{9,8},{10,11... | collective-permute-start | bytes 3145736 | tf_op jit(solution)/shard_map/ppermute | solution.py:229
  25.6 0.8 constant_dynamic-slice_fusion.1
  26.7 0.6 broadcast.44
  27.3 0.7 reduce.3
  28.0 0.2 reshape.111
  28.4 0.9 add.92
  29.5 0.9 lt.70
  30.5 1.2 compare_select_fusion.k_slot
  31.7 7.7 %all-to-all-done = bf16[32,24,512]{2,1,0:T(8,128)(2,1)S(1)} async-done(((bf16[32,24,512]{2,1,0:T(8,128)(2,1)}), bf16[32,24,512]{2,1,0:T(8,128)(2,1)S(1)}, u32[]{:S(2)}, u32[]{:S(2)}) %all-to-all-start) | async-done | bytes 786464 | tf_op jit(solution)/shard_map/all_to_all | solution.py:221
  39.5 1.1 shard_map.74
  40.6 5.1 %collective-permute-start = (bf16[256,512]{1,0:T(8,128)(2,1)S(1)}, bf16[256,512]{1,0:T(8,128)(2,1)S(1)}, u32[]{:S(2)}, u32[]{:S(2)}) collective-permute-start(bf16[256,512]{1,0:T(8,128)(2,1)S(1)} %get-tuple-element.38), channel_id=1, source_target_pairs={{0,2},{1,15},{2,4},{3,1},{4,6},{5,3},{6,8},{7,5},{8,10},{9,7},{10,... | collective-permute-start | bytes 786440 | tf_op jit(solution)/shard_map/ppermute | solution.py:252
  45.7 1.9 %collective-permute-start.2 = (bf16[256,512]{1,0:T(8,128)(2,1)S(1)}, bf16[256,512]{1,0:T(8,128)(2,1)S(1)}, u32[]{:S(2)}, u32[]{:S(2)}) collective-permute-start(bf16[256,512]{1,0:T(8,128)(2,1)S(1)} %get-tuple-element.39), channel_id=1, source_target_pairs={{2,0},{15,1},{4,2},{1,3},{6,4},{3,5},{8,6},{5,7},{10,8},{7,9},{12,... | collective-permute-start | bytes 786440 | tf_op jit(solution)/shard_map/ppermute | solution.py:253
  47.6 4.6 %collective-permute-start.4 = (bf16[256,512]{1,0:T(8,128)(2,1)S(1)}, bf16[256,512]{1,0:T(8,128)(2,1)S(1)}, u32[]{:S(2)}, u32[]{:S(2)}) collective-permute-start(bf16[256,512]{1,0:T(8,128)(2,1)S(1)} %get-tuple-element.39), channel_id=1, source_target_pairs={{0,2},{1,15},{2,4},{3,1},{4,6},{5,3},{6,8},{7,5},{8,10},{9,7},{10,... | collective-permute-start | bytes 786440 | tf_op jit(solution)/shard_map/ppermute | solution.py:254
  52.2 1.9 %collective-permute-start.5 = (bf16[256,512]{1,0:T(8,128)(2,1)S(1)}, bf16[256,512]{1,0:T(8,128)(2,1)S(1)}, u32[]{:S(2)}, u32[]{:S(2)}) collective-permute-start(bf16[256,512]{1,0:T(8,128)(2,1)S(1)} %get-tuple-element.38), channel_id=1, source_target_pairs={{2,0},{15,1},{4,2},{1,3},{6,4},{3,5},{8,6},{5,7},{10,8},{7,9},{12,... | collective-permute-start | bytes 786440 | tf_op jit(solution)/shard_map/ppermute | solution.py:255
  54.2 4.6 %collective-permute-start.1 = (bf16[256,512]{1,0:T(8,128)(2,1)S(1)}, bf16[256,512]{1,0:T(8,128)(2,1)S(1)}, u32[]{:S(2)}, u32[]{:S(2)}) collective-permute-start(bf16[256,512]{1,0:T(8,128)(2,1)S(1)} %collective-permute-done.major_a), channel_id=1, source_target_pairs={{0,2},{1,15},{2,4},{3,1},{4,6},{5,3},{6,8},{7,5},{8,10},{9,7},{10,... | collective-permute-start | bytes 786440 | tf_op jit(solution)/shard_map/ppermute | solution.py:256
  58.7 1.9 %collective-permute-start.3 = (bf16[256,512]{1,0:T(8,128)(2,1)S(1)}, bf16[256,512]{1,0:T(8,128)(2,1)S(1)}, u32[]{:S(2)}, u32[]{:S(2)}) collective-permute-start(bf16[256,512]{1,0:T(8,128)(2,1)S(1)} %collective-permute-done.2.minor_b), channel_id=1, source_target_pairs={{2,0},{15,1},{4,2},{1,3},{6,4},{3,5},{8,6},{5,7},{10,8},{7,9},{12,... | collective-permute-start | bytes 786440 | tf_op jit(solution)/shard_map/ppermute | solution.py:257
  60.7 1.6 %collective-permute-done.5.minor_a = bf16[256,512]{1,0:T(8,128)(2,1)S(1)} collective-permute-done((bf16[256,512]{1,0:T(8,128)(2,1)S(1)}, bf16[256,512]{1,0:T(8,128)(2,1)S(1)}, u32[]{:S(2)}, u32[]{:S(2)}) %collective-permute-start.5) | collective-permute-done | bytes 262176 | tf_op jit(solution)/shard_map/ppermute | solution.py:255
  62.3 4.1 %shard_map.75 = (f32[512,256]{1,0:T(8,128)S(1)}, f32[512,256]{1,0:T(8,128)S(1)}, f32[512,256]{1,0:T(8,128)S(1)}, f32[512,256]{1,0:T(8,128)S(1)}, bf16[4,2,256,256]{3,2,1,0:T(8,128)(2,1)S(1)}) custom-call(s32[4]{0:T(128)S(1)} %copy-done.1, bf16[512,512]{1,0:T(8,128)(2,1)S(1)} %get-tuple-element.40.own, bf16[256,512]{1,0:T(8,128)(2,1)S(1)} %collective-permute-done.major_a, ...), custom_call_target="tpu_custom_call" | custom-call | flops 1610612736 | bytes 8388608 | tf_op jit(solution)/shard_map/pallas_call | solution.py:185
  66.4 3.0 %collective-permute-done.3.far_b = bf16[256,512]{1,0:T(8,128)(2,1)S(1)} collective-permute-done((bf16[256,512]{1,0:T(8,128)(2,1)S(1)}, bf16[256,512]{1,0:T(8,128)(2,1)S(1)}, u32[]{:S(2)}, u32[]{:S(2)}) %collective-permute-start.3) | collective-permute-done | bytes 262176 | tf_op jit(solution)/shard_map/ppermute | solution.py:257
  69.4 1.7 %shard_map.76 = (bf16[512,256]{1,0:T(8,128)(2,1)S(1)}, bf16[512,256]{1,0:T(8,128)(2,1)S(1)}, bf16[256,256]{1,0:T(8,128)(2,1)S(1)}, bf16[256,256]{1,0:T(8,128)(2,1)S(1)}) custom-call(s32[4]{0:T(128)S(1)} %copy-done.1, bf16[256,512]{1,0:T(8,128)(2,1)S(1)} %collective-permute-done.1.far_a, bf16[256,512]{1,0:T(8,128)(2,1)S(1)} %collective-permute-done.3.far_b, ...), custom_call_target="tpu_custom_call" | custom-call | flops 671088640 | bytes 8388608 | tf_op jit(solution)/shard_map/pallas_call | solution.py:185
  71.0 1.0 shard_map.79
  72.0 1.9 %collective-permute-start.14 = (bf16[512,256]{1,0:T(8,128)(2,1)S(1)}, bf16[512,256]{1,0:T(8,128)(2,1)S(1)}, u32[]{:S(2)}, u32[]{:S(2)}) collective-permute-start(bf16[512,256]{1,0:T(8,128)(2,1)S(1)} %get-tuple-element.59), channel_id=1, source_target_pairs={{2,0},{15,1},{4,2},{1,3},{6,4},{3,5},{8,6},{5,7},{10,8},{7,9},{12,... | collective-permute-start | bytes 786440 | tf_op jit(solution)/shard_map/ppermute | solution.py:299
  74.0 1.9 %collective-permute-start.13 = (bf16[256,256]{1,0:T(8,128)(2,1)S(1)}, bf16[256,256]{1,0:T(8,128)(2,1)S(1)}, u32[]{:S(2)}, u32[]{:S(2)}) collective-permute-start(bf16[256,256]{1,0:T(8,128)(2,1)S(1)} %get-tuple-element.58), channel_id=1, source_target_pairs={{4,0},{13,1},{6,2},{15,3},{8,4},{1,5},{10,6},{3,7},{12,8},{5,9},{1... | collective-permute-start | bytes 393224 | tf_op jit(solution)/shard_map/ppermute | solution.py:296
  75.9 4.6 %collective-permute-start.10 = (bf16[512,256]{1,0:T(8,128)(2,1)S(1)}, bf16[512,256]{1,0:T(8,128)(2,1)S(1)}, u32[]{:S(2)}, u32[]{:S(2)}) collective-permute-start(bf16[512,256]{1,0:T(8,128)(2,1)S(1)} %get-tuple-element.55), channel_id=1, source_target_pairs={{0,2},{1,15},{2,4},{3,1},{4,6},{5,3},{6,8},{7,5},{8,10},{9,7},{10,... | collective-permute-start | bytes 786440 | tf_op jit(solution)/shard_map/ppermute | solution.py:298
  80.5 4.3 %collective-permute-start.9 = (bf16[256,256]{1,0:T(8,128)(2,1)S(1)}, bf16[256,256]{1,0:T(8,128)(2,1)S(1)}, u32[]{:S(2)}, u32[]{:S(2)}) collective-permute-start(bf16[256,256]{1,0:T(8,128)(2,1)S(1)} %get-tuple-element.54), channel_id=1, source_target_pairs={{0,4},{1,13},{2,6},{3,15},{4,8},{5,1},{6,10},{7,3},{8,12},{9,5},{1... | collective-permute-start | bytes 393224 | tf_op jit(solution)/shard_map/ppermute | solution.py:295
  84.7 1.0 shard_map.78
  85.8 1.9 %collective-permute-start.15 = (bf16[512,256]{1,0:T(8,128)(2,1)S(1)}, bf16[512,256]{1,0:T(8,128)(2,1)S(1)}, u32[]{:S(2)}, u32[]{:S(2)}) collective-permute-start(bf16[512,256]{1,0:T(8,128)(2,1)S(1)} %add_convert_fusion.1), channel_id=1, source_target_pairs={{2,0},{15,1},{4,2},{1,3},{6,4},{3,5},{8,6},{5,7},{10,8},{7,9},{12,... | collective-permute-start | bytes 786440 | tf_op jit(solution)/shard_map/ppermute | solution.py:304
  87.8 2.2 %collective-permute-done.9 = bf16[256,256]{1,0:T(8,128)(2,1)S(1)} collective-permute-done((bf16[256,256]{1,0:T(8,128)(2,1)S(1)}, bf16[256,256]{1,0:T(8,128)(2,1)S(1)}, u32[]{:S(2)}, u32[]{:S(2)}) %collective-permute-start.9) | collective-permute-done | bytes 131104 | tf_op jit(solution)/shard_map/ppermute | solution.py:295
  90.0 2.6 %collective-permute-start.11 = (bf16[512,256]{1,0:T(8,128)(2,1)S(1)}, bf16[512,256]{1,0:T(8,128)(2,1)S(1)}, u32[]{:S(2)}, u32[]{:S(2)}) collective-permute-start(bf16[512,256]{1,0:T(8,128)(2,1)S(1)} %add_convert_fusion.3), channel_id=1, source_target_pairs={{0,2},{1,15},{2,4},{3,1},{4,6},{5,3},{6,8},{7,5},{8,10},{9,7},{10,... | collective-permute-start | bytes 786440 | tf_op jit(solution)/shard_map/ppermute | solution.py:303
  92.6 1.1 shard_map.77
  93.8 1.8 %collective-permute-done.15 = bf16[512,256]{1,0:T(8,128)(2,1)S(1)} collective-permute-done((bf16[512,256]{1,0:T(8,128)(2,1)S(1)}, bf16[512,256]{1,0:T(8,128)(2,1)S(1)}, u32[]{:S(2)}, u32[]{:S(2)}) %collective-permute-start.15) | collective-permute-done | bytes 262176 | tf_op jit(solution)/shard_map/ppermute | solution.py:304
  95.6 1.9 %collective-permute-start.16 = (bf16[512,256]{1,0:T(8,128)(2,1)S(1)}, bf16[512,256]{1,0:T(8,128)(2,1)S(1)}, u32[]{:S(2)}, u32[]{:S(2)}) collective-permute-start(bf16[512,256]{1,0:T(8,128)(2,1)S(1)} %add_convert_fusion), channel_id=1, source_target_pairs={{2,0},{15,1},{4,2},{1,3},{6,4},{3,5},{8,6},{5,7},{10,8},{7,9},{12,... | collective-permute-start | bytes 786440 | tf_op jit(solution)/shard_map/ppermute | solution.py:307
  97.6 1.4 collective-permute-done.11
  99.0 4.3 %collective-permute-start.12 = (bf16[512,256]{1,0:T(8,128)(2,1)S(1)}, bf16[512,256]{1,0:T(8,128)(2,1)S(1)}, u32[]{:S(2)}, u32[]{:S(2)}) collective-permute-start(bf16[512,256]{1,0:T(8,128)(2,1)S(1)} %add_convert_fusion.2), channel_id=1, source_target_pairs={{0,2},{1,15},{2,4},{3,1},{4,6},{5,3},{6,8},{7,5},{8,10},{9,7},{10,... | collective-permute-start | bytes 786440 | tf_op jit(solution)/shard_map/ppermute | solution.py:306
  103.3 3.1 %collective-permute-done.16.r_minor = bf16[512,256]{1,0:T(8,128)(2,1)S(1)} collective-permute-done((bf16[512,256]{1,0:T(8,128)(2,1)S(1)}, bf16[512,256]{1,0:T(8,128)(2,1)S(1)}, u32[]{:S(2)}, u32[]{:S(2)}) %collective-permute-start.16) | collective-permute-done | bytes 262176 | tf_op jit(solution)/shard_map/ppermute | solution.py:307
  106.4 2.0 %collective-permute-done.12.r_major = bf16[512,256]{1,0:T(8,128)(2,1)S(1)} collective-permute-done((bf16[512,256]{1,0:T(8,128)(2,1)S(1)}, bf16[512,256]{1,0:T(8,128)(2,1)S(1)}, u32[]{:S(2)}, u32[]{:S(2)}) %collective-permute-start.12) | collective-permute-done | bytes 262176 | tf_op jit(solution)/shard_map/ppermute | solution.py:306
  108.4 1.8 %shard_map.80 = bf16[768,256]{1,0:T(8,128)(2,1)} custom-call(s32[4]{0:T(128)S(1)} %copy-done.1, s32[768,1]{1,0:T(8,128)S(1)} %compare_select_fusion.k_slot, f32[512,256]{1,0:T(8,128)S(1)} %get-tuple-element.51.own, bf16[512,256]{1,0:T(8,128)(2,1)S(1)} %collective-permute-done.12.r_major, bf16[512,256]{1,0:T(8,128)(2,1)S(1)} %collective-permute-done.16.r_minor, ...), custom_call_target="tpu_custom_call" | custom-call | flops 201326592 | bytes 8388608 | tf_op jit(solution)/shard_map/pallas_call | solution.py:185
  110.2 8.4 %all-to-all-start.1 = ((bf16[32,24,256]{2,1,0:T(8,128)(2,1)}), bf16[32,24,256]{2,1,0:T(8,128)(2,1)S(1)}, u32[]{:S(2)}, u32[]{:S(2)}) async-start(bf16[32,24,256]{2,1,0:T(8,128)(2,1)} %bitcast.15), calls=%async_computation.1 | async-start | bytes 786432 | tf_op jit(solution)/shard_map/all_to_all | solution.py:316
  118.6 11.4 %all-to-all-done.1 = bf16[32,24,256]{2,1,0:T(8,128)(2,1)S(1)} async-done(((bf16[32,24,256]{2,1,0:T(8,128)(2,1)}), bf16[32,24,256]{2,1,0:T(8,128)(2,1)S(1)}, u32[]{:S(2)}, u32[]{:S(2)}) %all-to-all-start.1) | async-done | bytes 393248 | tf_op jit(solution)/shard_map/all_to_all | solution.py:316
  130.0 0.3 fusion.1
  130.4 8.6 %collective-permute-start.17 = (bf16[256,128]{1,0:T(8,128)(2,1)S(1)}, bf16[256,128]{1,0:T(8,128)(2,1)S(1)}, u32[]{:S(2)}, u32[]{:S(2)}) collective-permute-start(bf16[256,128]{1,0:T(8,128)(2,1)S(1)} %dynamic-slice_convert_fusion), channel_id=1, source_target_pairs={{0,1},{1,0},{2,3},{3,2},{4,5},{5,4},{6,7},{7,6},{8,9},{9,8},{10,11... | collective-permute-start | bytes 196616 | tf_op jit(solution)/shard_map/ppermute | solution.py:320
  139.0 0.9 collective-permute-done.17
  139.9 0.6 add_convert_fusion.4
  (33 shorter events, 1.0 us)
Async XLA Ops:
  4.5 18.7 %copy-start = (bf16[1,256,2048]{2,1,0:T(8,128)(2,1)S(1)}, bf16[1,256,2048]{2,1,0:T(8,128)(2,1)}, u32[]{:S(2)}) copy-start(bf16[1,256,2048]{2,1,0:T(8,128)(2,1)} %param.13) | copy-start | bytes 3145732
  4.5 34.9 %all-to-all-start = ((bf16[32,24,512]{2,1,0:T(8,128)(2,1)}), bf16[32,24,512]{2,1,0:T(8,128)(2,1)S(1)}, u32[]{:S(2)}, u32[]{:S(2)}) async-start(bf16[32,24,512]{2,1,0:T(8,128)(2,1)} %bitcast.26), calls=%async_computation | async-start | bytes 1572864 | tf_op jit(solution)/shard_map/all_to_all | solution.py:221
  18.4 29.2 %collective-permute-start.6 = (bf16[2048,256]{1,0:T(8,128)(2,1)}, bf16[2048,256]{1,0:T(8,128)(2,1)}, u32[]{:S(2)}, u32[]{:S(2)}) collective-permute-start(bf16[2048,256]{1,0:T(8,128)(2,1)} %bitcast.8), channel_id=1, source_target_pairs={{0,1},{1,0},{2,3},{3,2},{4,5},{5,4},{6,7},{7,6},{8,9},{9,8},{10,11... | collective-permute-start | bytes 3145736 | tf_op jit(solution)/shard_map/ppermute | solution.py:227
  21.3 30.9 %collective-permute-start.7 = (bf16[2048,256]{1,0:T(8,128)(2,1)}, bf16[2048,256]{1,0:T(8,128)(2,1)}, u32[]{:S(2)}, u32[]{:S(2)}) collective-permute-start(bf16[2048,256]{1,0:T(8,128)(2,1)} %bitcast.9), channel_id=1, source_target_pairs={{0,1},{1,0},{2,3},{3,2},{4,5},{5,4},{6,7},{7,6},{8,9},{9,8},{10,11... | collective-permute-start | bytes 3145736 | tf_op jit(solution)/shard_map/ppermute | solution.py:228
  23.2 43.2 %collective-permute-start.8 = (bf16[256,2048]{1,0:T(8,128)(2,1)S(1)}, bf16[256,2048]{1,0:T(8,128)(2,1)S(1)}, u32[]{:S(2)}, u32[]{:S(2)}) collective-permute-start(bf16[256,2048]{1,0:T(8,128)(2,1)S(1)} %bitcast.19), channel_id=1, source_target_pairs={{0,1},{1,0},{2,3},{3,2},{4,5},{5,4},{6,7},{7,6},{8,9},{9,8},{10,11... | collective-permute-start | bytes 3145736 | tf_op jit(solution)/shard_map/ppermute | solution.py:229
  26.6 0.7 copy-start.3
  31.7 7.8 %copy-start.1 = (s32[4]{0:T(128)S(1)}, s32[4]{0:T(128)}, u32[]{:S(2)}) copy-start(s32[4]{0:T(128)} %pad_add_fusion.where_ref) | copy-start | bytes 52
  40.6 13.6 %collective-permute-start = (bf16[256,512]{1,0:T(8,128)(2,1)S(1)}, bf16[256,512]{1,0:T(8,128)(2,1)S(1)}, u32[]{:S(2)}, u32[]{:S(2)}) collective-permute-start(bf16[256,512]{1,0:T(8,128)(2,1)S(1)} %get-tuple-element.38), channel_id=1, source_target_pairs={{0,2},{1,15},{2,4},{3,1},{4,6},{5,3},{6,8},{7,5},{8,10},{9,7},{10,... | collective-permute-start | bytes 786440 | tf_op jit(solution)/shard_map/ppermute | solution.py:252
  45.7 13.1 %collective-permute-start.2 = (bf16[256,512]{1,0:T(8,128)(2,1)S(1)}, bf16[256,512]{1,0:T(8,128)(2,1)S(1)}, u32[]{:S(2)}, u32[]{:S(2)}) collective-permute-start(bf16[256,512]{1,0:T(8,128)(2,1)S(1)} %get-tuple-element.39), channel_id=1, source_target_pairs={{2,0},{15,1},{4,2},{1,3},{6,4},{3,5},{8,6},{5,7},{10,8},{7,9},{12,... | collective-permute-start | bytes 786440 | tf_op jit(solution)/shard_map/ppermute | solution.py:253
  47.6 13.1 %collective-permute-start.4 = (bf16[256,512]{1,0:T(8,128)(2,1)S(1)}, bf16[256,512]{1,0:T(8,128)(2,1)S(1)}, u32[]{:S(2)}, u32[]{:S(2)}) collective-permute-start(bf16[256,512]{1,0:T(8,128)(2,1)S(1)} %get-tuple-element.39), channel_id=1, source_target_pairs={{0,2},{1,15},{2,4},{3,1},{4,6},{5,3},{6,8},{7,5},{8,10},{9,7},{10,... | collective-permute-start | bytes 786440 | tf_op jit(solution)/shard_map/ppermute | solution.py:254
  52.2 10.0 %collective-permute-start.5 = (bf16[256,512]{1,0:T(8,128)(2,1)S(1)}, bf16[256,512]{1,0:T(8,128)(2,1)S(1)}, u32[]{:S(2)}, u32[]{:S(2)}) collective-permute-start(bf16[256,512]{1,0:T(8,128)(2,1)S(1)} %get-tuple-element.38), channel_id=1, source_target_pairs={{2,0},{15,1},{4,2},{1,3},{6,4},{3,5},{8,6},{5,7},{10,8},{7,9},{12,... | collective-permute-start | bytes 786440 | tf_op jit(solution)/shard_map/ppermute | solution.py:255
  54.2 12.2 %collective-permute-start.1 = (bf16[256,512]{1,0:T(8,128)(2,1)S(1)}, bf16[256,512]{1,0:T(8,128)(2,1)S(1)}, u32[]{:S(2)}, u32[]{:S(2)}) collective-permute-start(bf16[256,512]{1,0:T(8,128)(2,1)S(1)} %collective-permute-done.major_a), channel_id=1, source_target_pairs={{0,2},{1,15},{2,4},{3,1},{4,6},{5,3},{6,8},{7,5},{8,10},{9,7},{10,... | collective-permute-start | bytes 786440 | tf_op jit(solution)/shard_map/ppermute | solution.py:256
  58.7 10.6 %collective-permute-start.3 = (bf16[256,512]{1,0:T(8,128)(2,1)S(1)}, bf16[256,512]{1,0:T(8,128)(2,1)S(1)}, u32[]{:S(2)}, u32[]{:S(2)}) collective-permute-start(bf16[256,512]{1,0:T(8,128)(2,1)S(1)} %collective-permute-done.2.minor_b), channel_id=1, source_target_pairs={{2,0},{15,1},{4,2},{1,3},{6,4},{3,5},{8,6},{5,7},{10,8},{7,9},{12,... | collective-permute-start | bytes 786440 | tf_op jit(solution)/shard_map/ppermute | solution.py:257
  72.0 13.7 %collective-permute-start.14 = (bf16[512,256]{1,0:T(8,128)(2,1)S(1)}, bf16[512,256]{1,0:T(8,128)(2,1)S(1)}, u32[]{:S(2)}, u32[]{:S(2)}) collective-permute-start(bf16[512,256]{1,0:T(8,128)(2,1)S(1)} %get-tuple-element.59), channel_id=1, source_target_pairs={{2,0},{15,1},{4,2},{1,3},{6,4},{3,5},{8,6},{5,7},{10,8},{7,9},{12,... | collective-permute-start | bytes 786440 | tf_op jit(solution)/shard_map/ppermute | solution.py:299
  74.0 11.8 %collective-permute-start.13 = (bf16[256,256]{1,0:T(8,128)(2,1)S(1)}, bf16[256,256]{1,0:T(8,128)(2,1)S(1)}, u32[]{:S(2)}, u32[]{:S(2)}) collective-permute-start(bf16[256,256]{1,0:T(8,128)(2,1)S(1)} %get-tuple-element.58), channel_id=1, source_target_pairs={{4,0},{13,1},{6,2},{15,3},{8,4},{1,5},{10,6},{3,7},{12,8},{5,9},{1... | collective-permute-start | bytes 393224 | tf_op jit(solution)/shard_map/ppermute | solution.py:296
  75.9 14.1 %collective-permute-start.10 = (bf16[512,256]{1,0:T(8,128)(2,1)S(1)}, bf16[512,256]{1,0:T(8,128)(2,1)S(1)}, u32[]{:S(2)}, u32[]{:S(2)}) collective-permute-start(bf16[512,256]{1,0:T(8,128)(2,1)S(1)} %get-tuple-element.55), channel_id=1, source_target_pairs={{0,2},{1,15},{2,4},{3,1},{4,6},{5,3},{6,8},{7,5},{8,10},{9,7},{10,... | collective-permute-start | bytes 786440 | tf_op jit(solution)/shard_map/ppermute | solution.py:298
  80.5 9.5 %collective-permute-start.9 = (bf16[256,256]{1,0:T(8,128)(2,1)S(1)}, bf16[256,256]{1,0:T(8,128)(2,1)S(1)}, u32[]{:S(2)}, u32[]{:S(2)}) collective-permute-start(bf16[256,256]{1,0:T(8,128)(2,1)S(1)} %get-tuple-element.54), channel_id=1, source_target_pairs={{0,4},{1,13},{2,6},{3,15},{4,8},{5,1},{6,10},{7,3},{8,12},{9,5},{1... | collective-permute-start | bytes 393224 | tf_op jit(solution)/shard_map/ppermute | solution.py:295
  85.8 9.7 %collective-permute-start.15 = (bf16[512,256]{1,0:T(8,128)(2,1)S(1)}, bf16[512,256]{1,0:T(8,128)(2,1)S(1)}, u32[]{:S(2)}, u32[]{:S(2)}) collective-permute-start(bf16[512,256]{1,0:T(8,128)(2,1)S(1)} %add_convert_fusion.1), channel_id=1, source_target_pairs={{2,0},{15,1},{4,2},{1,3},{6,4},{3,5},{8,6},{5,7},{10,8},{7,9},{12,... | collective-permute-start | bytes 786440 | tf_op jit(solution)/shard_map/ppermute | solution.py:304
  90.0 8.9 %collective-permute-start.11 = (bf16[512,256]{1,0:T(8,128)(2,1)S(1)}, bf16[512,256]{1,0:T(8,128)(2,1)S(1)}, u32[]{:S(2)}, u32[]{:S(2)}) collective-permute-start(bf16[512,256]{1,0:T(8,128)(2,1)S(1)} %add_convert_fusion.3), channel_id=1, source_target_pairs={{0,2},{1,15},{2,4},{3,1},{4,6},{5,3},{6,8},{7,5},{8,10},{9,7},{10,... | collective-permute-start | bytes 786440 | tf_op jit(solution)/shard_map/ppermute | solution.py:303
  95.6 10.8 %collective-permute-start.16 = (bf16[512,256]{1,0:T(8,128)(2,1)S(1)}, bf16[512,256]{1,0:T(8,128)(2,1)S(1)}, u32[]{:S(2)}, u32[]{:S(2)}) collective-permute-start(bf16[512,256]{1,0:T(8,128)(2,1)S(1)} %add_convert_fusion), channel_id=1, source_target_pairs={{2,0},{15,1},{4,2},{1,3},{6,4},{3,5},{8,6},{5,7},{10,8},{7,9},{12,... | collective-permute-start | bytes 786440 | tf_op jit(solution)/shard_map/ppermute | solution.py:307
  99.0 9.4 %collective-permute-start.12 = (bf16[512,256]{1,0:T(8,128)(2,1)S(1)}, bf16[512,256]{1,0:T(8,128)(2,1)S(1)}, u32[]{:S(2)}, u32[]{:S(2)}) collective-permute-start(bf16[512,256]{1,0:T(8,128)(2,1)S(1)} %add_convert_fusion.2), channel_id=1, source_target_pairs={{0,2},{1,15},{2,4},{3,1},{4,6},{5,3},{6,8},{7,5},{8,10},{9,7},{10,... | collective-permute-start | bytes 786440 | tf_op jit(solution)/shard_map/ppermute | solution.py:306
  110.2 19.8 %copy-start.2 = (bf16[768,256]{1,0:T(8,128)(2,1)S(1)}, bf16[768,256]{1,0:T(8,128)(2,1)}, u32[]{:S(2)}) copy-start(bf16[768,256]{1,0:T(8,128)(2,1)} %get-tuple-element.33) | copy-start | bytes 1179652
  110.2 19.8 %all-to-all-start.1 = ((bf16[32,24,256]{2,1,0:T(8,128)(2,1)}), bf16[32,24,256]{2,1,0:T(8,128)(2,1)S(1)}, u32[]{:S(2)}, u32[]{:S(2)}) async-start(bf16[32,24,256]{2,1,0:T(8,128)(2,1)} %bitcast.15), calls=%async_computation.1 | async-start | bytes 786432 | tf_op jit(solution)/shard_map/all_to_all | solution.py:316
  130.4 9.5 %collective-permute-start.17 = (bf16[256,128]{1,0:T(8,128)(2,1)S(1)}, bf16[256,128]{1,0:T(8,128)(2,1)S(1)}, u32[]{:S(2)}, u32[]{:S(2)}) collective-permute-start(bf16[256,128]{1,0:T(8,128)(2,1)S(1)} %dynamic-slice_convert_fusion), channel_id=1, source_target_pairs={{0,1},{1,0},{2,3},{3,2},{4,5},{5,4},{6,7},{7,6},{8,9},{9,8},{10,11... | collective-permute-start | bytes 196616 | tf_op jit(solution)/shard_map/ppermute | solution.py:320

commit v2 on v1

--- a/solution.py
+++ b/solution.py
@@ -33,7 +33,7 @@
     copies[0].wait()
     tok_rows, width = tokens_ref.shape
     experts, capacity = chosen_ref.shape
-    q, first_token, parity = where_ref[0] & 3, where_ref[2], where_ref[3]
+    q, first_token, parity = where_ref[0] & 3, where_ref[1], where_ref[2]
     chosen = chosen_ref[...]
     run_start = jnp.sum((chosen < first_token).astype(I32), axis=1, keepdims=True)
     run_end = jnp.sum((chosen < first_token + tok_rows).astype(I32), axis=1, keepdims=True)
@@ -95,14 +95,14 @@
 
 
 def columns(ref, where_ref, k, piece):
-    j = (where_ref[0] + k * where_ref[1]) & 7
+    j = (where_ref[0] + k) & 7
     return ref[:, pl.ds(pl.multiple_of(j * piece, piece), piece)]
 
 
 def near_kernel(where_ref, own, major_a, major_b, minor_a, minor_b, *refs):
     weights, totals, far_rows, held, sems = refs[:4], refs[4:8], refs[8], refs[9], refs[10]
-    y, d = where_ref[0], where_ref[1]
-    quarters = (y & 3, (y - d) & 3, (y + d) & 3, (y + 2) & 3)
+    y = where_ref[0]
+    quarters = (y & 3, (y + 3) & 3, (y + 1) & 3, (y + 2) & 3)
     copies = [
         [
             pltpu.make_async_copy(
@@ -209,14 +209,14 @@
     mate = [(0, 1), (1, 0)]
     tp = ("y", "c")
     to_major, to_major_2 = [
-        [(2 * i + j, 2 * ((i + k * (1 - 2 * j)) % 8) + j) for i in range(8) for j in range(2)]
+        [(2 * i + j, 2 * ((i + k) % 8) + j) for i in range(8) for j in range(2)]
         for k in (1, 2)
     ]
     to_minor, to_minor_2 = [
         [(target, source) for source, target in pairs] for pairs in (to_major, to_major_2)
     ]
 
-    place = jnp.stack([y, 1 - 2 * c, p * tok_rows, c]).astype(I32)
+    place = jnp.stack([y, p * tok_rows, c]).astype(I32)
     pick_token, sent = dispatch(tokens, norm_gain, chosen, place, slots)
     got = lax.all_to_all(sent.reshape(experts, slots, quarter), "ep", 0, 0, tiled=True)
     got = got.reshape(experts * slots, quarter)

time: 141 us -> 142 us (level)
  starting transfers between devices: 81.4 us -> 84.8 us
  waiting for transfers between devices: 35.2 us -> 31.9 us
    ppermute x1, waiting for transfers between devices: 2.02 us -> 7.75 us  [shards(): r_major = lax.ppermute(passed(major_1, r_major), tp, to_major)]
    ppermute x1, starting transfers between devices: 8.64 us -> 13.4 us  [shards(): theirs = lax.ppermute(other, 'c', mate)]
    all_to_all x1, starting transfers between devices: 8.36 us -> 5.37 us  [shards(): lax.all_to_all(back, 'ep', 0, 0, tiled=True).reshape(experts * slots, piece)]
    ppermute x1, waiting for transfers between devices: 2.97 us -> 0.01 us  [shards(): far_b = lax.ppermute(minor_b, tp, to_minor)]
    ppermute x1, starting transfers between devices: 4.57 us -> 1.92 us  [shards(): far_a = lax.ppermute(major_a, tp, to_major)]
    ppermute x1, starting transfers between devices: 1.92 us -> 4.57 us  [shards(): far_b = lax.ppermute(minor_b, tp, to_minor)]
    ppermute x1, starting transfers between devices: 4.57 us -> 1.92 us  [shards(): major_b = lax.ppermute(own_b, tp, to_major)]
    ppermute x1, starting transfers between devices: 1.92 us -> 4.57 us  [shards(): minor_a = lax.ppermute(own_a, tp, to_minor)]
  transfers between devices with their start and end apart: 20 -> 20, of which waited for: 10 -> 8; matrix products, arithmetic and copies ran while one was open for 4% -> 4% of each run, Pallas kernels for 5% -> 5%
where the time goes in v2:
time: 142 us; the launch traced here: 141 us
  starting transfers between devices  84.8 us (60%)
  waiting for transfers between devices  31.9 us (22%)
  Pallas kernels  15.6 us (11%)
  local copies, waits for them, and re-layouts  3.91 us (3%)
  other arithmetic  3.68 us (3%)
    all_to_all x1, starting transfers between devices, shards(): lax.all_to_all(sent.reshape(experts, slots, quarter), 'ep', 0, 0, tiled=T...  13.8 us
    ppermute x1, starting transfers between devices, shards(): theirs = lax.ppermute(other, 'c', mate)  13.4 us
    pallas_call x7, Pallas kernels, call_vmem(): pl.pallas_call(kernel, out_shape=out_shape, in_specs=[pl.BlockSpec(memory...  11.8 us
    all_to_all x1, waiting for transfers between devices, shards(): lax.all_to_all(back, 'ep', 0, 0, tiled=True).reshape(experts * slots, piece)  11.4 us
    all_to_all x1, waiting for transfers between devices, shards(): lax.all_to_all(sent.reshape(experts, slots, quarter), 'ep', 0, 0, tiled=T...  7.75 us
    ppermute x1, waiting for transfers between devices, shards(): r_major = lax.ppermute(passed(major_1, r_major), tp, to_major)  7.75 us
    all_to_all x1, starting transfers between devices, shards(): lax.all_to_all(back, 'ep', 0, 0, tiled=True).reshape(experts * slots, piece)  5.37 us
    ppermute x1, starting transfers between devices, shards(): minor_a = lax.ppermute(own_a, tp, to_minor)  4.57 us
  transfers between devices with their start and end apart: 20, of which 8 were waited for; matrix products, arithmetic and copies ran while one was open for 4% of the time, Pallas kernels for 5%

profile of v2, /device:TPU:1, one launch (start us, length us, event | category | flops | bytes accessed | tf_op | source)
XLA Modules:
  0.0 140.6 jit_solution(2479306849024181297)
XLA Ops:
  0.0 0.7 pad_add_fusion.where_ref
  0.7 3.9 %shard_map.73 = (bf16[768,256]{1,0:T(8,128)(2,1)}, bf16[768,512]{1,0:T(8,128)(2,1)}) custom-call(s32[3]{0:T(128)} %pad_add_fusion.where_ref, bf16[256,2048]{1,0:T(8,128)(2,1)} %tokens_in.1, f32[1,2048]{1,0:T(1,128)} %bitcast.27, s32[32,1024]{1,0:T(8,128)} %chosen_in.1), custom_call_target="tpu_custom_call" | custom-call | tf_op jit(solution)/shard_map/pallas_call | solution.py:74
  4.5 13.8 %all-to-all-start = ((bf16[32,24,512]{2,1,0:T(8,128)(2,1)}), bf16[32,24,512]{2,1,0:T(8,128)(2,1)S(1)}, u32[]{:S(2)}, u32[]{:S(2)}) async-start(bf16[32,24,512]{2,1,0:T(8,128)(2,1)} %bitcast.25), calls=%async_computation | async-start | bytes 1572864 | tf_op jit(solution)/shard_map/all_to_all | solution.py:221
  18.4 2.9 %collective-permute-start.6 = (bf16[2048,256]{1,0:T(8,128)(2,1)}, bf16[2048,256]{1,0:T(8,128)(2,1)}, u32[]{:S(2)}, u32[]{:S(2)}) collective-permute-start(bf16[2048,256]{1,0:T(8,128)(2,1)} %bitcast.7), channel_id=1, source_target_pairs={{0,1},{1,0},{2,3},{3,2},{4,5},{5,4},{6,7},{7,6},{8,9},{9,8},{10,11... | collective-permute-start | bytes 3145736 | tf_op jit(solution)/shard_map/ppermute | solution.py:227
  21.3 1.9 %collective-permute-start.7 = (bf16[2048,256]{1,0:T(8,128)(2,1)}, bf16[2048,256]{1,0:T(8,128)(2,1)}, u32[]{:S(2)}, u32[]{:S(2)}) collective-permute-start(bf16[2048,256]{1,0:T(8,128)(2,1)} %bitcast.8), channel_id=1, source_target_pairs={{0,1},{1,0},{2,3},{3,2},{4,5},{5,4},{6,7},{7,6},{8,9},{9,8},{10,11... | collective-permute-start | bytes 3145736 | tf_op jit(solution)/shard_map/ppermute | solution.py:228
  23.2 2.4 %collective-permute-start.8 = (bf16[256,2048]{1,0:T(8,128)(2,1)S(1)}, bf16[256,2048]{1,0:T(8,128)(2,1)S(1)}, u32[]{:S(2)}, u32[]{:S(2)}) collective-permute-start(bf16[256,2048]{1,0:T(8,128)(2,1)S(1)} %bitcast.18), channel_id=1, source_target_pairs={{0,1},{1,0},{2,3},{3,2},{4,5},{5,4},{6,7},{7,6},{8,9},{9,8},{10,11... | collective-permute-start | bytes 3145736 | tf_op jit(solution)/shard_map/ppermute | solution.py:229
  25.6 0.8 constant_dynamic-slice_fusion.1
  26.4 0.2 convert_reduce_fusion
  26.7 0.6 broadcast.44
  27.3 0.7 reduce.3
  28.0 0.2 reshape.111
  28.3 0.1 constant_dynamic-slice_fusion.weight
  28.4 0.9 add.92
  29.5 0.9 lt.70
  30.5 1.2 compare_select_fusion.k_slot
  31.7 7.8 %all-to-all-done = bf16[32,24,512]{2,1,0:T(8,128)(2,1)S(1)} async-done(((bf16[32,24,512]{2,1,0:T(8,128)(2,1)}), bf16[32,24,512]{2,1,0:T(8,128)(2,1)S(1)}, u32[]{:S(2)}, u32[]{:S(2)}) %all-to-all-start) | async-done | bytes 786464 | tf_op jit(solution)/shard_map/all_to_all | solution.py:221
  39.5 1.1 shard_map.74
  40.6 3.2 %collective-permute-start = (bf16[256,512]{1,0:T(8,128)(2,1)S(1)}, bf16[256,512]{1,0:T(8,128)(2,1)S(1)}, u32[]{:S(2)}, u32[]{:S(2)}) collective-permute-start(bf16[256,512]{1,0:T(8,128)(2,1)S(1)} %get-tuple-element.38), channel_id=1, source_target_pairs={{0,2},{1,3},{2,4},{3,5},{4,6},{5,7},{6,8},{7,9},{8,10},{9,11},{10,... | collective-permute-start | bytes 786440 | tf_op jit(solution)/shard_map/ppermute | solution.py:252
  43.8 3.8 %collective-permute-start.2 = (bf16[256,512]{1,0:T(8,128)(2,1)S(1)}, bf16[256,512]{1,0:T(8,128)(2,1)S(1)}, u32[]{:S(2)}, u32[]{:S(2)}) collective-permute-start(bf16[256,512]{1,0:T(8,128)(2,1)S(1)} %get-tuple-element.39), channel_id=1, source_target_pairs={{2,0},{3,1},{4,2},{5,3},{6,4},{7,5},{8,6},{9,7},{10,8},{11,9},{12,... | collective-permute-start | bytes 786440 | tf_op jit(solution)/shard_map/ppermute | solution.py:253
  47.6 1.9 %collective-permute-start.4 = (bf16[256,512]{1,0:T(8,128)(2,1)S(1)}, bf16[256,512]{1,0:T(8,128)(2,1)S(1)}, u32[]{:S(2)}, u32[]{:S(2)}) collective-permute-start(bf16[256,512]{1,0:T(8,128)(2,1)S(1)} %get-tuple-element.39), channel_id=1, source_target_pairs={{0,2},{1,3},{2,4},{3,5},{4,6},{5,7},{6,8},{7,9},{8,10},{9,11},{10,... | collective-permute-start | bytes 786440 | tf_op jit(solution)/shard_map/ppermute | solution.py:254
  49.6 4.6 %collective-permute-start.5 = (bf16[256,512]{1,0:T(8,128)(2,1)S(1)}, bf16[256,512]{1,0:T(8,128)(2,1)S(1)}, u32[]{:S(2)}, u32[]{:S(2)}) collective-permute-start(bf16[256,512]{1,0:T(8,128)(2,1)S(1)} %get-tuple-element.38), channel_id=1, source_target_pairs={{2,0},{3,1},{4,2},{5,3},{6,4},{7,5},{8,6},{9,7},{10,8},{11,9},{12,... | collective-permute-start | bytes 786440 | tf_op jit(solution)/shard_map/ppermute | solution.py:255
  54.2 1.9 %collective-permute-start.1 = (bf16[256,512]{1,0:T(8,128)(2,1)S(1)}, bf16[256,512]{1,0:T(8,128)(2,1)S(1)}, u32[]{:S(2)}, u32[]{:S(2)}) collective-permute-start(bf16[256,512]{1,0:T(8,128)(2,1)S(1)} %collective-permute-done.major_a), channel_id=1, source_target_pairs={{0,2},{1,3},{2,4},{3,5},{4,6},{5,7},{6,8},{7,9},{8,10},{9,11},{10,... | collective-permute-start | bytes 786440 | tf_op jit(solution)/shard_map/ppermute | solution.py:256
  56.1 4.6 %collective-permute-start.3 = (bf16[256,512]{1,0:T(8,128)(2,1)S(1)}, bf16[256,512]{1,0:T(8,128)(2,1)S(1)}, u32[]{:S(2)}, u32[]{:S(2)}) collective-permute-start(bf16[256,512]{1,0:T(8,128)(2,1)S(1)} %collective-permute-done.2.minor_b), channel_id=1, source_target_pairs={{2,0},{3,1},{4,2},{5,3},{6,4},{7,5},{8,6},{9,7},{10,8},{11,9},{12,... | collective-permute-start | bytes 786440 | tf_op jit(solution)/shard_map/ppermute | solution.py:257
  60.7 4.1 %shard_map.75 = (f32[512,256]{1,0:T(8,128)S(1)}, f32[512,256]{1,0:T(8,128)S(1)}, f32[512,256]{1,0:T(8,128)S(1)}, f32[512,256]{1,0:T(8,128)S(1)}, bf16[4,2,256,256]{3,2,1,0:T(8,128)(2,1)S(1)}) custom-call(s32[3]{0:T(128)S(1)} %copy-done.1, bf16[512,512]{1,0:T(8,128)(2,1)S(1)} %get-tuple-element.40.own, bf16[256,512]{1,0:T(8,128)(2,1)S(1)} %collective-permute-done.major_a, ...), custom_call_target="tpu_custom_call" | custom-call | flops 1610612736 | bytes 8388608 | tf_op jit(solution)/shard_map/pallas_call | solution.py:185
  64.8 1.7 %shard_map.76 = (bf16[512,256]{1,0:T(8,128)(2,1)S(1)}, bf16[512,256]{1,0:T(8,128)(2,1)S(1)}, bf16[256,256]{1,0:T(8,128)(2,1)S(1)}, bf16[256,256]{1,0:T(8,128)(2,1)S(1)}) custom-call(s32[3]{0:T(128)S(1)} %copy-done.1, bf16[256,512]{1,0:T(8,128)(2,1)S(1)} %collective-permute-done.1.far_a, bf16[256,512]{1,0:T(8,128)(2,1)S(1)} %collective-permute-done.3.far_b, ...), custom_call_target="tpu_custom_call" | custom-call | flops 671088640 | bytes 8388608 | tf_op jit(solution)/shard_map/pallas_call | solution.py:185
  66.5 1.0 shard_map.79
  67.5 4.2 %collective-permute-start.14 = (bf16[512,256]{1,0:T(8,128)(2,1)S(1)}, bf16[512,256]{1,0:T(8,128)(2,1)S(1)}, u32[]{:S(2)}, u32[]{:S(2)}) collective-permute-start(bf16[512,256]{1,0:T(8,128)(2,1)S(1)} %get-tuple-element.59), channel_id=1, source_target_pairs={{2,0},{3,1},{4,2},{5,3},{6,4},{7,5},{8,6},{9,7},{10,8},{11,9},{12,... | collective-permute-start | bytes 786440 | tf_op jit(solution)/shard_map/ppermute | solution.py:299
  71.8 2.5 %collective-permute-start.13 = (bf16[256,256]{1,0:T(8,128)(2,1)S(1)}, bf16[256,256]{1,0:T(8,128)(2,1)S(1)}, u32[]{:S(2)}, u32[]{:S(2)}) collective-permute-start(bf16[256,256]{1,0:T(8,128)(2,1)S(1)} %get-tuple-element.58), channel_id=1, source_target_pairs={{4,0},{5,1},{6,2},{7,3},{8,4},{9,5},{10,6},{11,7},{12,8},{13,9},{1... | collective-permute-start | bytes 393224 | tf_op jit(solution)/shard_map/ppermute | solution.py:296
  74.3 2.5 %collective-permute-start.10 = (bf16[512,256]{1,0:T(8,128)(2,1)S(1)}, bf16[512,256]{1,0:T(8,128)(2,1)S(1)}, u32[]{:S(2)}, u32[]{:S(2)}) collective-permute-start(bf16[512,256]{1,0:T(8,128)(2,1)S(1)} %get-tuple-element.55), channel_id=1, source_target_pairs={{0,2},{1,3},{2,4},{3,5},{4,6},{5,7},{6,8},{7,9},{8,10},{9,11},{10,... | collective-permute-start | bytes 786440 | tf_op jit(solution)/shard_map/ppermute | solution.py:298
  76.8 3.9 %collective-permute-start.9 = (bf16[256,256]{1,0:T(8,128)(2,1)S(1)}, bf16[256,256]{1,0:T(8,128)(2,1)S(1)}, u32[]{:S(2)}, u32[]{:S(2)}) collective-permute-start(bf16[256,256]{1,0:T(8,128)(2,1)S(1)} %get-tuple-element.54), channel_id=1, source_target_pairs={{0,4},{1,5},{2,6},{3,7},{4,8},{5,9},{6,10},{7,11},{8,12},{9,13},{1... | collective-permute-start | bytes 393224 | tf_op jit(solution)/shard_map/ppermute | solution.py:295
  80.7 1.0 shard_map.78
  81.8 3.7 %collective-permute-start.15 = (bf16[512,256]{1,0:T(8,128)(2,1)S(1)}, bf16[512,256]{1,0:T(8,128)(2,1)S(1)}, u32[]{:S(2)}, u32[]{:S(2)}) collective-permute-start(bf16[512,256]{1,0:T(8,128)(2,1)S(1)} %add_convert_fusion.1), channel_id=1, source_target_pairs={{2,0},{3,1},{4,2},{5,3},{6,4},{7,5},{8,6},{9,7},{10,8},{11,9},{12,... | collective-permute-start | bytes 786440 | tf_op jit(solution)/shard_map/ppermute | solution.py:304
  85.6 0.9 collective-permute-done.9
  86.5 1.9 %collective-permute-start.11 = (bf16[512,256]{1,0:T(8,128)(2,1)S(1)}, bf16[512,256]{1,0:T(8,128)(2,1)S(1)}, u32[]{:S(2)}, u32[]{:S(2)}) collective-permute-start(bf16[512,256]{1,0:T(8,128)(2,1)S(1)} %add_convert_fusion.3), channel_id=1, source_target_pairs={{0,2},{1,3},{2,4},{3,5},{4,6},{5,7},{6,8},{7,9},{8,10},{9,11},{10,... | collective-permute-start | bytes 786440 | tf_op jit(solution)/shard_map/ppermute | solution.py:303
  88.5 1.1 shard_map.77
  89.6 0.6 collective-permute-done.15
  90.2 4.2 %collective-permute-start.16 = (bf16[512,256]{1,0:T(8,128)(2,1)S(1)}, bf16[512,256]{1,0:T(8,128)(2,1)S(1)}, u32[]{:S(2)}, u32[]{:S(2)}) collective-permute-start(bf16[512,256]{1,0:T(8,128)(2,1)S(1)} %add_convert_fusion), channel_id=1, source_target_pairs={{2,0},{3,1},{4,2},{5,3},{6,4},{7,5},{8,6},{9,7},{10,8},{11,9},{12,... | collective-permute-start | bytes 786440 | tf_op jit(solution)/shard_map/ppermute | solution.py:307
  94.4 1.5 %collective-permute-done.11 = bf16[512,256]{1,0:T(8,128)(2,1)S(1)} collective-permute-done((bf16[512,256]{1,0:T(8,128)(2,1)S(1)}, bf16[512,256]{1,0:T(8,128)(2,1)S(1)}, u32[]{:S(2)}, u32[]{:S(2)}) %collective-permute-start.11) | collective-permute-done | bytes 262176 | tf_op jit(solution)/shard_map/ppermute | solution.py:303
  96.0 1.9 %collective-permute-start.12 = (bf16[512,256]{1,0:T(8,128)(2,1)S(1)}, bf16[512,256]{1,0:T(8,128)(2,1)S(1)}, u32[]{:S(2)}, u32[]{:S(2)}) collective-permute-start(bf16[512,256]{1,0:T(8,128)(2,1)S(1)} %add_convert_fusion.2), channel_id=1, source_target_pairs={{0,2},{1,3},{2,4},{3,5},{4,6},{5,7},{6,8},{7,9},{8,10},{9,11},{10,... | collective-permute-start | bytes 786440 | tf_op jit(solution)/shard_map/ppermute | solution.py:306
  97.9 1.0 collective-permute-done.16.r_minor
  99.0 7.8 %collective-permute-done.12.r_major = bf16[512,256]{1,0:T(8,128)(2,1)S(1)} collective-permute-done((bf16[512,256]{1,0:T(8,128)(2,1)S(1)}, bf16[512,256]{1,0:T(8,128)(2,1)S(1)}, u32[]{:S(2)}, u32[]{:S(2)}) %collective-permute-start.12) | collective-permute-done | bytes 262176 | tf_op jit(solution)/shard_map/ppermute | solution.py:306
  106.7 1.8 %shard_map.80 = bf16[768,256]{1,0:T(8,128)(2,1)} custom-call(s32[3]{0:T(128)S(1)} %copy-done.1, s32[768,1]{1,0:T(8,128)S(1)} %compare_select_fusion.k_slot, f32[512,256]{1,0:T(8,128)S(1)} %get-tuple-element.51.own, bf16[512,256]{1,0:T(8,128)(2,1)S(1)} %collective-permute-done.12.r_major, bf16[512,256]{1,0:T(8,128)(2,1)S(1)} %collective-permute-done.16.r_minor, ...), custom_call_target="tpu_custom_call" | custom-call | flops 201326592 | bytes 8388608 | tf_op jit(solution)/shard_map/pallas_call | solution.py:185
  108.5 5.4 %all-to-all-start.1 = ((bf16[32,24,256]{2,1,0:T(8,128)(2,1)}), bf16[32,24,256]{2,1,0:T(8,128)(2,1)S(1)}, u32[]{:S(2)}, u32[]{:S(2)}) async-start(bf16[32,24,256]{2,1,0:T(8,128)(2,1)} %bitcast.14), calls=%async_computation.1 | async-start | bytes 786432 | tf_op jit(solution)/shard_map/all_to_all | solution.py:316
  113.9 11.4 %all-to-all-done.1 = bf16[32,24,256]{2,1,0:T(8,128)(2,1)S(1)} async-done(((bf16[32,24,256]{2,1,0:T(8,128)(2,1)}), bf16[32,24,256]{2,1,0:T(8,128)(2,1)S(1)}, u32[]{:S(2)}, u32[]{:S(2)}) %all-to-all-start.1) | async-done | bytes 393248 | tf_op jit(solution)/shard_map/all_to_all | solution.py:316
  125.3 0.3 fusion.1
  125.7 13.4 %collective-permute-start.17 = (bf16[256,128]{1,0:T(8,128)(2,1)S(1)}, bf16[256,128]{1,0:T(8,128)(2,1)S(1)}, u32[]{:S(2)}, u32[]{:S(2)}) collective-permute-start(bf16[256,128]{1,0:T(8,128)(2,1)S(1)} %dynamic-slice_convert_fusion), channel_id=1, source_target_pairs={{0,1},{1,0},{2,3},{3,2},{4,5},{5,4},{6,7},{7,6},{8,9},{9,8},{10,11... | collective-permute-start | bytes 196616 | tf_op jit(solution)/shard_map/ppermute | solution.py:320
  139.1 0.9 collective-permute-done.17
  140.0 0.6 add_convert_fusion.4
  (33 shorter events, 0.7 us)
Async XLA Ops:
  4.5 18.7 %copy-start = (bf16[1,256,2048]{2,1,0:T(8,128)(2,1)S(1)}, bf16[1,256,2048]{2,1,0:T(8,128)(2,1)}, u32[]{:S(2)}) copy-start(bf16[1,256,2048]{2,1,0:T(8,128)(2,1)} %param.13) | copy-start | bytes 3145732
  4.5 34.9 %all-to-all-start = ((bf16[32,24,512]{2,1,0:T(8,128)(2,1)}), bf16[32,24,512]{2,1,0:T(8,128)(2,1)S(1)}, u32[]{:S(2)}, u32[]{:S(2)}) async-start(bf16[32,24,512]{2,1,0:T(8,128)(2,1)} %bitcast.25), calls=%async_computation | async-start | bytes 1572864 | tf_op jit(solution)/shard_map/all_to_all | solution.py:221
  18.4 29.2 %collective-permute-start.6 = (bf16[2048,256]{1,0:T(8,128)(2,1)}, bf16[2048,256]{1,0:T(8,128)(2,1)}, u32[]{:S(2)}, u32[]{:S(2)}) collective-permute-start(bf16[2048,256]{1,0:T(8,128)(2,1)} %bitcast.7), channel_id=1, source_target_pairs={{0,1},{1,0},{2,3},{3,2},{4,5},{5,4},{6,7},{7,6},{8,9},{9,8},{10,11... | collective-permute-start | bytes 3145736 | tf_op jit(solution)/shard_map/ppermute | solution.py:227
  21.3 28.3 %collective-permute-start.7 = (bf16[2048,256]{1,0:T(8,128)(2,1)}, bf16[2048,256]{1,0:T(8,128)(2,1)}, u32[]{:S(2)}, u32[]{:S(2)}) collective-permute-start(bf16[2048,256]{1,0:T(8,128)(2,1)} %bitcast.8), channel_id=1, source_target_pairs={{0,1},{1,0},{2,3},{3,2},{4,5},{5,4},{6,7},{7,6},{8,9},{9,8},{10,11... | collective-permute-start | bytes 3145736 | tf_op jit(solution)/shard_map/ppermute | solution.py:228
  23.2 41.6 %collective-permute-start.8 = (bf16[256,2048]{1,0:T(8,128)(2,1)S(1)}, bf16[256,2048]{1,0:T(8,128)(2,1)S(1)}, u32[]{:S(2)}, u32[]{:S(2)}) collective-permute-start(bf16[256,2048]{1,0:T(8,128)(2,1)S(1)} %bitcast.18), channel_id=1, source_target_pairs={{0,1},{1,0},{2,3},{3,2},{4,5},{5,4},{6,7},{7,6},{8,9},{9,8},{10,11... | collective-permute-start | bytes 3145736 | tf_op jit(solution)/shard_map/ppermute | solution.py:229
  26.6 0.7 copy-start.3
  31.7 7.8 %copy-start.1 = (s32[3]{0:T(128)S(1)}, s32[3]{0:T(128)}, u32[]{:S(2)}) copy-start(s32[3]{0:T(128)} %pad_add_fusion.where_ref) | copy-start | bytes 40
  40.6 13.6 %collective-permute-start = (bf16[256,512]{1,0:T(8,128)(2,1)S(1)}, bf16[256,512]{1,0:T(8,128)(2,1)S(1)}, u32[]{:S(2)}, u32[]{:S(2)}) collective-permute-start(bf16[256,512]{1,0:T(8,128)(2,1)S(1)} %get-tuple-element.38), channel_id=1, source_target_pairs={{0,2},{1,3},{2,4},{3,5},{4,6},{5,7},{6,8},{7,9},{8,10},{9,11},{10,... | collective-permute-start | bytes 786440 | tf_op jit(solution)/shard_map/ppermute | solution.py:252
  43.8 12.3 %collective-permute-start.2 = (bf16[256,512]{1,0:T(8,128)(2,1)S(1)}, bf16[256,512]{1,0:T(8,128)(2,1)S(1)}, u32[]{:S(2)}, u32[]{:S(2)}) collective-permute-start(bf16[256,512]{1,0:T(8,128)(2,1)S(1)} %get-tuple-element.39), channel_id=1, source_target_pairs={{2,0},{3,1},{4,2},{5,3},{6,4},{7,5},{8,6},{9,7},{10,8},{11,9},{12,... | collective-permute-start | bytes 786440 | tf_op jit(solution)/shard_map/ppermute | solution.py:253
  47.6 13.1 %collective-permute-start.4 = (bf16[256,512]{1,0:T(8,128)(2,1)S(1)}, bf16[256,512]{1,0:T(8,128)(2,1)S(1)}, u32[]{:S(2)}, u32[]{:S(2)}) collective-permute-start(bf16[256,512]{1,0:T(8,128)(2,1)S(1)} %get-tuple-element.39), channel_id=1, source_target_pairs={{0,2},{1,3},{2,4},{3,5},{4,6},{5,7},{6,8},{7,9},{8,10},{9,11},{10,... | collective-permute-start | bytes 786440 | tf_op jit(solution)/shard_map/ppermute | solution.py:254
  49.6 11.1 %collective-permute-start.5 = (bf16[256,512]{1,0:T(8,128)(2,1)S(1)}, bf16[256,512]{1,0:T(8,128)(2,1)S(1)}, u32[]{:S(2)}, u32[]{:S(2)}) collective-permute-start(bf16[256,512]{1,0:T(8,128)(2,1)S(1)} %get-tuple-element.38), channel_id=1, source_target_pairs={{2,0},{3,1},{4,2},{5,3},{6,4},{7,5},{8,6},{9,7},{10,8},{11,9},{12,... | collective-permute-start | bytes 786440 | tf_op jit(solution)/shard_map/ppermute | solution.py:255
  54.2 10.7 %collective-permute-start.1 = (bf16[256,512]{1,0:T(8,128)(2,1)S(1)}, bf16[256,512]{1,0:T(8,128)(2,1)S(1)}, u32[]{:S(2)}, u32[]{:S(2)}) collective-permute-start(bf16[256,512]{1,0:T(8,128)(2,1)S(1)} %collective-permute-done.major_a), channel_id=1, source_target_pairs={{0,2},{1,3},{2,4},{3,5},{4,6},{5,7},{6,8},{7,9},{8,10},{9,11},{10,... | collective-permute-start | bytes 786440 | tf_op jit(solution)/shard_map/ppermute | solution.py:256
  56.1 8.7 %collective-permute-start.3 = (bf16[256,512]{1,0:T(8,128)(2,1)S(1)}, bf16[256,512]{1,0:T(8,128)(2,1)S(1)}, u32[]{:S(2)}, u32[]{:S(2)}) collective-permute-start(bf16[256,512]{1,0:T(8,128)(2,1)S(1)} %collective-permute-done.2.minor_b), channel_id=1, source_target_pairs={{2,0},{3,1},{4,2},{5,3},{6,4},{7,5},{8,6},{9,7},{10,8},{11,9},{12,... | collective-permute-start | bytes 786440 | tf_op jit(solution)/shard_map/ppermute | solution.py:257
  67.5 14.2 %collective-permute-start.14 = (bf16[512,256]{1,0:T(8,128)(2,1)S(1)}, bf16[512,256]{1,0:T(8,128)(2,1)S(1)}, u32[]{:S(2)}, u32[]{:S(2)}) collective-permute-start(bf16[512,256]{1,0:T(8,128)(2,1)S(1)} %get-tuple-element.59), channel_id=1, source_target_pairs={{2,0},{3,1},{4,2},{5,3},{6,4},{7,5},{8,6},{9,7},{10,8},{11,9},{12,... | collective-permute-start | bytes 786440 | tf_op jit(solution)/shard_map/ppermute | solution.py:299
  71.8 10.0 %collective-permute-start.13 = (bf16[256,256]{1,0:T(8,128)(2,1)S(1)}, bf16[256,256]{1,0:T(8,128)(2,1)S(1)}, u32[]{:S(2)}, u32[]{:S(2)}) collective-permute-start(bf16[256,256]{1,0:T(8,128)(2,1)S(1)} %get-tuple-element.58), channel_id=1, source_target_pairs={{4,0},{5,1},{6,2},{7,3},{8,4},{9,5},{10,6},{11,7},{12,8},{13,9},{1... | collective-permute-start | bytes 393224 | tf_op jit(solution)/shard_map/ppermute | solution.py:296
  74.3 12.2 %collective-permute-start.10 = (bf16[512,256]{1,0:T(8,128)(2,1)S(1)}, bf16[512,256]{1,0:T(8,128)(2,1)S(1)}, u32[]{:S(2)}, u32[]{:S(2)}) collective-permute-start(bf16[512,256]{1,0:T(8,128)(2,1)S(1)} %get-tuple-element.55), channel_id=1, source_target_pairs={{0,2},{1,3},{2,4},{3,5},{4,6},{5,7},{6,8},{7,9},{8,10},{9,11},{10,... | collective-permute-start | bytes 786440 | tf_op jit(solution)/shard_map/ppermute | solution.py:298
  76.8 9.7 %collective-permute-start.9 = (bf16[256,256]{1,0:T(8,128)(2,1)S(1)}, bf16[256,256]{1,0:T(8,128)(2,1)S(1)}, u32[]{:S(2)}, u32[]{:S(2)}) collective-permute-start(bf16[256,256]{1,0:T(8,128)(2,1)S(1)} %get-tuple-element.54), channel_id=1, source_target_pairs={{0,4},{1,5},{2,6},{3,7},{4,8},{5,9},{6,10},{7,11},{8,12},{9,13},{1... | collective-permute-start | bytes 393224 | tf_op jit(solution)/shard_map/ppermute | solution.py:295
  81.8 8.3 %collective-permute-start.15 = (bf16[512,256]{1,0:T(8,128)(2,1)S(1)}, bf16[512,256]{1,0:T(8,128)(2,1)S(1)}, u32[]{:S(2)}, u32[]{:S(2)}) collective-permute-start(bf16[512,256]{1,0:T(8,128)(2,1)S(1)} %add_convert_fusion.1), channel_id=1, source_target_pairs={{2,0},{3,1},{4,2},{5,3},{6,4},{7,5},{8,6},{9,7},{10,8},{11,9},{12,... | collective-permute-start | bytes 786440 | tf_op jit(solution)/shard_map/ppermute | solution.py:304
  86.5 9.4 %collective-permute-start.11 = (bf16[512,256]{1,0:T(8,128)(2,1)S(1)}, bf16[512,256]{1,0:T(8,128)(2,1)S(1)}, u32[]{:S(2)}, u32[]{:S(2)}) collective-permute-start(bf16[512,256]{1,0:T(8,128)(2,1)S(1)} %add_convert_fusion.3), channel_id=1, source_target_pairs={{0,2},{1,3},{2,4},{3,5},{4,6},{5,7},{6,8},{7,9},{8,10},{9,11},{10,... | collective-permute-start | bytes 786440 | tf_op jit(solution)/shard_map/ppermute | solution.py:303
  90.2 8.7 %collective-permute-start.16 = (bf16[512,256]{1,0:T(8,128)(2,1)S(1)}, bf16[512,256]{1,0:T(8,128)(2,1)S(1)}, u32[]{:S(2)}, u32[]{:S(2)}) collective-permute-start(bf16[512,256]{1,0:T(8,128)(2,1)S(1)} %add_convert_fusion), channel_id=1, source_target_pairs={{2,0},{3,1},{4,2},{5,3},{6,4},{7,5},{8,6},{9,7},{10,8},{11,9},{12,... | collective-permute-start | bytes 786440 | tf_op jit(solution)/shard_map/ppermute | solution.py:307
  96.0 10.7 %collective-permute-start.12 = (bf16[512,256]{1,0:T(8,128)(2,1)S(1)}, bf16[512,256]{1,0:T(8,128)(2,1)S(1)}, u32[]{:S(2)}, u32[]{:S(2)}) collective-permute-start(bf16[512,256]{1,0:T(8,128)(2,1)S(1)} %add_convert_fusion.2), channel_id=1, source_target_pairs={{0,2},{1,3},{2,4},{3,5},{4,6},{5,7},{6,8},{7,9},{8,10},{9,11},{10,... | collective-permute-start | bytes 786440 | tf_op jit(solution)/shard_map/ppermute | solution.py:306
  108.5 16.8 %copy-start.2 = (bf16[768,256]{1,0:T(8,128)(2,1)S(1)}, bf16[768,256]{1,0:T(8,128)(2,1)}, u32[]{:S(2)}) copy-start(bf16[768,256]{1,0:T(8,128)(2,1)} %get-tuple-element.33) | copy-start | bytes 1179652
  108.5 16.8 %all-to-all-start.1 = ((bf16[32,24,256]{2,1,0:T(8,128)(2,1)}), bf16[32,24,256]{2,1,0:T(8,128)(2,1)S(1)}, u32[]{:S(2)}, u32[]{:S(2)}) async-start(bf16[32,24,256]{2,1,0:T(8,128)(2,1)} %bitcast.14), calls=%async_computation.1 | async-start | bytes 786432 | tf_op jit(solution)/shard_map/all_to_all | solution.py:316
  125.7 14.3 %collective-permute-start.17 = (bf16[256,128]{1,0:T(8,128)(2,1)S(1)}, bf16[256,128]{1,0:T(8,128)(2,1)S(1)}, u32[]{:S(2)}, u32[]{:S(2)}) collective-permute-start(bf16[256,128]{1,0:T(8,128)(2,1)S(1)} %dynamic-slice_convert_fusion), channel_id=1, source_target_pairs={{0,1},{1,0},{2,3},{3,2},{4,5},{5,4},{6,7},{7,6},{8,9},{9,8},{10,11... | collective-permute-start | bytes 196616 | tf_op jit(solution)/shard_map/ppermute | solution.py:320

commit v3 on v2

--- a/solution.py
+++ b/solution.py
@@ -20,7 +20,7 @@
 
 
 def dispatch_kernel(
-    slots, where_ref, tokens_in, gain_in, chosen_in, pick_ref, sent_ref,
+    slots, tokens_in, gain_in, chosen_in, pick_ref, sent_ref,
     held, tokens_ref, gain_ref, chosen_ref, sems,
 ):
     copies = [
@@ -33,7 +33,8 @@
     copies[0].wait()
     tok_rows, width = tokens_ref.shape
     experts, capacity = chosen_ref.shape
-    q, first_token, parity = where_ref[0] & 3, where_ref[1], where_ref[2]
+    q, parity = lax.axis_index("y") & 3, lax.axis_index("c")
+    first_token = lax.axis_index("ep") * tok_rows
     chosen = chosen_ref[...]
     run_start = jnp.sum((chosen < first_token).astype(I32), axis=1, keepdims=True)
     run_end = jnp.sum((chosen < first_token + tok_rows).astype(I32), axis=1, keepdims=True)
@@ -66,7 +67,7 @@
         ).astype(BF16)
 
 
-def dispatch(tokens, norm_gain, chosen, where, slots):
+def dispatch(tokens, norm_gain, chosen, slots):
     experts = chosen.shape[0]
     tok_rows, width = tokens.shape
     rows = experts * slots
@@ -77,7 +78,7 @@
             jax.ShapeDtypeStruct((rows, tok_rows), BF16),
             jax.ShapeDtypeStruct((rows, width // 4), BF16),
         ),
-        in_specs=[pl.BlockSpec(memory_space=pltpu.SMEM)] + [pl.BlockSpec(memory_space=pltpu.HBM)] * 3,
+        in_specs=[pl.BlockSpec(memory_space=pltpu.HBM)] * 3,
         out_specs=(vmem, vmem),
         scratch_shapes=[
             pltpu.VMEM((rows, tok_rows), F32),
@@ -87,7 +88,7 @@
             pltpu.SemaphoreType.DMA((3,)),
         ],
         compiler_params=pltpu.CompilerParams(vmem_limit_bytes=60 << 20),
-    )(where, tokens, norm_gain.reshape(1, width), chosen)
+    )(tokens, norm_gain.reshape(1, width), chosen)
 
 
 def flat(rows):
@@ -133,13 +134,13 @@
 
 def far_kernel(
     where_ref, far_a, far_b, t_gate, t_up, t_gate_m, t_up_m, far_rows, down, down_m,
-    hid, hid_m, first_a, first_b,
+    hid, hid_m, first,
 ):
-    mid, piece = first_a.shape
+    mid, piece = far_a.shape[0], first.shape[1]
     d_own = columns(down, where_ref, 4, piece)
     d_mate = columns(down_m, where_ref, 4, piece)
     w = [flat(far_rows[n]) for n in range(4)]
-    for r, (far, first) in enumerate(((far_a, first_a), (far_b, first_b))):
+    for r, far in enumerate((far_a, far_b)):
         rows = slice(r * mid, (r + 1) * mid)
 
         def gated(t_g, t_u, w_g, w_u):
@@ -151,14 +152,17 @@
         h_mate = gated(t_gate_m, t_up_m, w[2], w[3])
         hid[rows, :] = h_own
         hid_m[rows, :] = h_mate
-        first[...] = (dot(h_own, d_own) + dot(h_mate, d_mate)).astype(first.dtype)
-
-
-def out_kernel(offsets, where_ref, hid, hid_m, down, down_m, *outs):
+        first[rows, :] = (dot(h_own, d_own) + dot(h_mate, d_mate)).astype(first.dtype)
+
+
+def out_kernel(offsets, where_ref, hid, hid_m, down, down_m, *refs):
+    outs = refs[-len(offsets) :]
     piece = outs[0].shape[1]
-    for k, out in zip(offsets, outs):
+    for n, (k, out) in enumerate(zip(offsets, outs)):
         value = dot(hid[...], columns(down, where_ref, k, piece))
         value = value + dot(hid_m[...], columns(down_m, where_ref, k, piece))
+        if len(refs) > len(offsets):
+            value = value + jnp.where(lax.axis_index("c") == n, refs[0][...].astype(F32), 0.0)
         out[...] = value.astype(out.dtype)
 
 
@@ -208,16 +212,12 @@
     slots = 3 * tok_rows // 32
     mate = [(0, 1), (1, 0)]
     tp = ("y", "c")
-    to_major, to_major_2 = [
-        [(2 * i + j, 2 * ((i + k) % 8) + j) for i in range(8) for j in range(2)]
-        for k in (1, 2)
-    ]
-    to_minor, to_minor_2 = [
-        [(target, source) for source, target in pairs] for pairs in (to_major, to_major_2)
-    ]
-
-    place = jnp.stack([y, p * tok_rows, c]).astype(I32)
-    pick_token, sent = dispatch(tokens, norm_gain, chosen, place, slots)
+    to_major = [(2 * i + j, 2 * ((i + 1) % 8) + j) for i in range(8) for j in range(2)]
+    to_minor = [(target, source) for source, target in to_major]
+    jumps = [(2 * i + j, 2 * ((i + 2 - 4 * j) % 8) + j) for i in range(8) for j in range(2)]
+
+    place = y.astype(I32).reshape(1)
+    pick_token, sent = dispatch(tokens, norm_gain, chosen, slots)
     got = lax.all_to_all(sent.reshape(experts, slots, quarter), "ep", 0, 0, tiled=True)
     got = got.reshape(experts * slots, quarter)
 
@@ -271,35 +271,31 @@
         [pltpu.VMEM((4, 3, 2, piece, units), BF16), pltpu.SemaphoreType.DMA((4, 4))],
     )
     hid_shape = jax.ShapeDtypeStruct((half_rows, units), BF16)
-    first_shape = jax.ShapeDtypeStruct((mid, piece), BF16)
-    hid, hid_m, first_a, first_b = call_vmem(
+    hid, hid_m, first = call_vmem(
         far_kernel,
-        [hid_shape, hid_shape, first_shape, first_shape],
+        [hid_shape, hid_shape, jax.ShapeDtypeStruct((half_rows, piece), BF16)],
         2 * half_rows * (quarter * 4 * units + 2 * units * piece),
         place,
         [far_a, far_b, *totals, far_rows, down_w, down_m],
     )
 
-    def outs_at(offsets, dtype):
+    def outs_at(offsets, dtype, *more):
         return call_vmem(
             functools.partial(out_kernel, offsets),
             [jax.ShapeDtypeStruct((half_rows, piece), dtype)] * len(offsets),
             2 * half_rows * 2 * units * len(offsets) * piece,
             place,
-            [hid, hid_m, down_w, down_m],
+            [hid, hid_m, down_w, down_m, *more],
         )
 
     def passed(mine, received):
         return (mine + received.astype(F32)).astype(BF16)
 
-    jump_major = lax.ppermute(first_a, tp, to_major_2)
-    jump_minor = lax.ppermute(first_b, tp, to_minor_2)
+    jumped = lax.ppermute(first, tp, jumps)
     major_3, minor_3 = outs_at((3, -3), BF16)
     r_major = lax.ppermute(major_3, tp, to_major)
     r_minor = lax.ppermute(minor_3, tp, to_minor)
-    major_2, minor_2 = outs_at((2, -2), F32)
-    major_2 = major_2 + jnp.pad(jump_major.astype(F32), ((0, mid), (0, 0)))
-    minor_2 = minor_2 + jnp.pad(jump_minor.astype(F32), ((mid, 0), (0, 0)))
+    major_2, minor_2 = outs_at((2, -2), F32, jumped)
     r_major = lax.ppermute(passed(major_2, r_major), tp, to_major)
     r_minor = lax.ppermute(passed(minor_2, r_minor), tp, to_minor)
     major_1, minor_1, own_out = outs_at((1, -1, 0), F32)

time: 142 us -> 130 us (0.915)
  starting transfers between devices: 84.8 us -> 78.2 us
  Pallas kernels: 15.6 us -> 11.2 us
    ppermute x1, starting transfers between devices: 13.4 us -> 7.2 us  [shards(): theirs = lax.ppermute(other, 'c', mate)]
    pallas_call x7, Pallas kernels: 11.8 us -> 8 us  [call_vmem(): pl.pallas_call(kernel, out_shape=out_shape, in_specs=[pl.BlockSpec(memory...]
    ppermute x1, waiting for transfers between devices: 0.01 us -> 3.78 us  [shards(): r_minor = lax.ppermute(minor_3, tp, to_minor)]
    ppermute x2 -> x1, starting transfers between devices: 6.46 us -> 4.08 us  [shards(): jumped = lax.ppermute(first, tp, jumps)]
    ppermute x1, waiting for transfers between devices: 7.75 us -> 6.23 us  [shards(): r_major = lax.ppermute(passed(major_1, r_major), tp, to_major)]
  transfers between devices with their start and end apart: 20 -> 19, of which waited for: 8 -> 8; matrix products, arithmetic and copies ran while one was open for 4% -> 5% of each run, Pallas kernels for 5% -> 4%
where the time goes in v3:
time: 130 us
  starting transfers between devices  78.2 us (60%)
  waiting for transfers between devices  32.5 us (25%)
  Pallas kernels  11.2 us (9%)
  local copies, waits for them, and re-layouts  3.89 us (3%)
  other arithmetic  2.97 us (2%)
    all_to_all x1, starting transfers between devices, shards(): lax.all_to_all(sent.reshape(experts, slots, quarter), 'ep', 0, 0, tiled=T...  13.8 us
    all_to_all x1, waiting for transfers between devices, shards(): lax.all_to_all(back, 'ep', 0, 0, tiled=True).reshape(experts * slots, piece)  11.6 us
    pallas_call x7, Pallas kernels, call_vmem(): pl.pallas_call(kernel, out_shape=out_shape, in_specs=[pl.BlockSpec(memory...  8 us
    all_to_all x1, waiting for transfers between devices, shards(): lax.all_to_all(sent.reshape(experts, slots, quarter), 'ep', 0, 0, tiled=T...  7.81 us
    ppermute x1, starting transfers between devices, shards(): theirs = lax.ppermute(other, 'c', mate)  7.2 us
    all_to_all x1, starting transfers between devices, shards(): lax.all_to_all(back, 'ep', 0, 0, tiled=True).reshape(experts * slots, piece)  6.23 us
    ppermute x1, waiting for transfers between devices, shards(): r_major = lax.ppermute(passed(major_1, r_major), tp, to_major)  6.23 us
    ppermute x1, starting transfers between devices, shards(): r_minor = lax.ppermute(passed(minor_1, r_minor), tp, to_minor)  4.75 us
  transfers between devices with their start and end apart: 19, of which 8 were waited for; matrix products, arithmetic and copies ran while one was open for 5% of the time, Pallas kernels for 4%

profile of v3, /device:TPU:1, one launch (start us, length us, event | category | flops | bytes accessed | tf_op | source)
XLA Modules:
  0.0 129.5 jit_solution(1562319281000116200)
XLA Ops:
  0.0 3.2 %shard_map.73 = (bf16[768,256]{1,0:T(8,128)(2,1)}, bf16[768,512]{1,0:T(8,128)(2,1)}) custom-call(bf16[256,2048]{1,0:T(8,128)(2,1)} %tokens_in.1, f32[1,2048]{1,0:T(1,128)} %bitcast.25, s32[32,1024]{1,0:T(8,128)} %chosen_in.1), custom_call_target="tpu_custom_call" | custom-call | tf_op jit(solution)/shard_map/pallas_call | solution.py:75
  3.2 13.8 %all-to-all-start = ((bf16[32,24,512]{2,1,0:T(8,128)(2,1)}), bf16[32,24,512]{2,1,0:T(8,128)(2,1)S(1)}, u32[]{:S(2)}, u32[]{:S(2)}) async-start(bf16[32,24,512]{2,1,0:T(8,128)(2,1)} %bitcast.23), calls=%async_computation | async-start | bytes 1572864 | tf_op jit(solution)/shard_map/all_to_all | solution.py:221
  17.1 2.9 %collective-permute-start.6 = (bf16[2048,256]{1,0:T(8,128)(2,1)}, bf16[2048,256]{1,0:T(8,128)(2,1)}, u32[]{:S(2)}, u32[]{:S(2)}) collective-permute-start(bf16[2048,256]{1,0:T(8,128)(2,1)} %bitcast.5), channel_id=1, source_target_pairs={{0,1},{1,0},{2,3},{3,2},{4,5},{5,4},{6,7},{7,6},{8,9},{9,8},{10,11... | collective-permute-start | bytes 3145736 | tf_op jit(solution)/shard_map/ppermute | solution.py:227
  20.0 1.9 %collective-permute-start.7 = (bf16[2048,256]{1,0:T(8,128)(2,1)}, bf16[2048,256]{1,0:T(8,128)(2,1)}, u32[]{:S(2)}, u32[]{:S(2)}) collective-permute-start(bf16[2048,256]{1,0:T(8,128)(2,1)} %bitcast.6), channel_id=1, source_target_pairs={{0,1},{1,0},{2,3},{3,2},{4,5},{5,4},{6,7},{7,6},{8,9},{9,8},{10,11... | collective-permute-start | bytes 3145736 | tf_op jit(solution)/shard_map/ppermute | solution.py:228
  21.9 2.4 %collective-permute-start.8 = (bf16[256,2048]{1,0:T(8,128)(2,1)S(1)}, bf16[256,2048]{1,0:T(8,128)(2,1)S(1)}, u32[]{:S(2)}, u32[]{:S(2)}) collective-permute-start(bf16[256,2048]{1,0:T(8,128)(2,1)S(1)} %bitcast.16), channel_id=1, source_target_pairs={{0,1},{1,0},{2,3},{3,2},{4,5},{5,4},{6,7},{7,6},{8,9},{9,8},{10,11... | collective-permute-start | bytes 3145736 | tf_op jit(solution)/shard_map/ppermute | solution.py:229
  24.3 0.8 constant_dynamic-slice_fusion.1
  25.1 0.2 convert_reduce_fusion
  25.4 0.5 broadcast.40
  25.9 0.1 copy-done.2
  26.0 0.7 reduce.3
  26.7 0.2 reshape.115
  26.9 0.1 constant_dynamic-slice_fusion.weight
  27.1 0.9 add.80
  28.0 0.1 add.70
  28.2 0.9 lt.70
  29.2 1.2 compare_select_fusion.k_slot
  30.3 7.8 %all-to-all-done = bf16[32,24,512]{2,1,0:T(8,128)(2,1)S(1)} async-done(((bf16[32,24,512]{2,1,0:T(8,128)(2,1)}), bf16[32,24,512]{2,1,0:T(8,128)(2,1)S(1)}, u32[]{:S(2)}, u32[]{:S(2)}) %all-to-all-start) | async-done | bytes 786464 | tf_op jit(solution)/shard_map/all_to_all | solution.py:221
  38.1 0.6 shard_map.74
  38.7 3.2 %collective-permute-start = (bf16[256,512]{1,0:T(8,128)(2,1)S(1)}, bf16[256,512]{1,0:T(8,128)(2,1)S(1)}, u32[]{:S(2)}, u32[]{:S(2)}) collective-permute-start(bf16[256,512]{1,0:T(8,128)(2,1)S(1)} %get-tuple-element.37), channel_id=1, source_target_pairs={{0,2},{1,3},{2,4},{3,5},{4,6},{5,7},{6,8},{7,9},{8,10},{9,11},{10,... | collective-permute-start | bytes 786440 | tf_op jit(solution)/shard_map/ppermute | solution.py:252
  41.9 3.8 %collective-permute-start.2 = (bf16[256,512]{1,0:T(8,128)(2,1)S(1)}, bf16[256,512]{1,0:T(8,128)(2,1)S(1)}, u32[]{:S(2)}, u32[]{:S(2)}) collective-permute-start(bf16[256,512]{1,0:T(8,128)(2,1)S(1)} %get-tuple-element.38), channel_id=1, source_target_pairs={{2,0},{3,1},{4,2},{5,3},{6,4},{7,5},{8,6},{9,7},{10,8},{11,9},{12,... | collective-permute-start | bytes 786440 | tf_op jit(solution)/shard_map/ppermute | solution.py:253
  45.8 1.9 %collective-permute-start.4 = (bf16[256,512]{1,0:T(8,128)(2,1)S(1)}, bf16[256,512]{1,0:T(8,128)(2,1)S(1)}, u32[]{:S(2)}, u32[]{:S(2)}) collective-permute-start(bf16[256,512]{1,0:T(8,128)(2,1)S(1)} %get-tuple-element.38), channel_id=1, source_target_pairs={{0,2},{1,3},{2,4},{3,5},{4,6},{5,7},{6,8},{7,9},{8,10},{9,11},{10,... | collective-permute-start | bytes 786440 | tf_op jit(solution)/shard_map/ppermute | solution.py:254
  47.7 4.6 %collective-permute-start.5 = (bf16[256,512]{1,0:T(8,128)(2,1)S(1)}, bf16[256,512]{1,0:T(8,128)(2,1)S(1)}, u32[]{:S(2)}, u32[]{:S(2)}) collective-permute-start(bf16[256,512]{1,0:T(8,128)(2,1)S(1)} %get-tuple-element.37), channel_id=1, source_target_pairs={{2,0},{3,1},{4,2},{5,3},{6,4},{7,5},{8,6},{9,7},{10,8},{11,9},{12,... | collective-permute-start | bytes 786440 | tf_op jit(solution)/shard_map/ppermute | solution.py:255
  52.3 1.9 %collective-permute-start.1 = (bf16[256,512]{1,0:T(8,128)(2,1)S(1)}, bf16[256,512]{1,0:T(8,128)(2,1)S(1)}, u32[]{:S(2)}, u32[]{:S(2)}) collective-permute-start(bf16[256,512]{1,0:T(8,128)(2,1)S(1)} %collective-permute-done.major_a), channel_id=1, source_target_pairs={{0,2},{1,3},{2,4},{3,5},{4,6},{5,7},{6,8},{7,9},{8,10},{9,11},{10,... | collective-permute-start | bytes 786440 | tf_op jit(solution)/shard_map/ppermute | solution.py:256
  54.2 4.6 %collective-permute-start.3 = (bf16[256,512]{1,0:T(8,128)(2,1)S(1)}, bf16[256,512]{1,0:T(8,128)(2,1)S(1)}, u32[]{:S(2)}, u32[]{:S(2)}) collective-permute-start(bf16[256,512]{1,0:T(8,128)(2,1)S(1)} %collective-permute-done.2.minor_b), channel_id=1, source_target_pairs={{2,0},{3,1},{4,2},{5,3},{6,4},{7,5},{8,6},{9,7},{10,8},{11,9},{12,... | collective-permute-start | bytes 786440 | tf_op jit(solution)/shard_map/ppermute | solution.py:257
  58.8 3.6 %shard_map.75 = (f32[512,256]{1,0:T(8,128)S(1)}, f32[512,256]{1,0:T(8,128)S(1)}, f32[512,256]{1,0:T(8,128)S(1)}, f32[512,256]{1,0:T(8,128)S(1)}, bf16[4,2,256,256]{3,2,1,0:T(8,128)(2,1)S(1)}) custom-call(s32[1]{0:T(128)} %bitcast.1.where_ref, bf16[512,512]{1,0:T(8,128)(2,1)S(1)} %get-tuple-element.39.own, bf16[256,512]{1,0:T(8,128)(2,1)S(1)} %collective-permute-done.major_a, ...), custom_call_target="tpu_custom_call" | custom-call | flops 1610612736 | bytes 8388608 | tf_op jit(solution)/shard_map/pallas_call | solution.py:189
  62.5 1.1 shard_map.76
  63.6 4.1 %collective-permute-start.9 = (bf16[512,256]{1,0:T(8,128)(2,1)S(1)}, bf16[512,256]{1,0:T(8,128)(2,1)S(1)}, u32[]{:S(2)}, u32[]{:S(2)}) collective-permute-start(bf16[512,256]{1,0:T(8,128)(2,1)S(1)} %get-tuple-element.52), channel_id=1, source_target_pairs={{0,4},{1,13},{2,6},{3,15},{4,8},{5,1},{6,10},{7,3},{8,12},{9,5},{1... | collective-permute-start | bytes 786440 | tf_op jit(solution)/shard_map/ppermute | solution.py:294
  67.7 0.5 shard_map.79
  68.1 3.0 %collective-permute-start.13 = (bf16[512,256]{1,0:T(8,128)(2,1)S(1)}, bf16[512,256]{1,0:T(8,128)(2,1)S(1)}, u32[]{:S(2)}, u32[]{:S(2)}) collective-permute-start(bf16[512,256]{1,0:T(8,128)(2,1)S(1)} %get-tuple-element.57), channel_id=1, source_target_pairs={{2,0},{3,1},{4,2},{5,3},{6,4},{7,5},{8,6},{9,7},{10,8},{11,9},{12,... | collective-permute-start | bytes 786440 | tf_op jit(solution)/shard_map/ppermute | solution.py:297
  71.1 2.7 %collective-permute-start.10 = (bf16[512,256]{1,0:T(8,128)(2,1)S(1)}, bf16[512,256]{1,0:T(8,128)(2,1)S(1)}, u32[]{:S(2)}, u32[]{:S(2)}) collective-permute-start(bf16[512,256]{1,0:T(8,128)(2,1)S(1)} %get-tuple-element.54), channel_id=1, source_target_pairs={{0,2},{1,3},{2,4},{3,5},{4,6},{5,7},{6,8},{7,9},{8,10},{9,11},{10,... | collective-permute-start | bytes 786440 | tf_op jit(solution)/shard_map/ppermute | solution.py:296
  73.9 0.5 shard_map.78
  74.3 3.8 %collective-permute-done.13 = bf16[512,256]{1,0:T(8,128)(2,1)S(1)} collective-permute-done((bf16[512,256]{1,0:T(8,128)(2,1)S(1)}, bf16[512,256]{1,0:T(8,128)(2,1)S(1)}, u32[]{:S(2)}, u32[]{:S(2)}) %collective-permute-start.13) | collective-permute-done | bytes 262176 | tf_op jit(solution)/shard_map/ppermute | solution.py:297
  78.2 4.6 %collective-permute-start.14 = (bf16[512,256]{1,0:T(8,128)(2,1)S(1)}, bf16[512,256]{1,0:T(8,128)(2,1)S(1)}, u32[]{:S(2)}, u32[]{:S(2)}) collective-permute-start(bf16[512,256]{1,0:T(8,128)(2,1)S(1)} %add_convert_fusion.1), channel_id=1, source_target_pairs={{2,0},{3,1},{4,2},{5,3},{6,4},{7,5},{8,6},{9,7},{10,8},{11,9},{12,... | collective-permute-start | bytes 786440 | tf_op jit(solution)/shard_map/ppermute | solution.py:300
  82.7 0.9 collective-permute-done.10
  83.7 2.7 %collective-permute-start.11 = (bf16[512,256]{1,0:T(8,128)(2,1)S(1)}, bf16[512,256]{1,0:T(8,128)(2,1)S(1)}, u32[]{:S(2)}, u32[]{:S(2)}) collective-permute-start(bf16[512,256]{1,0:T(8,128)(2,1)S(1)} %add_convert_fusion.3), channel_id=1, source_target_pairs={{0,2},{1,3},{2,4},{3,5},{4,6},{5,7},{6,8},{7,9},{8,10},{9,11},{10,... | collective-permute-start | bytes 786440 | tf_op jit(solution)/shard_map/ppermute | solution.py:299
  86.5 0.6 shard_map.77
  87.2 4.8 %collective-permute-start.15 = (bf16[512,256]{1,0:T(8,128)(2,1)S(1)}, bf16[512,256]{1,0:T(8,128)(2,1)S(1)}, u32[]{:S(2)}, u32[]{:S(2)}) collective-permute-start(bf16[512,256]{1,0:T(8,128)(2,1)S(1)} %add_convert_fusion), channel_id=1, source_target_pairs={{2,0},{3,1},{4,2},{5,3},{6,4},{7,5},{8,6},{9,7},{10,8},{11,9},{12,... | collective-permute-start | bytes 786440 | tf_op jit(solution)/shard_map/ppermute | solution.py:303
  91.9 1.1 collective-permute-done.11
  93.1 1.9 %collective-permute-start.12 = (bf16[512,256]{1,0:T(8,128)(2,1)S(1)}, bf16[512,256]{1,0:T(8,128)(2,1)S(1)}, u32[]{:S(2)}, u32[]{:S(2)}) collective-permute-start(bf16[512,256]{1,0:T(8,128)(2,1)S(1)} %add_convert_fusion.2), channel_id=1, source_target_pairs={{0,2},{1,3},{2,4},{3,5},{4,6},{5,7},{6,8},{7,9},{8,10},{9,11},{10,... | collective-permute-start | bytes 786440 | tf_op jit(solution)/shard_map/ppermute | solution.py:302
  95.0 0.2 collective-permute-done.15.r_minor
  95.2 6.2 %collective-permute-done.12.r_major = bf16[512,256]{1,0:T(8,128)(2,1)S(1)} collective-permute-done((bf16[512,256]{1,0:T(8,128)(2,1)S(1)}, bf16[512,256]{1,0:T(8,128)(2,1)S(1)}, u32[]{:S(2)}, u32[]{:S(2)}) %collective-permute-start.12) | collective-permute-done | bytes 262176 | tf_op jit(solution)/shard_map/ppermute | solution.py:302
  101.4 1.2 shard_map.80
  102.7 6.2 %all-to-all-start.1 = ((bf16[32,24,256]{2,1,0:T(8,128)(2,1)}), bf16[32,24,256]{2,1,0:T(8,128)(2,1)S(1)}, u32[]{:S(2)}, u32[]{:S(2)}) async-start(bf16[32,24,256]{2,1,0:T(8,128)(2,1)} %bitcast.12), calls=%async_computation.1 | async-start | bytes 786432 | tf_op jit(solution)/shard_map/all_to_all | solution.py:312
  108.9 11.6 %all-to-all-done.1 = bf16[32,24,256]{2,1,0:T(8,128)(2,1)S(1)} async-done(((bf16[32,24,256]{2,1,0:T(8,128)(2,1)}), bf16[32,24,256]{2,1,0:T(8,128)(2,1)S(1)}, u32[]{:S(2)}, u32[]{:S(2)}) %all-to-all-start.1) | async-done | bytes 393248 | tf_op jit(solution)/shard_map/all_to_all | solution.py:312
  120.5 0.3 fusion.1
  120.8 7.2 %collective-permute-start.16 = (bf16[256,128]{1,0:T(8,128)(2,1)S(1)}, bf16[256,128]{1,0:T(8,128)(2,1)S(1)}, u32[]{:S(2)}, u32[]{:S(2)}) collective-permute-start(bf16[256,128]{1,0:T(8,128)(2,1)S(1)} %dynamic-slice_convert_fusion), channel_id=1, source_target_pairs={{0,1},{1,0},{2,3},{3,2},{4,5},{5,4},{6,7},{7,6},{8,9},{9,8},{10,11... | collective-permute-start | bytes 196616 | tf_op jit(solution)/shard_map/ppermute | solution.py:316
  128.0 0.9 collective-permute-done.16
  128.9 0.6 add_convert_fusion.4
  (28 shorter events, 0.6 us)
Async XLA Ops:
  3.2 18.7 %copy-start = (bf16[1,256,2048]{2,1,0:T(8,128)(2,1)S(1)}, bf16[1,256,2048]{2,1,0:T(8,128)(2,1)}, u32[]{:S(2)}) copy-start(bf16[1,256,2048]{2,1,0:T(8,128)(2,1)} %param.13) | copy-start | bytes 3145732
  3.2 34.9 %all-to-all-start = ((bf16[32,24,512]{2,1,0:T(8,128)(2,1)}), bf16[32,24,512]{2,1,0:T(8,128)(2,1)S(1)}, u32[]{:S(2)}, u32[]{:S(2)}) async-start(bf16[32,24,512]{2,1,0:T(8,128)(2,1)} %bitcast.23), calls=%async_computation | async-start | bytes 1572864 | tf_op jit(solution)/shard_map/all_to_all | solution.py:221
  17.1 28.7 %collective-permute-start.6 = (bf16[2048,256]{1,0:T(8,128)(2,1)}, bf16[2048,256]{1,0:T(8,128)(2,1)}, u32[]{:S(2)}, u32[]{:S(2)}) collective-permute-start(bf16[2048,256]{1,0:T(8,128)(2,1)} %bitcast.5), channel_id=1, source_target_pairs={{0,1},{1,0},{2,3},{3,2},{4,5},{5,4},{6,7},{7,6},{8,9},{9,8},{10,11... | collective-permute-start | bytes 3145736 | tf_op jit(solution)/shard_map/ppermute | solution.py:227
  20.0 27.8 %collective-permute-start.7 = (bf16[2048,256]{1,0:T(8,128)(2,1)}, bf16[2048,256]{1,0:T(8,128)(2,1)}, u32[]{:S(2)}, u32[]{:S(2)}) collective-permute-start(bf16[2048,256]{1,0:T(8,128)(2,1)} %bitcast.6), channel_id=1, source_target_pairs={{0,1},{1,0},{2,3},{3,2},{4,5},{5,4},{6,7},{7,6},{8,9},{9,8},{10,11... | collective-permute-start | bytes 3145736 | tf_op jit(solution)/shard_map/ppermute | solution.py:228
  21.9 40.5 %collective-permute-start.8 = (bf16[256,2048]{1,0:T(8,128)(2,1)S(1)}, bf16[256,2048]{1,0:T(8,128)(2,1)S(1)}, u32[]{:S(2)}, u32[]{:S(2)}) collective-permute-start(bf16[256,2048]{1,0:T(8,128)(2,1)S(1)} %bitcast.16), channel_id=1, source_target_pairs={{0,1},{1,0},{2,3},{3,2},{4,5},{5,4},{6,7},{7,6},{8,9},{9,8},{10,11... | collective-permute-start | bytes 3145736 | tf_op jit(solution)/shard_map/ppermute | solution.py:229
  25.3 0.7 copy-start.2
  38.7 13.6 %collective-permute-start = (bf16[256,512]{1,0:T(8,128)(2,1)S(1)}, bf16[256,512]{1,0:T(8,128)(2,1)S(1)}, u32[]{:S(2)}, u32[]{:S(2)}) collective-permute-start(bf16[256,512]{1,0:T(8,128)(2,1)S(1)} %get-tuple-element.37), channel_id=1, source_target_pairs={{0,2},{1,3},{2,4},{3,5},{4,6},{5,7},{6,8},{7,9},{8,10},{9,11},{10,... | collective-permute-start | bytes 786440 | tf_op jit(solution)/shard_map/ppermute | solution.py:252
  41.9 12.3 %collective-permute-start.2 = (bf16[256,512]{1,0:T(8,128)(2,1)S(1)}, bf16[256,512]{1,0:T(8,128)(2,1)S(1)}, u32[]{:S(2)}, u32[]{:S(2)}) collective-permute-start(bf16[256,512]{1,0:T(8,128)(2,1)S(1)} %get-tuple-element.38), channel_id=1, source_target_pairs={{2,0},{3,1},{4,2},{5,3},{6,4},{7,5},{8,6},{9,7},{10,8},{11,9},{12,... | collective-permute-start | bytes 786440 | tf_op jit(solution)/shard_map/ppermute | solution.py:253
  45.8 13.1 %collective-permute-start.4 = (bf16[256,512]{1,0:T(8,128)(2,1)S(1)}, bf16[256,512]{1,0:T(8,128)(2,1)S(1)}, u32[]{:S(2)}, u32[]{:S(2)}) collective-permute-start(bf16[256,512]{1,0:T(8,128)(2,1)S(1)} %get-tuple-element.38), channel_id=1, source_target_pairs={{0,2},{1,3},{2,4},{3,5},{4,6},{5,7},{6,8},{7,9},{8,10},{9,11},{10,... | collective-permute-start | bytes 786440 | tf_op jit(solution)/shard_map/ppermute | solution.py:254
  47.7 11.1 %collective-permute-start.5 = (bf16[256,512]{1,0:T(8,128)(2,1)S(1)}, bf16[256,512]{1,0:T(8,128)(2,1)S(1)}, u32[]{:S(2)}, u32[]{:S(2)}) collective-permute-start(bf16[256,512]{1,0:T(8,128)(2,1)S(1)} %get-tuple-element.37), channel_id=1, source_target_pairs={{2,0},{3,1},{4,2},{5,3},{6,4},{7,5},{8,6},{9,7},{10,8},{11,9},{12,... | collective-permute-start | bytes 786440 | tf_op jit(solution)/shard_map/ppermute | solution.py:255
  52.3 10.1 %collective-permute-start.1 = (bf16[256,512]{1,0:T(8,128)(2,1)S(1)}, bf16[256,512]{1,0:T(8,128)(2,1)S(1)}, u32[]{:S(2)}, u32[]{:S(2)}) collective-permute-start(bf16[256,512]{1,0:T(8,128)(2,1)S(1)} %collective-permute-done.major_a), channel_id=1, source_target_pairs={{0,2},{1,3},{2,4},{3,5},{4,6},{5,7},{6,8},{7,9},{8,10},{9,11},{10,... | collective-permute-start | bytes 786440 | tf_op jit(solution)/shard_map/ppermute | solution.py:256
  54.2 8.2 %collective-permute-start.3 = (bf16[256,512]{1,0:T(8,128)(2,1)S(1)}, bf16[256,512]{1,0:T(8,128)(2,1)S(1)}, u32[]{:S(2)}, u32[]{:S(2)}) collective-permute-start(bf16[256,512]{1,0:T(8,128)(2,1)S(1)} %collective-permute-done.2.minor_b), channel_id=1, source_target_pairs={{2,0},{3,1},{4,2},{5,3},{6,4},{7,5},{8,6},{9,7},{10,8},{11,9},{12,... | collective-permute-start | bytes 786440 | tf_op jit(solution)/shard_map/ppermute | solution.py:257
  63.6 10.3 %collective-permute-start.9 = (bf16[512,256]{1,0:T(8,128)(2,1)S(1)}, bf16[512,256]{1,0:T(8,128)(2,1)S(1)}, u32[]{:S(2)}, u32[]{:S(2)}) collective-permute-start(bf16[512,256]{1,0:T(8,128)(2,1)S(1)} %get-tuple-element.52), channel_id=1, source_target_pairs={{0,4},{1,13},{2,6},{3,15},{4,8},{5,1},{6,10},{7,3},{8,12},{9,5},{1... | collective-permute-start | bytes 786440 | tf_op jit(solution)/shard_map/ppermute | solution.py:294
  68.1 10.0 %collective-permute-start.13 = (bf16[512,256]{1,0:T(8,128)(2,1)S(1)}, bf16[512,256]{1,0:T(8,128)(2,1)S(1)}, u32[]{:S(2)}, u32[]{:S(2)}) collective-permute-start(bf16[512,256]{1,0:T(8,128)(2,1)S(1)} %get-tuple-element.57), channel_id=1, source_target_pairs={{2,0},{3,1},{4,2},{5,3},{6,4},{7,5},{8,6},{9,7},{10,8},{11,9},{12,... | collective-permute-start | bytes 786440 | tf_op jit(solution)/shard_map/ppermute | solution.py:297
  71.1 12.6 %collective-permute-start.10 = (bf16[512,256]{1,0:T(8,128)(2,1)S(1)}, bf16[512,256]{1,0:T(8,128)(2,1)S(1)}, u32[]{:S(2)}, u32[]{:S(2)}) collective-permute-start(bf16[512,256]{1,0:T(8,128)(2,1)S(1)} %get-tuple-element.54), channel_id=1, source_target_pairs={{0,2},{1,3},{2,4},{3,5},{4,6},{5,7},{6,8},{7,9},{8,10},{9,11},{10,... | collective-permute-start | bytes 786440 | tf_op jit(solution)/shard_map/ppermute | solution.py:296
  78.2 8.9 %collective-permute-start.14 = (bf16[512,256]{1,0:T(8,128)(2,1)S(1)}, bf16[512,256]{1,0:T(8,128)(2,1)S(1)}, u32[]{:S(2)}, u32[]{:S(2)}) collective-permute-start(bf16[512,256]{1,0:T(8,128)(2,1)S(1)} %add_convert_fusion.1), channel_id=1, source_target_pairs={{2,0},{3,1},{4,2},{5,3},{6,4},{7,5},{8,6},{9,7},{10,8},{11,9},{12,... | collective-permute-start | bytes 786440 | tf_op jit(solution)/shard_map/ppermute | solution.py:300
  83.7 9.3 %collective-permute-start.11 = (bf16[512,256]{1,0:T(8,128)(2,1)S(1)}, bf16[512,256]{1,0:T(8,128)(2,1)S(1)}, u32[]{:S(2)}, u32[]{:S(2)}) collective-permute-start(bf16[512,256]{1,0:T(8,128)(2,1)S(1)} %add_convert_fusion.3), channel_id=1, source_target_pairs={{0,2},{1,3},{2,4},{3,5},{4,6},{5,7},{6,8},{7,9},{8,10},{9,11},{10,... | collective-permute-start | bytes 786440 | tf_op jit(solution)/shard_map/ppermute | solution.py:299
  87.2 8.1 %collective-permute-start.15 = (bf16[512,256]{1,0:T(8,128)(2,1)S(1)}, bf16[512,256]{1,0:T(8,128)(2,1)S(1)}, u32[]{:S(2)}, u32[]{:S(2)}) collective-permute-start(bf16[512,256]{1,0:T(8,128)(2,1)S(1)} %add_convert_fusion), channel_id=1, source_target_pairs={{2,0},{3,1},{4,2},{5,3},{6,4},{7,5},{8,6},{9,7},{10,8},{11,9},{12,... | collective-permute-start | bytes 786440 | tf_op jit(solution)/shard_map/ppermute | solution.py:303
  93.1 8.3 %collective-permute-start.12 = (bf16[512,256]{1,0:T(8,128)(2,1)S(1)}, bf16[512,256]{1,0:T(8,128)(2,1)S(1)}, u32[]{:S(2)}, u32[]{:S(2)}) collective-permute-start(bf16[512,256]{1,0:T(8,128)(2,1)S(1)} %add_convert_fusion.2), channel_id=1, source_target_pairs={{0,2},{1,3},{2,4},{3,5},{4,6},{5,7},{6,8},{7,9},{8,10},{9,11},{10,... | collective-permute-start | bytes 786440 | tf_op jit(solution)/shard_map/ppermute | solution.py:302
  102.7 17.8 %copy-start.1 = (bf16[768,256]{1,0:T(8,128)(2,1)S(1)}, bf16[768,256]{1,0:T(8,128)(2,1)}, u32[]{:S(2)}) copy-start(bf16[768,256]{1,0:T(8,128)(2,1)} %get-tuple-element.32) | copy-start | bytes 1179652
  102.7 17.8 %all-to-all-start.1 = ((bf16[32,24,256]{2,1,0:T(8,128)(2,1)}), bf16[32,24,256]{2,1,0:T(8,128)(2,1)S(1)}, u32[]{:S(2)}, u32[]{:S(2)}) async-start(bf16[32,24,256]{2,1,0:T(8,128)(2,1)} %bitcast.12), calls=%async_computation.1 | async-start | bytes 786432 | tf_op jit(solution)/shard_map/all_to_all | solution.py:312
  120.8 8.1 %collective-permute-start.16 = (bf16[256,128]{1,0:T(8,128)(2,1)S(1)}, bf16[256,128]{1,0:T(8,128)(2,1)S(1)}, u32[]{:S(2)}, u32[]{:S(2)}) collective-permute-start(bf16[256,128]{1,0:T(8,128)(2,1)S(1)} %dynamic-slice_convert_fusion), channel_id=1, source_target_pairs={{0,1},{1,0},{2,3},{3,2},{4,5},{5,4},{6,7},{7,6},{8,9},{9,8},{10,11... | collective-permute-start | bytes 196616 | tf_op jit(solution)/shard_map/ppermute | solution.py:316

commit v4 on v2

--- a/solution.py
+++ b/solution.py
@@ -20,7 +20,7 @@
 
 
 def dispatch_kernel(
-    slots, where_ref, tokens_in, gain_in, chosen_in, pick_ref, sent_ref,
+    slots, tokens_in, gain_in, chosen_in, pick_ref, sent_ref,
     held, tokens_ref, gain_ref, chosen_ref, sems,
 ):
     copies = [
@@ -33,7 +33,8 @@
     copies[0].wait()
     tok_rows, width = tokens_ref.shape
     experts, capacity = chosen_ref.shape
-    q, first_token, parity = where_ref[0] & 3, where_ref[1], where_ref[2]
+    q, parity = lax.axis_index("y") & 3, lax.axis_index("c")
+    first_token = lax.axis_index("ep") * tok_rows
     chosen = chosen_ref[...]
     run_start = jnp.sum((chosen < first_token).astype(I32), axis=1, keepdims=True)
     run_end = jnp.sum((chosen < first_token + tok_rows).astype(I32), axis=1, keepdims=True)
@@ -66,7 +67,7 @@
         ).astype(BF16)
 
 
-def dispatch(tokens, norm_gain, chosen, where, slots):
+def dispatch(tokens, norm_gain, chosen, slots):
     experts = chosen.shape[0]
     tok_rows, width = tokens.shape
     rows = experts * slots
@@ -77,7 +78,7 @@
             jax.ShapeDtypeStruct((rows, tok_rows), BF16),
             jax.ShapeDtypeStruct((rows, width // 4), BF16),
         ),
-        in_specs=[pl.BlockSpec(memory_space=pltpu.SMEM)] + [pl.BlockSpec(memory_space=pltpu.HBM)] * 3,
+        in_specs=[pl.BlockSpec(memory_space=pltpu.HBM)] * 3,
         out_specs=(vmem, vmem),
         scratch_shapes=[
             pltpu.VMEM((rows, tok_rows), F32),
@@ -87,7 +88,7 @@
             pltpu.SemaphoreType.DMA((3,)),
         ],
         compiler_params=pltpu.CompilerParams(vmem_limit_bytes=60 << 20),
-    )(where, tokens, norm_gain.reshape(1, width), chosen)
+    )(tokens, norm_gain.reshape(1, width), chosen)
 
 
 def flat(rows):
@@ -216,8 +217,8 @@
         [(target, source) for source, target in pairs] for pairs in (to_major, to_major_2)
     ]
 
-    place = jnp.stack([y, p * tok_rows, c]).astype(I32)
-    pick_token, sent = dispatch(tokens, norm_gain, chosen, place, slots)
+    place = y.astype(I32).reshape(1)
+    pick_token, sent = dispatch(tokens, norm_gain, chosen, slots)
     got = lax.all_to_all(sent.reshape(experts, slots, quarter), "ep", 0, 0, tiled=True)
     got = got.reshape(experts * slots, quarter)
 

time: 142 us -> 138 us (0.972)
  Pallas kernels: 15.6 us -> 11.2 us
    pallas_call x7, Pallas kernels: 11.8 us -> 8.01 us  [call_vmem(): pl.pallas_call(kernel, out_shape=out_shape, in_specs=[pl.BlockSpec(memory...]
  transfers between devices with their start and end apart: 20 -> 20, of which waited for: 8 -> 8; matrix products, arithmetic and copies ran while one was open for 4% -> 4% of each run, Pallas kernels for 5% -> 4%
where the time goes in v4:
time: 138 us; the launch traced here: 137 us
  starting transfers between devices  85.3 us (62%)
  waiting for transfers between devices  33 us (24%)
  Pallas kernels  11.2 us (8%)
  local copies, waits for them, and re-layouts  3.88 us (3%)
  other arithmetic  2.99 us (2%)
    all_to_all x1, starting transfers between devices, shards(): lax.all_to_all(sent.reshape(experts, slots, quarter), 'ep', 0, 0, tiled=T...  13.8 us
    ppermute x1, starting transfers between devices, shards(): theirs = lax.ppermute(other, 'c', mate)  13.4 us
    all_to_all x1, waiting for transfers between devices, shards(): lax.all_to_all(back, 'ep', 0, 0, tiled=True).reshape(experts * slots, piece)  11.4 us
    ppermute x1, waiting for transfers between devices, shards(): r_major = lax.ppermute(passed(major_1, r_major), tp, to_major)  8.31 us
    pallas_call x7, Pallas kernels, call_vmem(): pl.pallas_call(kernel, out_shape=out_shape, in_specs=[pl.BlockSpec(memory...  8.01 us
    all_to_all x1, waiting for transfers between devices, shards(): lax.all_to_all(sent.reshape(experts, slots, quarter), 'ep', 0, 0, tiled=T...  7.82 us
    all_to_all x1, starting transfers between devices, shards(): lax.all_to_all(back, 'ep', 0, 0, tiled=True).reshape(experts * slots, piece)  5.36 us
    ppermute x1, starting transfers between devices, shards(): r_minor = lax.ppermute(minor_3, tp, to_minor)  4.76 us
  transfers between devices with their start and end apart: 20, of which 8 were waited for; matrix products, arithmetic and copies ran while one was open for 4% of the time, Pallas kernels for 4%

profile of v4, /device:TPU:1, one launch (start us, length us, event | category | flops | bytes accessed | tf_op | source)
XLA Modules:
  0.0 137.1 jit_solution(6527046680196879513)
XLA Ops:
  0.0 3.2 %shard_map.73 = (bf16[768,256]{1,0:T(8,128)(2,1)}, bf16[768,512]{1,0:T(8,128)(2,1)}) custom-call(bf16[256,2048]{1,0:T(8,128)(2,1)} %tokens_in.1, f32[1,2048]{1,0:T(1,128)} %bitcast.25, s32[32,1024]{1,0:T(8,128)} %chosen_in.1), custom_call_target="tpu_custom_call" | custom-call | tf_op jit(solution)/shard_map/pallas_call | solution.py:75
  3.2 13.8 %all-to-all-start = ((bf16[32,24,512]{2,1,0:T(8,128)(2,1)}), bf16[32,24,512]{2,1,0:T(8,128)(2,1)S(1)}, u32[]{:S(2)}, u32[]{:S(2)}) async-start(bf16[32,24,512]{2,1,0:T(8,128)(2,1)} %bitcast.23), calls=%async_computation | async-start | bytes 1572864 | tf_op jit(solution)/shard_map/all_to_all | solution.py:222
  17.1 2.9 %collective-permute-start.6 = (bf16[2048,256]{1,0:T(8,128)(2,1)}, bf16[2048,256]{1,0:T(8,128)(2,1)}, u32[]{:S(2)}, u32[]{:S(2)}) collective-permute-start(bf16[2048,256]{1,0:T(8,128)(2,1)} %bitcast.5), channel_id=1, source_target_pairs={{0,1},{1,0},{2,3},{3,2},{4,5},{5,4},{6,7},{7,6},{8,9},{9,8},{10,11... | collective-permute-start | bytes 3145736 | tf_op jit(solution)/shard_map/ppermute | solution.py:228
  19.9 1.9 %collective-permute-start.7 = (bf16[2048,256]{1,0:T(8,128)(2,1)}, bf16[2048,256]{1,0:T(8,128)(2,1)}, u32[]{:S(2)}, u32[]{:S(2)}) collective-permute-start(bf16[2048,256]{1,0:T(8,128)(2,1)} %bitcast.6), channel_id=1, source_target_pairs={{0,1},{1,0},{2,3},{3,2},{4,5},{5,4},{6,7},{7,6},{8,9},{9,8},{10,11... | collective-permute-start | bytes 3145736 | tf_op jit(solution)/shard_map/ppermute | solution.py:229
  21.9 2.4 %collective-permute-start.8 = (bf16[256,2048]{1,0:T(8,128)(2,1)S(1)}, bf16[256,2048]{1,0:T(8,128)(2,1)S(1)}, u32[]{:S(2)}, u32[]{:S(2)}) collective-permute-start(bf16[256,2048]{1,0:T(8,128)(2,1)S(1)} %bitcast.16), channel_id=1, source_target_pairs={{0,1},{1,0},{2,3},{3,2},{4,5},{5,4},{6,7},{7,6},{8,9},{9,8},{10,11... | collective-permute-start | bytes 3145736 | tf_op jit(solution)/shard_map/ppermute | solution.py:230
  24.3 0.8 constant_dynamic-slice_fusion.1
  25.1 0.2 convert_reduce_fusion
  25.4 0.5 broadcast.44
  25.9 0.1 copy-done.2
  26.0 0.7 reduce.3
  26.6 0.2 reshape.115
  26.9 0.1 constant_dynamic-slice_fusion.weight
  27.1 0.9 add.92
  28.1 0.9 lt.70
  29.2 1.2 compare_select_fusion.k_slot
  30.3 7.8 %all-to-all-done = bf16[32,24,512]{2,1,0:T(8,128)(2,1)S(1)} async-done(((bf16[32,24,512]{2,1,0:T(8,128)(2,1)}), bf16[32,24,512]{2,1,0:T(8,128)(2,1)S(1)}, u32[]{:S(2)}, u32[]{:S(2)}) %all-to-all-start) | async-done | bytes 786464 | tf_op jit(solution)/shard_map/all_to_all | solution.py:222
  38.1 0.6 shard_map.74
  38.7 3.2 %collective-permute-start = (bf16[256,512]{1,0:T(8,128)(2,1)S(1)}, bf16[256,512]{1,0:T(8,128)(2,1)S(1)}, u32[]{:S(2)}, u32[]{:S(2)}) collective-permute-start(bf16[256,512]{1,0:T(8,128)(2,1)S(1)} %get-tuple-element.38), channel_id=1, source_target_pairs={{0,2},{1,3},{2,4},{3,5},{4,6},{5,7},{6,8},{7,9},{8,10},{9,11},{10,... | collective-permute-start | bytes 786440 | tf_op jit(solution)/shard_map/ppermute | solution.py:253
  41.9 3.8 %collective-permute-start.2 = (bf16[256,512]{1,0:T(8,128)(2,1)S(1)}, bf16[256,512]{1,0:T(8,128)(2,1)S(1)}, u32[]{:S(2)}, u32[]{:S(2)}) collective-permute-start(bf16[256,512]{1,0:T(8,128)(2,1)S(1)} %get-tuple-element.39), channel_id=1, source_target_pairs={{2,0},{3,1},{4,2},{5,3},{6,4},{7,5},{8,6},{9,7},{10,8},{11,9},{12,... | collective-permute-start | bytes 786440 | tf_op jit(solution)/shard_map/ppermute | solution.py:254
  45.8 1.9 %collective-permute-start.4 = (bf16[256,512]{1,0:T(8,128)(2,1)S(1)}, bf16[256,512]{1,0:T(8,128)(2,1)S(1)}, u32[]{:S(2)}, u32[]{:S(2)}) collective-permute-start(bf16[256,512]{1,0:T(8,128)(2,1)S(1)} %get-tuple-element.39), channel_id=1, source_target_pairs={{0,2},{1,3},{2,4},{3,5},{4,6},{5,7},{6,8},{7,9},{8,10},{9,11},{10,... | collective-permute-start | bytes 786440 | tf_op jit(solution)/shard_map/ppermute | solution.py:255
  47.7 4.6 %collective-permute-start.5 = (bf16[256,512]{1,0:T(8,128)(2,1)S(1)}, bf16[256,512]{1,0:T(8,128)(2,1)S(1)}, u32[]{:S(2)}, u32[]{:S(2)}) collective-permute-start(bf16[256,512]{1,0:T(8,128)(2,1)S(1)} %get-tuple-element.38), channel_id=1, source_target_pairs={{2,0},{3,1},{4,2},{5,3},{6,4},{7,5},{8,6},{9,7},{10,8},{11,9},{12,... | collective-permute-start | bytes 786440 | tf_op jit(solution)/shard_map/ppermute | solution.py:256
  52.3 1.9 %collective-permute-start.1 = (bf16[256,512]{1,0:T(8,128)(2,1)S(1)}, bf16[256,512]{1,0:T(8,128)(2,1)S(1)}, u32[]{:S(2)}, u32[]{:S(2)}) collective-permute-start(bf16[256,512]{1,0:T(8,128)(2,1)S(1)} %collective-permute-done.major_a), channel_id=1, source_target_pairs={{0,2},{1,3},{2,4},{3,5},{4,6},{5,7},{6,8},{7,9},{8,10},{9,11},{10,... | collective-permute-start | bytes 786440 | tf_op jit(solution)/shard_map/ppermute | solution.py:257
  54.2 4.6 %collective-permute-start.3 = (bf16[256,512]{1,0:T(8,128)(2,1)S(1)}, bf16[256,512]{1,0:T(8,128)(2,1)S(1)}, u32[]{:S(2)}, u32[]{:S(2)}) collective-permute-start(bf16[256,512]{1,0:T(8,128)(2,1)S(1)} %collective-permute-done.2.minor_b), channel_id=1, source_target_pairs={{2,0},{3,1},{4,2},{5,3},{6,4},{7,5},{8,6},{9,7},{10,8},{11,9},{12,... | collective-permute-start | bytes 786440 | tf_op jit(solution)/shard_map/ppermute | solution.py:258
  58.8 3.6 %shard_map.75 = (f32[512,256]{1,0:T(8,128)S(1)}, f32[512,256]{1,0:T(8,128)S(1)}, f32[512,256]{1,0:T(8,128)S(1)}, f32[512,256]{1,0:T(8,128)S(1)}, bf16[4,2,256,256]{3,2,1,0:T(8,128)(2,1)S(1)}) custom-call(s32[1]{0:T(128)} %bitcast.1.where_ref, bf16[512,512]{1,0:T(8,128)(2,1)S(1)} %get-tuple-element.40.own, bf16[256,512]{1,0:T(8,128)(2,1)S(1)} %collective-permute-done.major_a, ...), custom_call_target="tpu_custom_call" | custom-call | flops 1610612736 | bytes 8388608 | tf_op jit(solution)/shard_map/pallas_call | solution.py:186
  62.4 1.1 shard_map.76
  63.6 0.5 shard_map.79
  64.0 4.8 %collective-permute-start.14 = (bf16[512,256]{1,0:T(8,128)(2,1)S(1)}, bf16[512,256]{1,0:T(8,128)(2,1)S(1)}, u32[]{:S(2)}, u32[]{:S(2)}) collective-permute-start(bf16[512,256]{1,0:T(8,128)(2,1)S(1)} %get-tuple-element.59), channel_id=1, source_target_pairs={{2,0},{3,1},{4,2},{5,3},{6,4},{7,5},{8,6},{9,7},{10,8},{11,9},{12,... | collective-permute-start | bytes 786440 | tf_op jit(solution)/shard_map/ppermute | solution.py:300
  68.8 2.3 %collective-permute-start.13 = (bf16[256,256]{1,0:T(8,128)(2,1)S(1)}, bf16[256,256]{1,0:T(8,128)(2,1)S(1)}, u32[]{:S(2)}, u32[]{:S(2)}) collective-permute-start(bf16[256,256]{1,0:T(8,128)(2,1)S(1)} %get-tuple-element.58), channel_id=1, source_target_pairs={{4,0},{5,1},{6,2},{7,3},{8,4},{9,5},{10,6},{11,7},{12,8},{13,9},{1... | collective-permute-start | bytes 393224 | tf_op jit(solution)/shard_map/ppermute | solution.py:297
  71.1 2.7 %collective-permute-start.10 = (bf16[512,256]{1,0:T(8,128)(2,1)S(1)}, bf16[512,256]{1,0:T(8,128)(2,1)S(1)}, u32[]{:S(2)}, u32[]{:S(2)}) collective-permute-start(bf16[512,256]{1,0:T(8,128)(2,1)S(1)} %get-tuple-element.55), channel_id=1, source_target_pairs={{0,2},{1,3},{2,4},{3,5},{4,6},{5,7},{6,8},{7,9},{8,10},{9,11},{10,... | collective-permute-start | bytes 786440 | tf_op jit(solution)/shard_map/ppermute | solution.py:299
  73.8 3.9 %collective-permute-start.9 = (bf16[256,256]{1,0:T(8,128)(2,1)S(1)}, bf16[256,256]{1,0:T(8,128)(2,1)S(1)}, u32[]{:S(2)}, u32[]{:S(2)}) collective-permute-start(bf16[256,256]{1,0:T(8,128)(2,1)S(1)} %get-tuple-element.54), channel_id=1, source_target_pairs={{0,4},{1,5},{2,6},{3,7},{4,8},{5,9},{6,10},{7,11},{8,12},{9,13},{1... | collective-permute-start | bytes 393224 | tf_op jit(solution)/shard_map/ppermute | solution.py:296
  77.8 0.5 shard_map.78
  78.4 3.7 %collective-permute-start.15 = (bf16[512,256]{1,0:T(8,128)(2,1)S(1)}, bf16[512,256]{1,0:T(8,128)(2,1)S(1)}, u32[]{:S(2)}, u32[]{:S(2)}) collective-permute-start(bf16[512,256]{1,0:T(8,128)(2,1)S(1)} %add_convert_fusion.1), channel_id=1, source_target_pairs={{2,0},{3,1},{4,2},{5,3},{6,4},{7,5},{8,6},{9,7},{10,8},{11,9},{12,... | collective-permute-start | bytes 786440 | tf_op jit(solution)/shard_map/ppermute | solution.py:305
  82.1 1.5 %collective-permute-done.9 = bf16[256,256]{1,0:T(8,128)(2,1)S(1)} collective-permute-done((bf16[256,256]{1,0:T(8,128)(2,1)S(1)}, bf16[256,256]{1,0:T(8,128)(2,1)S(1)}, u32[]{:S(2)}, u32[]{:S(2)}) %collective-permute-start.9) | collective-permute-done | bytes 131104 | tf_op jit(solution)/shard_map/ppermute | solution.py:296
  83.6 1.9 %collective-permute-start.11 = (bf16[512,256]{1,0:T(8,128)(2,1)S(1)}, bf16[512,256]{1,0:T(8,128)(2,1)S(1)}, u32[]{:S(2)}, u32[]{:S(2)}) collective-permute-start(bf16[512,256]{1,0:T(8,128)(2,1)S(1)} %add_convert_fusion.3), channel_id=1, source_target_pairs={{0,2},{1,3},{2,4},{3,5},{4,6},{5,7},{6,8},{7,9},{8,10},{9,11},{10,... | collective-permute-start | bytes 786440 | tf_op jit(solution)/shard_map/ppermute | solution.py:304
  85.6 0.6 shard_map.77
  86.2 0.5 collective-permute-done.15
  86.7 4.2 %collective-permute-start.16 = (bf16[512,256]{1,0:T(8,128)(2,1)S(1)}, bf16[512,256]{1,0:T(8,128)(2,1)S(1)}, u32[]{:S(2)}, u32[]{:S(2)}) collective-permute-start(bf16[512,256]{1,0:T(8,128)(2,1)S(1)} %add_convert_fusion), channel_id=1, source_target_pairs={{2,0},{3,1},{4,2},{5,3},{6,4},{7,5},{8,6},{9,7},{10,8},{11,9},{12,... | collective-permute-start | bytes 786440 | tf_op jit(solution)/shard_map/ppermute | solution.py:308
  91.0 2.1 %collective-permute-done.11 = bf16[512,256]{1,0:T(8,128)(2,1)S(1)} collective-permute-done((bf16[512,256]{1,0:T(8,128)(2,1)S(1)}, bf16[512,256]{1,0:T(8,128)(2,1)S(1)}, u32[]{:S(2)}, u32[]{:S(2)}) %collective-permute-start.11) | collective-permute-done | bytes 262176 | tf_op jit(solution)/shard_map/ppermute | solution.py:304
  93.1 1.9 %collective-permute-start.12 = (bf16[512,256]{1,0:T(8,128)(2,1)S(1)}, bf16[512,256]{1,0:T(8,128)(2,1)S(1)}, u32[]{:S(2)}, u32[]{:S(2)}) collective-permute-start(bf16[512,256]{1,0:T(8,128)(2,1)S(1)} %add_convert_fusion.2), channel_id=1, source_target_pairs={{0,2},{1,3},{2,4},{3,5},{4,6},{5,7},{6,8},{7,9},{8,10},{9,11},{10,... | collective-permute-start | bytes 786440 | tf_op jit(solution)/shard_map/ppermute | solution.py:307
  95.0 0.5 collective-permute-done.16.r_minor
  95.5 8.3 %collective-permute-done.12.r_major = bf16[512,256]{1,0:T(8,128)(2,1)S(1)} collective-permute-done((bf16[512,256]{1,0:T(8,128)(2,1)S(1)}, bf16[512,256]{1,0:T(8,128)(2,1)S(1)}, u32[]{:S(2)}, u32[]{:S(2)}) %collective-permute-start.12) | collective-permute-done | bytes 262176 | tf_op jit(solution)/shard_map/ppermute | solution.py:307
  103.8 1.2 shard_map.80
  105.0 5.4 %all-to-all-start.1 = ((bf16[32,24,256]{2,1,0:T(8,128)(2,1)}), bf16[32,24,256]{2,1,0:T(8,128)(2,1)S(1)}, u32[]{:S(2)}, u32[]{:S(2)}) async-start(bf16[32,24,256]{2,1,0:T(8,128)(2,1)} %bitcast.12), calls=%async_computation.1 | async-start | bytes 786432 | tf_op jit(solution)/shard_map/all_to_all | solution.py:317
  110.4 11.4 %all-to-all-done.1 = bf16[32,24,256]{2,1,0:T(8,128)(2,1)S(1)} async-done(((bf16[32,24,256]{2,1,0:T(8,128)(2,1)}), bf16[32,24,256]{2,1,0:T(8,128)(2,1)S(1)}, u32[]{:S(2)}, u32[]{:S(2)}) %all-to-all-start.1) | async-done | bytes 393248 | tf_op jit(solution)/shard_map/all_to_all | solution.py:317
  121.8 0.3 fusion.1
  122.2 13.4 %collective-permute-start.17 = (bf16[256,128]{1,0:T(8,128)(2,1)S(1)}, bf16[256,128]{1,0:T(8,128)(2,1)S(1)}, u32[]{:S(2)}, u32[]{:S(2)}) collective-permute-start(bf16[256,128]{1,0:T(8,128)(2,1)S(1)} %dynamic-slice_convert_fusion), channel_id=1, source_target_pairs={{0,1},{1,0},{2,3},{3,2},{4,5},{5,4},{6,7},{7,6},{8,9},{9,8},{10,11... | collective-permute-start | bytes 196616 | tf_op jit(solution)/shard_map/ppermute | solution.py:321
  135.6 0.9 collective-permute-done.17
  136.5 0.6 add_convert_fusion.4
  (30 shorter events, 0.7 us)
Async XLA Ops:
  3.2 18.7 %copy-start = (bf16[1,256,2048]{2,1,0:T(8,128)(2,1)S(1)}, bf16[1,256,2048]{2,1,0:T(8,128)(2,1)}, u32[]{:S(2)}) copy-start(bf16[1,256,2048]{2,1,0:T(8,128)(2,1)} %param.13) | copy-start | bytes 3145732
  3.2 34.9 %all-to-all-start = ((bf16[32,24,512]{2,1,0:T(8,128)(2,1)}), bf16[32,24,512]{2,1,0:T(8,128)(2,1)S(1)}, u32[]{:S(2)}, u32[]{:S(2)}) async-start(bf16[32,24,512]{2,1,0:T(8,128)(2,1)} %bitcast.23), calls=%async_computation | async-start | bytes 1572864 | tf_op jit(solution)/shard_map/all_to_all | solution.py:222
  17.1 28.7 %collective-permute-start.6 = (bf16[2048,256]{1,0:T(8,128)(2,1)}, bf16[2048,256]{1,0:T(8,128)(2,1)}, u32[]{:S(2)}, u32[]{:S(2)}) collective-permute-start(bf16[2048,256]{1,0:T(8,128)(2,1)} %bitcast.5), channel_id=1, source_target_pairs={{0,1},{1,0},{2,3},{3,2},{4,5},{5,4},{6,7},{7,6},{8,9},{9,8},{10,11... | collective-permute-start | bytes 3145736 | tf_op jit(solution)/shard_map/ppermute | solution.py:228
  19.9 27.8 %collective-permute-start.7 = (bf16[2048,256]{1,0:T(8,128)(2,1)}, bf16[2048,256]{1,0:T(8,128)(2,1)}, u32[]{:S(2)}, u32[]{:S(2)}) collective-permute-start(bf16[2048,256]{1,0:T(8,128)(2,1)} %bitcast.6), channel_id=1, source_target_pairs={{0,1},{1,0},{2,3},{3,2},{4,5},{5,4},{6,7},{7,6},{8,9},{9,8},{10,11... | collective-permute-start | bytes 3145736 | tf_op jit(solution)/shard_map/ppermute | solution.py:229
  21.9 40.5 %collective-permute-start.8 = (bf16[256,2048]{1,0:T(8,128)(2,1)S(1)}, bf16[256,2048]{1,0:T(8,128)(2,1)S(1)}, u32[]{:S(2)}, u32[]{:S(2)}) collective-permute-start(bf16[256,2048]{1,0:T(8,128)(2,1)S(1)} %bitcast.16), channel_id=1, source_target_pairs={{0,1},{1,0},{2,3},{3,2},{4,5},{5,4},{6,7},{7,6},{8,9},{9,8},{10,11... | collective-permute-start | bytes 3145736 | tf_op jit(solution)/shard_map/ppermute | solution.py:230
  25.3 0.7 copy-start.2
  38.7 13.6 %collective-permute-start = (bf16[256,512]{1,0:T(8,128)(2,1)S(1)}, bf16[256,512]{1,0:T(8,128)(2,1)S(1)}, u32[]{:S(2)}, u32[]{:S(2)}) collective-permute-start(bf16[256,512]{1,0:T(8,128)(2,1)S(1)} %get-tuple-element.38), channel_id=1, source_target_pairs={{0,2},{1,3},{2,4},{3,5},{4,6},{5,7},{6,8},{7,9},{8,10},{9,11},{10,... | collective-permute-start | bytes 786440 | tf_op jit(solution)/shard_map/ppermute | solution.py:253
  41.9 12.3 %collective-permute-start.2 = (bf16[256,512]{1,0:T(8,128)(2,1)S(1)}, bf16[256,512]{1,0:T(8,128)(2,1)S(1)}, u32[]{:S(2)}, u32[]{:S(2)}) collective-permute-start(bf16[256,512]{1,0:T(8,128)(2,1)S(1)} %get-tuple-element.39), channel_id=1, source_target_pairs={{2,0},{3,1},{4,2},{5,3},{6,4},{7,5},{8,6},{9,7},{10,8},{11,9},{12,... | collective-permute-start | bytes 786440 | tf_op jit(solution)/shard_map/ppermute | solution.py:254
  45.8 13.1 %collective-permute-start.4 = (bf16[256,512]{1,0:T(8,128)(2,1)S(1)}, bf16[256,512]{1,0:T(8,128)(2,1)S(1)}, u32[]{:S(2)}, u32[]{:S(2)}) collective-permute-start(bf16[256,512]{1,0:T(8,128)(2,1)S(1)} %get-tuple-element.39), channel_id=1, source_target_pairs={{0,2},{1,3},{2,4},{3,5},{4,6},{5,7},{6,8},{7,9},{8,10},{9,11},{10,... | collective-permute-start | bytes 786440 | tf_op jit(solution)/shard_map/ppermute | solution.py:255
  47.7 11.1 %collective-permute-start.5 = (bf16[256,512]{1,0:T(8,128)(2,1)S(1)}, bf16[256,512]{1,0:T(8,128)(2,1)S(1)}, u32[]{:S(2)}, u32[]{:S(2)}) collective-permute-start(bf16[256,512]{1,0:T(8,128)(2,1)S(1)} %get-tuple-element.38), channel_id=1, source_target_pairs={{2,0},{3,1},{4,2},{5,3},{6,4},{7,5},{8,6},{9,7},{10,8},{11,9},{12,... | collective-permute-start | bytes 786440 | tf_op jit(solution)/shard_map/ppermute | solution.py:256
  52.3 10.1 %collective-permute-start.1 = (bf16[256,512]{1,0:T(8,128)(2,1)S(1)}, bf16[256,512]{1,0:T(8,128)(2,1)S(1)}, u32[]{:S(2)}, u32[]{:S(2)}) collective-permute-start(bf16[256,512]{1,0:T(8,128)(2,1)S(1)} %collective-permute-done.major_a), channel_id=1, source_target_pairs={{0,2},{1,3},{2,4},{3,5},{4,6},{5,7},{6,8},{7,9},{8,10},{9,11},{10,... | collective-permute-start | bytes 786440 | tf_op jit(solution)/shard_map/ppermute | solution.py:257
  54.2 8.2 %collective-permute-start.3 = (bf16[256,512]{1,0:T(8,128)(2,1)S(1)}, bf16[256,512]{1,0:T(8,128)(2,1)S(1)}, u32[]{:S(2)}, u32[]{:S(2)}) collective-permute-start(bf16[256,512]{1,0:T(8,128)(2,1)S(1)} %collective-permute-done.2.minor_b), channel_id=1, source_target_pairs={{2,0},{3,1},{4,2},{5,3},{6,4},{7,5},{8,6},{9,7},{10,8},{11,9},{12,... | collective-permute-start | bytes 786440 | tf_op jit(solution)/shard_map/ppermute | solution.py:258
  64.0 14.2 %collective-permute-start.14 = (bf16[512,256]{1,0:T(8,128)(2,1)S(1)}, bf16[512,256]{1,0:T(8,128)(2,1)S(1)}, u32[]{:S(2)}, u32[]{:S(2)}) collective-permute-start(bf16[512,256]{1,0:T(8,128)(2,1)S(1)} %get-tuple-element.59), channel_id=1, source_target_pairs={{2,0},{3,1},{4,2},{5,3},{6,4},{7,5},{8,6},{9,7},{10,8},{11,9},{12,... | collective-permute-start | bytes 786440 | tf_op jit(solution)/shard_map/ppermute | solution.py:300
  68.8 9.4 %collective-permute-start.13 = (bf16[256,256]{1,0:T(8,128)(2,1)S(1)}, bf16[256,256]{1,0:T(8,128)(2,1)S(1)}, u32[]{:S(2)}, u32[]{:S(2)}) collective-permute-start(bf16[256,256]{1,0:T(8,128)(2,1)S(1)} %get-tuple-element.58), channel_id=1, source_target_pairs={{4,0},{5,1},{6,2},{7,3},{8,4},{9,5},{10,6},{11,7},{12,8},{13,9},{1... | collective-permute-start | bytes 393224 | tf_op jit(solution)/shard_map/ppermute | solution.py:297
  71.1 12.4 %collective-permute-start.10 = (bf16[512,256]{1,0:T(8,128)(2,1)S(1)}, bf16[512,256]{1,0:T(8,128)(2,1)S(1)}, u32[]{:S(2)}, u32[]{:S(2)}) collective-permute-start(bf16[512,256]{1,0:T(8,128)(2,1)S(1)} %get-tuple-element.55), channel_id=1, source_target_pairs={{0,2},{1,3},{2,4},{3,5},{4,6},{5,7},{6,8},{7,9},{8,10},{9,11},{10,... | collective-permute-start | bytes 786440 | tf_op jit(solution)/shard_map/ppermute | solution.py:299
  73.8 9.7 %collective-permute-start.9 = (bf16[256,256]{1,0:T(8,128)(2,1)S(1)}, bf16[256,256]{1,0:T(8,128)(2,1)S(1)}, u32[]{:S(2)}, u32[]{:S(2)}) collective-permute-start(bf16[256,256]{1,0:T(8,128)(2,1)S(1)} %get-tuple-element.54), channel_id=1, source_target_pairs={{0,4},{1,5},{2,6},{3,7},{4,8},{5,9},{6,10},{7,11},{8,12},{9,13},{1... | collective-permute-start | bytes 393224 | tf_op jit(solution)/shard_map/ppermute | solution.py:296
  78.4 8.3 %collective-permute-start.15 = (bf16[512,256]{1,0:T(8,128)(2,1)S(1)}, bf16[512,256]{1,0:T(8,128)(2,1)S(1)}, u32[]{:S(2)}, u32[]{:S(2)}) collective-permute-start(bf16[512,256]{1,0:T(8,128)(2,1)S(1)} %add_convert_fusion.1), channel_id=1, source_target_pairs={{2,0},{3,1},{4,2},{5,3},{6,4},{7,5},{8,6},{9,7},{10,8},{11,9},{12,... | collective-permute-start | bytes 786440 | tf_op jit(solution)/shard_map/ppermute | solution.py:305
  83.6 9.4 %collective-permute-start.11 = (bf16[512,256]{1,0:T(8,128)(2,1)S(1)}, bf16[512,256]{1,0:T(8,128)(2,1)S(1)}, u32[]{:S(2)}, u32[]{:S(2)}) collective-permute-start(bf16[512,256]{1,0:T(8,128)(2,1)S(1)} %add_convert_fusion.3), channel_id=1, source_target_pairs={{0,2},{1,3},{2,4},{3,5},{4,6},{5,7},{6,8},{7,9},{8,10},{9,11},{10,... | collective-permute-start | bytes 786440 | tf_op jit(solution)/shard_map/ppermute | solution.py:304
  86.7 8.7 %collective-permute-start.16 = (bf16[512,256]{1,0:T(8,128)(2,1)S(1)}, bf16[512,256]{1,0:T(8,128)(2,1)S(1)}, u32[]{:S(2)}, u32[]{:S(2)}) collective-permute-start(bf16[512,256]{1,0:T(8,128)(2,1)S(1)} %add_convert_fusion), channel_id=1, source_target_pairs={{2,0},{3,1},{4,2},{5,3},{6,4},{7,5},{8,6},{9,7},{10,8},{11,9},{12,... | collective-permute-start | bytes 786440 | tf_op jit(solution)/shard_map/ppermute | solution.py:308
  93.1 10.7 %collective-permute-start.12 = (bf16[512,256]{1,0:T(8,128)(2,1)S(1)}, bf16[512,256]{1,0:T(8,128)(2,1)S(1)}, u32[]{:S(2)}, u32[]{:S(2)}) collective-permute-start(bf16[512,256]{1,0:T(8,128)(2,1)S(1)} %add_convert_fusion.2), channel_id=1, source_target_pairs={{0,2},{1,3},{2,4},{3,5},{4,6},{5,7},{6,8},{7,9},{8,10},{9,11},{10,... | collective-permute-start | bytes 786440 | tf_op jit(solution)/shard_map/ppermute | solution.py:307
  105.0 16.8 %copy-start.1 = (bf16[768,256]{1,0:T(8,128)(2,1)S(1)}, bf16[768,256]{1,0:T(8,128)(2,1)}, u32[]{:S(2)}) copy-start(bf16[768,256]{1,0:T(8,128)(2,1)} %get-tuple-element.33) | copy-start | bytes 1179652
  105.0 16.8 %all-to-all-start.1 = ((bf16[32,24,256]{2,1,0:T(8,128)(2,1)}), bf16[32,24,256]{2,1,0:T(8,128)(2,1)S(1)}, u32[]{:S(2)}, u32[]{:S(2)}) async-start(bf16[32,24,256]{2,1,0:T(8,128)(2,1)} %bitcast.12), calls=%async_computation.1 | async-start | bytes 786432 | tf_op jit(solution)/shard_map/all_to_all | solution.py:317
  122.2 14.3 %collective-permute-start.17 = (bf16[256,128]{1,0:T(8,128)(2,1)S(1)}, bf16[256,128]{1,0:T(8,128)(2,1)S(1)}, u32[]{:S(2)}, u32[]{:S(2)}) collective-permute-start(bf16[256,128]{1,0:T(8,128)(2,1)S(1)} %dynamic-slice_convert_fusion), channel_id=1, source_target_pairs={{0,1},{1,0},{2,3},{3,2},{4,5},{5,4},{6,7},{7,6},{8,9},{9,8},{10,11... | collective-permute-start | bytes 196616 | tf_op jit(solution)/shard_map/ppermute | solution.py:321
